TPU v7x, 256 devices: a whole 4x4x8 slice. The times are simulated.
256 devices in a mesh: kv: 64 (over z, y, core), tp: 4 (over x).
Axes of the slice: x: 4, y: 4, z: 8, core: 2. Of those that a mesh axis runs over, the one named last changes fastest.
Arguments:
- x_piece: bfloat16 [1024, 2048], P('kv'), may hold values from -6 to 6
- x_decode: bfloat16 [64, 2048], P('kv'), may hold values from -6 to 6
- norm_gain: float32 [2048], replicated, may hold values from 0.1 to 1.9
- w_query: bfloat16 [2048, 1024], P(None, 'tp'), may hold values from -0.1875 to 0.1875
- w_key: bfloat16 [2048, 1024], P(None, 'tp'), may hold values from -0.1875 to 0.1875
- w_value: bfloat16 [2048, 1024], P(None, 'tp'), may hold values from -0.125 to 0.125
- w_out: bfloat16 [1024, 2048], P(None, 'tp'), may hold values from -0.1875 to 0.1875
- head_gain: float32 [128], replicated, may hold values from 0.1 to 1.9
- lambdas: float32 [8], P('tp'), may hold values from 0.3 to 0.8
- piece_keys: bfloat16 [32768, 8, 128], P('kv', 'tp'), may hold values from -300 to 300
- piece_values: bfloat16 [32768, 8, 128], P('kv', 'tp'), may hold values from -6 to 6
- cache_keys: bfloat16 [64, 2048, 8, 128], P('kv', None, 'tp'), may hold values from -300 to 300
- cache_values: bfloat16 [64, 2048, 8, 128], P('kv', None, 'tp'), may hold values from -6 to 6
- cache_lengths: int32 [64], P('kv'), may hold values from 1 to 2048, as said below
Outputs:
- piece_out: bfloat16 [1024, 2048], P('kv', 'tp')
- decode_out: bfloat16 [64, 2048], P('kv', 'tp')
Inputs may be any that keep to these rules, and one draw needn't show every extreme that they name: `cache_lengths`: some sequence has exactly 2048 filled slots.
All inputs are finite; a program needn't handle non-finite values.
Results may differ from a plain program's by a relative error of at most 0.013.
The roundings to bfloat16 on the way count: a program that leaves them out, or rounds other values in their place, can miss the bound.
Values may be sent and summed in bfloat16 or wider, within the bound.
No kernel may reach another device: no remote copies, remote signals or barrier semaphores. Data moves between devices by JAX's collectives and lax.ppermute only.
A program may use at most 64 MiB of HBM per device.

v0:
```python
import math

import jax
import jax.numpy as jnp
from jax import lax
from jax.sharding import PartitionSpec as P

EPS = 1e-06


def sent_to_all(array, axis):
    length = lax.axis_size(axis)
    return lax.all_to_all(
        jnp.broadcast_to(array[None], (length, *array.shape)), axis, 0, 0, tiled=True
    )


def laid_out(blocks, dim):
    lengths = list(blocks.shape[1:])
    lengths[dim] *= blocks.shape[0]
    return jnp.moveaxis(blocks, 0, dim).reshape(lengths)


def gather_directly(array, axis, dim):
    blocks = sent_to_all(array, axis)
    return laid_out(blocks, dim)


def side_by_side(arrays, axis, split_dim, concat_dim, along):
    ends, at = ([], 0)
    for a in arrays[:-1]:
        at += a.shape[along]
        ends.append(at)
    both = jnp.concatenate(arrays, axis=along)
    return tuple(
        jnp.split(
            lax.all_to_all(both, axis, split_axis=split_dim, concat_axis=concat_dim, tiled=True),
            ends,
            axis=along,
        )
    )


def shards(
    x_piece,
    x_decode,
    norm_gain,
    w_query,
    w_key,
    w_value,
    w_out,
    head_gain,
    lambdas,
    piece_keys,
    piece_values,
    cache_keys,
    cache_values,
    cache_lengths,
):
    piece_rows = x_piece.shape[0]
    local_heads = lambdas.shape[0]
    pair_width = piece_keys.shape[2]
    half_width = pair_width // 2
    value_width = piece_values.shape[2]
    score_scale = 1.0 / math.sqrt(half_width)
    cached = piece_keys.shape[0]
    all_rows = jnp.concatenate([x_piece, x_decode], axis=0)
    row_count = all_rows.shape[0]
    rows32 = all_rows.astype(jnp.float32)
    normed = (
        rows32 * lax.rsqrt(jnp.mean(rows32 * rows32, axis=-1, keepdims=True) + EPS) * norm_gain
    ).astype(jnp.bfloat16)
    queries = (
        jnp.dot(normed, w_query, preferred_element_type=jnp.float32)
        .astype(jnp.bfloat16)
        .reshape(row_count, local_heads, pair_width)
    )
    new_keys = (
        jnp.dot(normed, w_key, preferred_element_type=jnp.float32)
        .astype(jnp.bfloat16)
        .reshape(row_count, local_heads, pair_width)
    )
    new_values = (
        jnp.dot(normed, w_value, preferred_element_type=jnp.float32)
        .astype(jnp.bfloat16)
        .reshape(row_count, local_heads, value_width)
    )
    keys_all = jnp.concatenate([piece_keys, new_keys[:piece_rows]], axis=0)
    values_all = jnp.concatenate([piece_values, new_values[:piece_rows]], axis=0)
    offset = lax.axis_index("kv") * piece_rows
    kv_count = lax.axis_size("kv")
    total_rows = piece_rows * kv_count
    key_index = jnp.arange(cached + piece_rows, dtype=jnp.int32)

    def block_terms(query_block, block_start):
        block_rows = query_block.shape[0]
        query_pos = block_start + jnp.arange(block_rows, dtype=jnp.int32)
        allowed = (key_index[None, :] < cached) | (
            key_index[None, :] - cached + offset <= query_pos[:, None]
        )
        results = []
        for which_map in range(2):
            lower = which_map * half_width
            scores = (
                jnp.einsum(
                    "qhd,khd->hqk",
                    query_block[:, :, lower : lower + half_width],
                    keys_all[:, :, lower : lower + half_width],
                    preferred_element_type=jnp.float32,
                )
                * score_scale
            )
            scores = jnp.where(allowed[None], scores, -jnp.inf)
            row_max = jnp.max(scores, axis=-1)
            weights = jnp.exp(scores - row_max[..., None])
            totals = jnp.sum(weights, axis=-1)
            mixed = jnp.einsum(
                "hqk,khd->qhd",
                weights.astype(jnp.bfloat16),
                values_all,
                preferred_element_type=jnp.float32,
            )
            results += [row_max, totals, mixed.reshape(block_rows, local_heads * value_width)]
        return tuple(results)

    stat_zeros = jnp.zeros((local_heads, total_rows), jnp.float32)
    value_zeros = jnp.zeros((total_rows, local_heads * value_width), jnp.float32)
    initial = (stat_zeros, stat_zeros, value_zeros, stat_zeros, stat_zeros, value_zeros)
    piece = gather_directly(queries[:piece_rows], "kv", 0)
    start = jnp.int32(0)
    block_rows = piece.shape[0]
    nblocks = block_rows // 512
    blocks = piece.reshape(nblocks, 512, local_heads, pair_width)
    starts = 512 * jnp.arange(nblocks, dtype=jnp.int32)
    mapped = lax.map(lambda inputs: block_terms(inputs[0], inputs[1]), (blocks, starts))
    results = []
    for index, entry in enumerate(mapped):
        if index % 3 == 2:
            results.append(entry.reshape(block_rows, local_heads * value_width))
        else:
            results.append(entry.transpose(1, 0, 2).reshape(local_heads, block_rows))
    results = tuple(results)
    updated = []
    for index in range(6):
        along = 0 if index % 3 == 2 else 1
        updated.append(
            lax.dynamic_update_slice_in_dim(initial[index], results[index], start, along)
        )
    partials = tuple(updated)
    moved_values = tuple(
        (
            part.astype(jnp.float32)
            for part in side_by_side(
                (partials[2].astype(jnp.bfloat16), partials[5].astype(jnp.bfloat16)), "kv", 0, 0, 1
            )
        )
    )
    moved_stats = side_by_side((partials[0], partials[1], partials[3], partials[4]), "kv", 1, 1, 0)
    own = []
    for which_map in range(2):
        maxima = moved_stats[2 * which_map].reshape(local_heads, kv_count, piece_rows)
        sums = moved_stats[2 * which_map + 1].reshape(local_heads, kv_count, piece_rows)
        weighted = moved_values[which_map].reshape(kv_count, piece_rows, local_heads * value_width)
        new_max = jnp.max(maxima, axis=1)
        factor = jnp.exp(maxima - new_max[:, None, :])
        value_factor = jnp.repeat(factor.transpose(1, 2, 0), value_width, axis=2)
        own += [new_max, jnp.sum(factor * sums, axis=1), jnp.sum(value_factor * weighted, axis=0)]
    lambda_wide = jnp.repeat(lambdas, value_width)[None, :]
    piece_mixed = own[2] / jnp.repeat(own[1].T, value_width, axis=1) - lambda_wide * own[
        5
    ] / jnp.repeat(own[4].T, value_width, axis=1)
    dec_query = queries[piece_rows:]
    own_keys = new_keys[piece_rows:]
    own_values = new_values[piece_rows:].astype(jnp.float32)
    slot_index = jnp.arange(cache_keys.shape[1], dtype=jnp.int32)
    slot_allowed = slot_index[None, None, :] < cache_lengths[:, None, None]
    dec_results = []
    for which_map in range(2):
        lower = which_map * half_width
        scores = (
            jnp.einsum(
                "bhd,bkhd->bhk",
                dec_query[:, :, lower : lower + half_width],
                cache_keys[:, :, :, lower : lower + half_width],
                preferred_element_type=jnp.float32,
            )
            * score_scale
        )
        scores = jnp.where(slot_allowed, scores, -jnp.inf)
        own_score = (
            jnp.einsum(
                "bhd,bhd->bh",
                dec_query[:, :, lower : lower + half_width],
                own_keys[:, :, lower : lower + half_width],
                preferred_element_type=jnp.float32,
            )
            * score_scale
        )
        row_max = jnp.maximum(jnp.max(scores, axis=-1), own_score)
        weights = jnp.exp(scores - row_max[..., None])
        own_weight = jnp.exp(own_score - row_max)
        totals = jnp.sum(weights, axis=-1) + own_weight
        mixed = jnp.einsum(
            "bhk,bkhd->bhd",
            weights.astype(jnp.bfloat16),
            cache_values,
            preferred_element_type=jnp.float32,
        )
        mixed = mixed + own_weight.astype(jnp.bfloat16).astype(jnp.float32)[..., None] * own_values
        dec_results.append(mixed / totals[..., None])
    dec_mixed = (dec_results[0] - lambdas[None, :, None] * dec_results[1]).reshape(
        -1, local_heads * value_width
    )
    attended = jnp.concatenate([piece_mixed, dec_mixed], axis=0).reshape(
        row_count, local_heads, value_width
    )
    head_out = (
        attended
        * lax.rsqrt(jnp.mean(attended * attended, axis=-1, keepdims=True) + EPS)
        * head_gain
    ).astype(jnp.bfloat16)
    head_out = head_out.reshape(row_count, local_heads * value_width)
    output = jnp.dot(gather_directly(head_out, "tp", 1), w_out, preferred_element_type=jnp.float32)
    output = output.astype(jnp.bfloat16)
    return (output[:piece_rows], output[piece_rows:])


def solution(mesh):
    placed = (
        P("kv", None),
        P("kv", None),
        P(),
        P(None, "tp"),
        P(None, "tp"),
        P(None, "tp"),
        P(None, "tp"),
        P(),
        P("tp"),
        P("kv", "tp", None),
        P("kv", "tp", None),
        P("kv", None, "tp", None),
        P("kv", None, "tp", None),
        P("kv"),
    )
    return jax.shard_map(
        shards,
        mesh=mesh,
        in_specs=placed,
        out_specs=(P("kv", "tp"), P("kv", "tp")),
        check_vma=False,
    )
```

profile of v0, /device:TPU:8, one launch (start us, length us, event | category | flops | bytes accessed | tf_op | source)
XLA Modules:
  0.0 146.6 jit_solution(14942968073056447797)
XLA Ops:
  0.7 1.1 fusion.39
  1.9 1.6 %convolution_convert_fusion.3 = bf16[17,256]{1,0:T(8,128)(2,1)S(1)} fusion(bf16[2048,256]{1,0:T(8,128)(2,1)} %param.19, f32[2048]{0:T(1024)} %param.18, f32[17]{0:T(128)S(1)} %add_rsqrt_fusion.1, bf16[1,2048]{1,0:T(2,128)(2,1)} %param.17, bf16[16,2048]{1,0:T(8,128)(2,1)} %param.16), kind=kOutput, calls=%fused_computation.46 | convolution fusion | flops 18073856 | bytes 1135172 | tf_op jit(solution)/shard_map/dot_general | solution.py:74
  3.5 0.9 broadcast_in_dim.128
  4.4 12.3 %all-to-all-start = ((bf16[64,16,2,128]{3,1,2,0:T(8,128)(2,1)}), bf16[64,16,2,128]{3,1,2,0:T(8,128)(2,1)}, u32[]{:S(2)}, u32[]{:S(2)}) async-start(bf16[64,16,2,128]{3,1,2,0:T(8,128)(2,1)} %broadcast_in_dim.128), calls=%async_computation | async-start | bytes 1048576 | tf_op jit(solution)/shard_map/all_to_all | solution.py:13
  18.4 2.7 %slice_bitcast_fusion = (bf16[2048,2,64]{2,1,0:T(2,128)(2,1)S(1)}, bf16[2048,2,64]{2,1,0:T(2,128)(2,1)}) fusion(bf16[1,2048,2,128]{3,2,1,0:T(2,128)(2,1)S(1)} %copy-done.2), kind=kLoop, calls=%fused_computation.52 | loop fusion | bytes 2097152 | tf_op jit(solution)/shard_map/reshape.52
  22.6 1.1 copy.63
  23.7 1.7 %copy.65 = bf16[512,2,128]{2,0,1:T(8,128)(2,1)} copy(bf16[512,2,128]{2,1,0:T(2,128)(2,1)} %param.26) | data formatting | bytes 524288 | tf_op args[10]
  25.4 1.6 %fusion.33 = f32[2,1,2048]{2,1,0:T(1,128)S(1)} fusion(bf16[2048,2,64]{2,1,0:T(2,128)(2,1)} %get-tuple-element.319, bf16[2,64,1]{1,0,2:T(2,128)(2,1)} %get-tuple-element.331), kind=kOutput, calls=%fused_computation.50 | convolution fusion | flops 524288 | bytes 540928 | tf_op jit(solution)/shard_map/bhd,bkhd->bhk/dot_general | solution.py:181
  27.0 1.7 %fusion.31 = f32[2,1,2048]{2,1,0:T(1,128)} fusion(bf16[2048,2,64]{2,1,0:T(2,128)(2,1)S(1)} %get-tuple-element.318, bf16[2,64,1]{1,0,2:T(2,128)(2,1)} %get-tuple-element.330), kind=kOutput, calls=%fused_computation.48 | convolution fusion | flops 524288 | bytes 540928 | tf_op jit(solution)/shard_map/bhd,bkhd->bhk/dot_general | solution.py:181
  28.7 1.4 fusion.66
  30.6 1.0 convolution_convert_fusion.1
  31.7 1.7 %pad_maximum_fusion.2 = bf16[528,2,128]{2,0,1:T(8,128)(2,1)} fusion(bf16[16,2,128]{2,0,1:T(8,128)(2,1)S(1)} %copy_bitcast_fusion, bf16[512,2,128]{2,0,1:T(8,128)(2,1)} %copy.65), kind=kLoop, calls=%fused_computation.63 | loop fusion | flops 540672 | bytes 540672 | tf_op jit(solution)/shard_map/concatenate | solution.py:89
  33.4 0.8 pad_maximum_fusion.1
  34.7 1.9 %copy.62 = bf16[64,16,2,128]{3,1,0,2:T(8,128)(2,1)} copy(bf16[64,16,2,128]{3,1,2,0:T(8,128)(2,1)} %all-to-all-done) | data formatting | bytes 1048576 | tf_op jit(solution)/shard_map/all_to_all | solution.py:13
  36.6 33.4 %while.24 = (s32[]{:T(128)}, f32[2,2,512]{2,1,0:T(2,128)}, f32[2,2,512]{2,1,0:T(2,128)}, bf16[2,512,256]{2,1,0:T(8,128)(2,1)}, f32[2,2,512]{2,1,0:T(2,128)}, /*i...) while((s32[]{:T(128)}, f32[2,2,512]{2,1,0:T(2,128)}, ...), condition=%wide.region_6.7_spmd.clone.clone, body=%wide.region_1.6_spmd.clone.clone.sunk | while | flops 427669568 | bytes 24839804 | solution.py:135
  36.6 1.2 dynamic_slice.22
  38.6 1.0 constant_dynamic-slice_fusion.2
  39.6 0.9 copy.164
  40.5 1.5 %fusion.97 = f32[2,512,528]{1,2,0:T(8,128)S(1)} fusion(bf16[528,2,128]{0,2,1:T(8,128)(2,1)} %get-tuple-element.467, bf16[512,2,128]{0,2,1:T(8,128)(2,1)} %bitcast.146), kind=kOutput, calls=%fused_computation.24.clone.1 | convolution fusion | flops 69206016 | bytes 2457600 | tf_op jit(solution)/shard_map/while/body/eval_jaxpr/qhd,khd->hqk/dot_general | solution.py:105
  42.1 0.8 fusion.98
  42.9 1.0 fusion.99
  43.9 1.5 %fusion.100 = bf16[2,512,128]{1,2,0:T(8,128)(2,1)} fusion(bf16[528,2,128]{2,0,1:T(8,128)(2,1)S(1)} %copy-done.8, f32[2,512,528]{1,2,0:T(8,128)S(1)} %get-tuple-element.420, f32[2,512]{1,0:T(2,128)S(1)} %get-tuple-element.421, pred[512,528]{0,1:T(8,128)(4,1)S(1)} %compare_or_fusion.2), kind=kOutput, calls=%fused_computation.11.clone.1 | convolution fusion | flops 140574720 | bytes 2969600 | tf_op jit(solution)/shard_map/while/body/eval_jaxpr/hqk,khd->qhd/dot_general | solution.py:117
  45.4 1.8 %copy.165 = bf16[1,512,256]{2,1,0:T(8,128)(2,1)} copy(bf16[1,512,256]{1,2,0:T(8,128)(2,1)} %bitcast.149) | data formatting | bytes 524288 | tf_op jit(solution)/shard_map/while/body/jit(dynamic_update_index_in_dim)/dynamic_update_slice | solution.py:135
  47.3 2.5 %fusion.101 = bf16[2,512,128]{1,2,0:T(8,128)(2,1)} fusion(bf16[528,2,128]{2,0,1:T(8,128)(2,1)} %get-tuple-element.468, f32[2,512,528]{1,2,0:T(8,128)S(1)} %fusion.97, f32[2,512]{1,0:T(2,128)S(1)} %get-tuple-element.422, pred[512,528]{0,1:T(8,128)(4,1)S(1)} %compare_or_fusion.2), kind=kOutput, calls=%fused_computation.12.clone.1 | convolution fusion | flops 140574720 | bytes 2969600 | tf_op jit(solution)/shard_map/while/body/eval_jaxpr/hqk,khd->qhd/dot_general | solution.py:117
  49.7 1.1 copy.166
  50.8 1.8 %constant_dynamic-update-slice_fusion.3 = (bf16[2,512,256]{2,1,0:T(8,128)(2,1)}, bf16[2,512,256]{2,1,0:T(8,128)(2,1)}) fusion(bf16[2,512,256]{2,1,0:T(8,128)(2,1)} %get-tuple-element.450, bf16[1,512,256]{2,1,0:T(8,128)(2,1)} %copy.165, s32[]{:T(128)S(6)} %copy.180, bf16[2,512,256]{2,1,0:T(8,128)(2,1)} %get-tuple-element.447, ...), kind=kLoop, calls=%fused_computation.35.clone.1 | loop fusion | bytes 1048580 | tf_op jit(solution)/shard_map/while/body/jit(dynamic_update_index_in_dim)/dynamic_update_slice | solution.py:135
  53.2 1.2 dynamic_slice.22
  55.3 1.0 constant_dynamic-slice_fusion.2
  56.3 0.9 copy.164
  57.2 1.5 %fusion.97 = f32[2,512,528]{1,2,0:T(8,128)S(1)} fusion(bf16[528,2,128]{0,2,1:T(8,128)(2,1)} %get-tuple-element.467, bf16[512,2,128]{0,2,1:T(8,128)(2,1)} %bitcast.146), kind=kOutput, calls=%fused_computation.24.clone.1 | convolution fusion | flops 69206016 | bytes 2457600 | tf_op jit(solution)/shard_map/while/body/eval_jaxpr/qhd,khd->hqk/dot_general | solution.py:105
  58.7 0.8 fusion.98
  59.6 1.0 fusion.99
  60.6 1.5 %fusion.100 = bf16[2,512,128]{1,2,0:T(8,128)(2,1)} fusion(bf16[528,2,128]{2,0,1:T(8,128)(2,1)S(1)} %copy-done.8, f32[2,512,528]{1,2,0:T(8,128)S(1)} %get-tuple-element.420, f32[2,512]{1,0:T(2,128)S(1)} %get-tuple-element.421, pred[512,528]{0,1:T(8,128)(4,1)S(1)} %compare_or_fusion.2), kind=kOutput, calls=%fused_computation.11.clone.1 | convolution fusion | flops 140574720 | bytes 2969600 | tf_op jit(solution)/shard_map/while/body/eval_jaxpr/hqk,khd->qhd/dot_general | solution.py:117
  62.1 1.8 %copy.165 = bf16[1,512,256]{2,1,0:T(8,128)(2,1)} copy(bf16[1,512,256]{1,2,0:T(8,128)(2,1)} %bitcast.149) | data formatting | bytes 524288 | tf_op jit(solution)/shard_map/while/body/jit(dynamic_update_index_in_dim)/dynamic_update_slice | solution.py:135
  63.9 2.5 %fusion.101 = bf16[2,512,128]{1,2,0:T(8,128)(2,1)} fusion(bf16[528,2,128]{2,0,1:T(8,128)(2,1)} %get-tuple-element.468, f32[2,512,528]{1,2,0:T(8,128)S(1)} %fusion.97, f32[2,512]{1,0:T(2,128)S(1)} %get-tuple-element.422, pred[512,528]{0,1:T(8,128)(4,1)S(1)} %compare_or_fusion.2), kind=kOutput, calls=%fused_computation.12.clone.1 | convolution fusion | flops 140574720 | bytes 2969600 | tf_op jit(solution)/shard_map/while/body/eval_jaxpr/hqk,khd->qhd/dot_general | solution.py:117
  66.4 1.1 copy.166
  67.5 1.8 %constant_dynamic-update-slice_fusion.3 = (bf16[2,512,256]{2,1,0:T(8,128)(2,1)}, bf16[2,512,256]{2,1,0:T(8,128)(2,1)}) fusion(bf16[2,512,256]{2,1,0:T(8,128)(2,1)} %get-tuple-element.450, bf16[1,512,256]{2,1,0:T(8,128)(2,1)} %copy.165, s32[]{:T(128)S(6)} %copy.180, bf16[2,512,256]{2,1,0:T(8,128)(2,1)} %get-tuple-element.447, ...), kind=kLoop, calls=%fused_computation.35.clone.1 | loop fusion | bytes 1048580 | tf_op jit(solution)/shard_map/while/body/jit(dynamic_update_index_in_dim)/dynamic_update_slice | solution.py:135
  74.1 10.4 %all-to-all-start.1 = ((f32[64,1,128]{2,1,0:T(1,128)}), f32[64,1,128]{2,1,0:T(1,128)S(1)}, u32[]{:S(2)}, u32[]{:S(2)}) async-start(f32[64,1,128]{2,1,0:T(1,128)} %reshape.373), calls=%async_computation.1 | async-start | bytes 65536 | tf_op jit(solution)/shard_map/all_to_all | solution.py:37
  84.5 2.3 %pad_maximum_fusion = bf16[64,16,512]{2,1,0:T(8,128)(2,1)} fusion(bf16[64,16,256]{2,1,0:T(8,128)(2,1)} %bitcast.155, bf16[64,16,256]{2,1,0:T(8,128)(2,1)} %bitcast.154), kind=kLoop, calls=%fused_computation.47 | loop fusion | flops 2097152 | bytes 2097152 | tf_op jit(solution)/shard_map/concatenate | solution.py:34
  86.8 6.3 %all-to-all-done.1 = f32[64,1,128]{2,1,0:T(1,128)S(1)} async-done(((f32[64,1,128]{2,1,0:T(1,128)}), f32[64,1,128]{2,1,0:T(1,128)S(1)}, u32[]{:S(2)}, u32[]{:S(2)}) %all-to-all-start.1) | async-done | bytes 32800 | tf_op jit(solution)/shard_map/all_to_all | solution.py:37
  93.2 5.6 %all-to-all-start.2 = ((bf16[64,16,512]{2,1,0:T(8,128)(2,1)}), bf16[64,16,512]{2,1,0:T(8,128)(2,1)S(1)}, u32[]{:S(2)}, u32[]{:S(2)}) async-start(bf16[64,16,512]{2,1,0:T(8,128)(2,1)} %pad_maximum_fusion), calls=%async_computation.2 | async-start | bytes 2097152 | tf_op jit(solution)/shard_map/all_to_all | solution.py:37
  102.0 1.3 copy.78
  103.3 1.3 copy.73
  104.7 22.9 %all-to-all-done.2 = bf16[64,16,512]{2,1,0:T(8,128)(2,1)S(1)} async-done(((bf16[64,16,512]{2,1,0:T(8,128)(2,1)}), bf16[64,16,512]{2,1,0:T(8,128)(2,1)S(1)}, u32[]{:S(2)}, u32[]{:S(2)}) %all-to-all-start.2) | async-done | bytes 1048608 | tf_op jit(solution)/shard_map/all_to_all | solution.py:37
  127.6 1.1 slice_convert_fusion.1
  129.3 1.7 %reshape.353 = f32[64,16,2,128]{3,2,1,0:T(2,128)S(1)} reshape(f32[1024,256]{1,0:T(8,128)} %get-tuple-element.316) | data formatting | bytes 2097152 | tf_op jit(solution)/shard_map/reshape | solution.py:163
  131.0 3.9 %multiply_reduce_fusion = (f32[16,2,128]{2,1,0:T(2,128)S(1)}, f32[16,2,128]{2,1,0:T(2,128)S(1)}) fusion(f32[64,16,2,128]{3,2,1,0:T(2,128)S(1)} %reshape.355, f32[64,16,2]{2,1,0:T(8,128)} %copy.78, f32[64,16,2,128]{3,2,1,0:T(2,128)S(1)} %reshape.353, f32[64,16,2]{2,1,0:T(8,128)} %copy.73), kind=kLoop, calls=%fused_computation.54 | loop fusion | flops 1040384 | bytes 2146304 | tf_op jit(solution)/shard_map/reduce_sum | solution.py:167
  135.4 9.6 %all_to_all.25 = bf16[4,17,256]{2,1,0:T(8,128)(2,1)S(1)} all-to-all(bf16[4,17,256]{2,1,0:T(8,128)(2,1)S(1)} %broadcast_in_dim.136), channel_id=1, replica_groups=mesh['kv'=64,'tp'=4] {'tp'}, dimensions={0} | all-to-all | bytes 69632 | tf_op jit(solution)/shard_map/all_to_all | solution.py:13
  (157 shorter events, 16.4 us)
Async XLA Ops:
  0.6 99.1 %copy-start = (bf16[1,2048,2,128]{3,2,1,0:T(2,128)(2,1)S(1)}, bf16[1,2048,2,128]{3,2,1,0:T(2,128)(2,1)}, u32[]{:S(2)}) copy-start(bf16[1,2048,2,128]{3,2,1,0:T(2,128)(2,1)} %param.28) | copy-start | bytes 3145732
  0.6 16.1 %copy-start.10 = (bf16[1,2048]{1,0:T(2,128)(2,1)S(1)}, bf16[1,2048]{1,0:T(2,128)(2,1)}, u32[]{:S(2)}) copy-start(bf16[1,2048]{1,0:T(2,128)(2,1)} %param.17) | copy-start | bytes 12292
  0.7 16.1 %copy-start.4 = (bf16[16,2048]{1,0:T(8,128)(2,1)S(1)}, bf16[16,2048]{1,0:T(8,128)(2,1)}, u32[]{:S(2)}) copy-start(bf16[16,2048]{1,0:T(8,128)(2,1)} %param.16) | copy-start | bytes 196612
  0.7 16.1 %copy-start.11 = (f32[2048]{0:T(1024)S(1)}, f32[2048]{0:T(1024)}, u32[]{:S(2)}) copy-start(f32[2048]{0:T(1024)} %param.18) | copy-start | bytes 24580
  0.7 16.1 %copy-start.5 = (bf16[2048,256]{1,0:T(8,128)(2,1)S(1)}, bf16[2048,256]{1,0:T(8,128)(2,1)}, u32[]{:S(2)}) copy-start(bf16[2048,256]{1,0:T(8,128)(2,1)} %param.20) | copy-start | bytes 3145732
  0.7 17.8 %copy-start.2 = (bf16[1,2048,2,128]{3,2,1,0:T(2,128)(2,1)S(1)}, bf16[1,2048,2,128]{3,2,1,0:T(2,128)(2,1)}, u32[]{:S(2)}) copy-start(bf16[1,2048,2,128]{3,2,1,0:T(2,128)(2,1)} %param.27) | copy-start | bytes 3145732
  1.9 19.3 %copy-start.22 = (f32[17]{0:T(128)}, f32[17]{0:T(128)S(1)}, u32[]{:S(2)}) copy-start(f32[17]{0:T(128)S(1)} %add_rsqrt_fusion.1) | copy-start | bytes 208
  4.4 30.3 %all-to-all-start = ((bf16[64,16,2,128]{3,1,2,0:T(8,128)(2,1)}), bf16[64,16,2,128]{3,1,2,0:T(8,128)(2,1)}, u32[]{:S(2)}, u32[]{:S(2)}) async-start(bf16[64,16,2,128]{3,1,2,0:T(8,128)(2,1)} %broadcast_in_dim.128), calls=%async_computation | async-start | bytes 1048576 | tf_op jit(solution)/shard_map/all_to_all | solution.py:13
  21.1 9.5 %copy-start.6 = (bf16[2048,256]{1,0:T(8,128)(2,1)S(1)}, bf16[2048,256]{1,0:T(8,128)(2,1)}, u32[]{:S(2)}) copy-start(bf16[2048,256]{1,0:T(8,128)(2,1)} %param.21) | copy-start | bytes 3145732
  30.1 6.5 %copy-start.23 = (f32[2]{0:T(128)}, f32[2]{0:T(128)S(1)}, u32[]{:S(2)}) copy-start(f32[2]{0:T(128)S(1)} %get-tuple-element.279) | copy-start | bytes 28
  31.6 4.9 %copy-start.12 = (bf16[17,256]{1,0:T(8,128)(2,1)}, bf16[17,256]{1,0:T(8,128)(2,1)S(1)}, u32[]{:S(2)}) copy-start(bf16[17,256]{1,0:T(8,128)(2,1)S(1)} %convolution_convert_fusion.1) | copy-start | bytes 26116
  40.5 1.5 %copy-start.1 = (bf16[1,512,2,128]{1,3,2,0:T(8,128)(2,1)S(1)}, bf16[1,512,2,128]{1,3,2,0:T(8,128)(2,1)}, u32[]{:S(2)}) copy-start(bf16[1,512,2,128]{1,3,2,0:T(8,128)(2,1)} %copy.164) | copy-start | bytes 786436 | tf_op jit(solution)/shard_map/while
  40.5 1.6 %copy-start.3 = (bf16[528,2,128]{0,2,1:T(8,128)(2,1)S(1)}, bf16[528,2,128]{0,2,1:T(8,128)(2,1)}, u32[]{:S(2)}) copy-start(bf16[528,2,128]{0,2,1:T(8,128)(2,1)} %get-tuple-element.467) | copy-start | bytes 811012 | tf_op jit(solution)/shard_map/while
  42.9 1.0 copy-start.14
  42.9 1.0 copy-start.16
  42.9 1.0 copy-start.8
  43.9 3.4 %copy-start.15 = (f32[2,2,512]{2,1,0:T(2,128)}, f32[2,2,512]{2,1,0:T(2,128)S(1)}, u32[]{:S(2)}) copy-start(f32[2,2,512]{2,1,0:T(2,128)S(1)} %get-tuple-element.458) | copy-start | bytes 24580 | tf_op jit(solution)/shard_map/while
  43.9 3.3 %copy-start.17 = (f32[2,2,512]{2,1,0:T(2,128)}, f32[2,2,512]{2,1,0:T(2,128)S(1)}, u32[]{:S(2)}) copy-start(f32[2,2,512]{2,1,0:T(2,128)S(1)} %get-tuple-element.459) | copy-start | bytes 24580 | tf_op jit(solution)/shard_map/while
  47.2 5.4 %copy-start.18 = (f32[2,2,512]{2,1,0:T(2,128)S(1)}, f32[2,2,512]{2,1,0:T(2,128)}, u32[]{:S(2)}) copy-start(f32[2,2,512]{2,1,0:T(2,128)} %get-tuple-element.448) | copy-start | bytes 24580 | tf_op jit(solution)/shard_map/while
  47.2 5.4 %copy-start.20 = (f32[2,2,512]{2,1,0:T(2,128)S(1)}, f32[2,2,512]{2,1,0:T(2,128)}, u32[]{:S(2)}) copy-start(f32[2,2,512]{2,1,0:T(2,128)} %get-tuple-element.449) | copy-start | bytes 24580 | tf_op jit(solution)/shard_map/while
  52.6 0.6 copy-start.19
  52.6 0.6 copy-start.21
  57.2 1.5 %copy-start.1 = (bf16[1,512,2,128]{1,3,2,0:T(8,128)(2,1)S(1)}, bf16[1,512,2,128]{1,3,2,0:T(8,128)(2,1)}, u32[]{:S(2)}) copy-start(bf16[1,512,2,128]{1,3,2,0:T(8,128)(2,1)} %copy.164) | copy-start | bytes 786436 | tf_op jit(solution)/shard_map/while
  57.2 1.5 %copy-start.3 = (bf16[528,2,128]{0,2,1:T(8,128)(2,1)S(1)}, bf16[528,2,128]{0,2,1:T(8,128)(2,1)}, u32[]{:S(2)}) copy-start(bf16[528,2,128]{0,2,1:T(8,128)(2,1)} %get-tuple-element.467) | copy-start | bytes 811012 | tf_op jit(solution)/shard_map/while
  59.5 1.0 copy-start.14
  59.5 1.0 copy-start.16
  59.6 1.0 copy-start.8
  60.5 3.4 %copy-start.15 = (f32[2,2,512]{2,1,0:T(2,128)}, f32[2,2,512]{2,1,0:T(2,128)S(1)}, u32[]{:S(2)}) copy-start(f32[2,2,512]{2,1,0:T(2,128)S(1)} %get-tuple-element.458) | copy-start | bytes 24580 | tf_op jit(solution)/shard_map/while
  60.6 3.3 %copy-start.17 = (f32[2,2,512]{2,1,0:T(2,128)}, f32[2,2,512]{2,1,0:T(2,128)S(1)}, u32[]{:S(2)}) copy-start(f32[2,2,512]{2,1,0:T(2,128)S(1)} %get-tuple-element.459) | copy-start | bytes 24580 | tf_op jit(solution)/shard_map/while
  63.9 5.4 %copy-start.18 = (f32[2,2,512]{2,1,0:T(2,128)S(1)}, f32[2,2,512]{2,1,0:T(2,128)}, u32[]{:S(2)}) copy-start(f32[2,2,512]{2,1,0:T(2,128)} %get-tuple-element.448) | copy-start | bytes 24580 | tf_op jit(solution)/shard_map/while
  63.9 5.4 %copy-start.20 = (f32[2,2,512]{2,1,0:T(2,128)S(1)}, f32[2,2,512]{2,1,0:T(2,128)}, u32[]{:S(2)}) copy-start(f32[2,2,512]{2,1,0:T(2,128)} %get-tuple-element.449) | copy-start | bytes 24580 | tf_op jit(solution)/shard_map/while
  69.3 0.6 copy-start.19
  69.3 0.6 copy-start.21
  74.1 24.7 %copy-start.25 = (f32[2]{0:T(128)S(1)}, f32[2]{0:T(128)}, u32[]{:S(2)}) copy-start(f32[2]{0:T(128)} %get-tuple-element.280) | copy-start | bytes 28
  74.1 24.7 %copy-start.28 = (f32[2]{0:T(128)S(1)}, f32[2]{0:T(128)}, u32[]{:S(2)}) copy-start(f32[2]{0:T(128)} %get-tuple-element.282) | copy-start | bytes 28
  74.1 24.7 %copy-start.9 = (f32[2,1,2048]{2,1,0:T(1,128)S(1)}, f32[2,1,2048]{2,1,0:T(1,128)}, u32[]{:S(2)}) copy-start(f32[2,1,2048]{2,1,0:T(1,128)} %fusion.31) | copy-start | bytes 49156
  74.1 24.7 %copy-start.13 = (pred[2048]{0:T(1024)(128)(4,1)S(1)}, pred[2048]{0:T(1024)(128)(4,1)}, u32[]{:S(2)}) copy-start(pred[2048]{0:T(1024)(128)(4,1)} %iota_compare_fusion.1) | copy-start | bytes 6148
  74.1 24.9 %copy-start.29 = (f32[128]{0:T(128)S(1)}, f32[128]{0:T(128)}, u32[]{:S(2)}) copy-start(f32[128]{0:T(128)} %param.23) | copy-start | bytes 1540
  74.1 25.6 %copy-start.24 = (f32[2]{0:T(128)S(1)}, f32[2]{0:T(128)}, u32[]{:S(2)}) copy-start(f32[2]{0:T(128)} %copy-done.23) | copy-start | bytes 28
  74.1 25.6 %copy-start.27 = (f32[2]{0:T(128)S(1)}, f32[2]{0:T(128)}, u32[]{:S(2)}) copy-start(f32[2]{0:T(128)} %get-tuple-element.281) | copy-start | bytes 28
  74.1 19.1 %all-to-all-start.1 = ((f32[64,1,128]{2,1,0:T(1,128)}), f32[64,1,128]{2,1,0:T(1,128)S(1)}, u32[]{:S(2)}, u32[]{:S(2)}) async-start(f32[64,1,128]{2,1,0:T(1,128)} %reshape.373), calls=%async_computation.1 | async-start | bytes 65536 | tf_op jit(solution)/shard_map/all_to_all | solution.py:37
  86.8 13.4 %copy-start.26 = (f32[2]{0:T(128)S(1)}, f32[2]{0:T(128)}, u32[]{:S(2)}) copy-start(f32[2]{0:T(128)} %param.24) | copy-start | bytes 28
  93.2 34.4 %all-to-all-start.2 = ((bf16[64,16,512]{2,1,0:T(8,128)(2,1)}), bf16[64,16,512]{2,1,0:T(8,128)(2,1)S(1)}, u32[]{:S(2)}, u32[]{:S(2)}) async-start(bf16[64,16,512]{2,1,0:T(8,128)(2,1)} %pad_maximum_fusion), calls=%async_computation.2 | async-start | bytes 2097152 | tf_op jit(solution)/shard_map/all_to_all | solution.py:37
  131.0 14.1 %copy-start.7 = (bf16[1024,512]{1,0:T(8,128)(2,1)S(1)}, bf16[1024,512]{1,0:T(8,128)(2,1)}, u32[]{:S(2)}) copy-start(bf16[1024,512]{1,0:T(8,128)(2,1)} %param.22) | copy-start | bytes 3145732
where the time goes:
time: 148 us; the launch traced here: 147 us
  local copies, waits for them, and re-layouts  37.1 us (25%)
  waiting for transfers between devices  29.2 us (20%)
  starting transfers between devices  28.3 us (19%)
  other arithmetic  20.6 us (14%)
  matrix products  19.6 us (13%)
  blocking collectives  9.63 us (7%)
  between operations  1.86 us (1%)
    all_to_all x2, waiting for transfers between devices, side_by_side(): lax.all_to_all(both, axis, split_axis=split_dim, concat_axis=concat_dim,...  29.2 us
    all_to_all x2, starting transfers between devices, side_by_side(): lax.all_to_all(both, axis, split_axis=split_dim, concat_axis=concat_dim,...  16 us
    all_to_all x1, starting transfers between devices, sent_to_all(): lax.all_to_all(jnp.broadcast_to(array[None], (length, *array.shape)), axi...  12.3 us
    all_to_all x1, blocking collectives, sent_to_all(): lax.all_to_all(jnp.broadcast_to(array[None], (length, *array.shape)), axi...  9.63 us
    dynamic_update_slice x10, local copies, waits for them, and re-layouts, shards(): lax.map(lambda inputs: block_terms(inputs[0], inputs[1]), (blocks, starts))  9.45 us
    dot_general x4, matrix products, block_terms(): jnp.einsum('hqk,khd->qhd', weights.astype(jnp.bfloat16), values_all, pref...  7.99 us
    dynamic_slice x6, local copies, waits for them, and re-layouts, shards(): lax.map(lambda inputs: block_terms(inputs[0], inputs[1]), (blocks, starts))  6.17 us
    dot_general x4, matrix products, block_terms(): jnp.einsum('qhd,khd->hqk', query_block[:, :, lower:lower + half_width], k...  4.66 us
  transfers between devices with their start and end apart: 3, of which 2 were waited for; matrix products, arithmetic and copies ran while one was open for 17% of the time, Pallas kernels for 0%

commit v1 on v0

v1 whole, which is shorter than its diff:
```python
import math

import jax
import jax.numpy as jnp
from jax import lax
from jax.experimental import pallas as pl
from jax.experimental.pallas import tpu as pltpu
from jax.sharding import PartitionSpec as P

EPS = 1e-06
SHARE = 2
NEG = -jnp.inf
F32 = jnp.float32
BF16 = jnp.bfloat16
MIB = 1024 * 1024


def nt_dot(a, b):
    return lax.dot_general(a, b, (((1,), (1,)), ((), ())), preferred_element_type=F32)


def nn_dot(a, b):
    return lax.dot_general(a, b, (((1,), (0,)), ((), ())), preferred_element_type=F32)


def lane_iota(shape):
    return lax.broadcasted_iota(jnp.int32, shape, len(shape) - 1)


def rms(rows, gain):
    return rows * lax.rsqrt(jnp.mean(rows * rows, axis=-1, keepdims=True) + EPS) * gain


def vmem(count):
    return [pl.BlockSpec(memory_space=pltpu.VMEM)] * count


def prep_body(keys, values, out, wide):
    slots = keys.shape[0] // 2
    for index, source in enumerate((keys, values)):
        wide[index] = source[...].astype(F32)
        for head in range(2):
            out[2 * index + head] = wide[index, pl.ds(head, slots, stride=2), :].astype(BF16)


def prep(keys, values):
    rows = keys.shape[0]
    return pl.pallas_call(
        prep_body,
        out_shape=jax.ShapeDtypeStruct((4, rows // 2, 128), BF16),
        in_specs=vmem(2),
        out_specs=vmem(1)[0],
        scratch_shapes=[pltpu.VMEM((2, rows, 128), F32)],
        compiler_params=pltpu.CompilerParams(vmem_limit_bytes=8 * MIB),
        cost_estimate=pl.CostEstimate(flops=10**8, bytes_accessed=MIB, transcendentals=0),
        name="prep",
    )(keys, values)


def query_body(x, x_dec, gain, w, out, out_dec, normed):
    rows = x.shape[0]
    normed[:rows] = rms(x[...].astype(F32), gain[...]).astype(BF16)
    normed[rows:] = jnp.broadcast_to(
        rms(x_dec[...].astype(F32), gain[...]).astype(BF16), (16, x.shape[1])
    )
    result = nn_dot(normed[...], w[...]).astype(BF16)
    for member in range(out.shape[0]):
        out[member] = result[:rows]
    out_dec[...] = result[rows : rows + 1]


def query_rows(x, x_dec, gain, w, members):
    rows, width = x.shape
    return pl.pallas_call(
        query_body,
        out_shape=(
            jax.ShapeDtypeStruct((members, rows, w.shape[1]), BF16),
            jax.ShapeDtypeStruct((1, w.shape[1]), BF16),
        ),
        in_specs=vmem(4),
        out_specs=tuple(vmem(2)),
        scratch_shapes=[pltpu.VMEM((rows + 16, width), BF16)],
        compiler_params=pltpu.CompilerParams(vmem_limit_bytes=8 * MIB),
        cost_estimate=pl.CostEstimate(flops=10**8, bytes_accessed=MIB, transcendentals=0),
        name="query_rows",
    )(x, x_dec, gain, w)


def decode_body(count, *refs):
    xs = refs[:count]
    (x_dec, gain, w_key, w_value, q_dec, keys, values, length, lambdas, head_gain) = refs[
        count : count + 10
    ]
    k_out, v_out, head_out, normed = refs[count + 10 :]
    rows = xs[0].shape[0]
    for slot, x in enumerate(xs):
        normed[slot * rows : (slot + 1) * rows] = rms(x[...].astype(F32), gain[...]).astype(BF16)
    total = rows * count
    normed[total:] = jnp.broadcast_to(
        rms(x_dec[...].astype(F32), gain[...]).astype(BF16), (16, x_dec.shape[1])
    )
    new_keys = nn_dot(normed[...], w_key[...]).astype(BF16)
    new_values = nn_dot(normed[...], w_value[...]).astype(BF16)
    k_out[...] = new_keys[:total]
    v_out[...] = new_values[:total]

    row = lax.broadcasted_iota(jnp.int32, (8, 128), 0)
    lane = lane_iota((8, 128))
    second = (row // 2) % 2 == 1

    def per_head(line):
        line = line.astype(F32)
        return jnp.where(
            second,
            jnp.broadcast_to(line[:, 128:], (8, 128)),
            jnp.broadcast_to(line[:, :128], (8, 128)),
        )

    half = lane // 64 == row % 2
    queries = jnp.where(half, per_head(q_dec[...]), 0.0)
    own_keys = per_head(new_keys[total : total + 1])
    own_values = per_head(new_values[total : total + 1])
    scale = 0.125 * math.log2(math.e)
    scores = nt_dot(queries.astype(BF16), keys[...])
    width = keys.shape[0]
    column = lane_iota((8, width))
    wide_row = lax.broadcasted_iota(jnp.int32, (8, width), 0)
    allowed = (column % 2 == (wide_row // 2) % 2) & (column // 2 < length[0])
    scores = jnp.where(allowed, scores, NEG)
    own_score = jnp.sum(queries * own_keys, axis=-1, keepdims=True)
    row_max = jnp.maximum(jnp.max(scores, axis=-1, keepdims=True), own_score)
    weights = jnp.exp2((scores - row_max) * scale)
    own_weight = jnp.exp2((own_score - row_max) * scale)
    totals = jnp.sum(weights, axis=-1, keepdims=True) + own_weight
    mixed = nn_dot(weights.astype(BF16), values[...])
    mixed = (mixed + own_weight.astype(BF16).astype(F32) * own_values) / totals
    for head in range(2):
        attended = mixed[2 * head : 2 * head + 1] - lambdas[head] * mixed[2 * head + 1 : 2 * head + 2]
        head_out[:, head * 128 : (head + 1) * 128] = rms(attended, head_gain[...]).astype(BF16)


def decode(xs, x_dec, gain, w_key, w_value, q_dec, keys, values, length, lambdas, head_gain):
    count = len(xs)
    rows, width = xs[0].shape
    smem = pl.BlockSpec(memory_space=pltpu.SMEM)
    return pl.pallas_call(
        lambda *refs: decode_body(count, *refs),
        out_shape=(
            jax.ShapeDtypeStruct((count * rows, 256), BF16),
            jax.ShapeDtypeStruct((count * rows, 256), BF16),
            jax.ShapeDtypeStruct((1, 256), BF16),
        ),
        in_specs=vmem(count + 7) + [smem, smem] + vmem(1),
        out_specs=tuple(vmem(3)),
        scratch_shapes=[pltpu.VMEM((count * rows + 16, width), BF16)],
        compiler_params=pltpu.CompilerParams(vmem_limit_bytes=16 * MIB),
        cost_estimate=pl.CostEstimate(flops=2 * 10**9, bytes_accessed=4 * MIB, transcendentals=0),
        name="decode",
    )(*xs, x_dec, gain, w_key, w_value, q_dec, keys, values, length, lambdas, head_gain)


def attend_body(count, *refs):
    device, queries = refs[:2]
    pools = refs[2 : 2 + count]
    k_new, v_new, out = refs[2 + count :]
    rows = queries.shape[0]
    fresh = k_new.shape[0]
    each = fresh // count
    scale = 0.125 * math.log2(math.e)
    me = device[0]
    block = min(256, rows)
    key_lane = lane_iota((block, fresh))
    key_pos = each * jnp.bitwise_xor(key_lane // each, me) + key_lane % each
    row = lax.broadcasted_iota(jnp.int32, (block, fresh), 0)
    lane = lane_iota((block, 128))
    for start in range(0, rows, block):
        at = row + start
        row_pos = each * (count * (at // each) + lax.rem(me, count)) + at % each
        allowed = key_pos <= row_pos
        stats = jnp.zeros((block, 128), F32)
        for head in range(2):
            cols = slice(head * 128, (head + 1) * 128)
            q = queries[start : start + block, cols].astype(F32)
            for which in range(2):
                combo = 2 * head + which
                kept = (lane < 64) if which == 0 else (lane >= 64)
                masked = jnp.where(kept, q, 0.0).astype(BF16)
                scores = [nt_dot(masked, pool[head]) for pool in pools]
                last = jnp.where(allowed, nt_dot(masked, k_new[:, cols]), NEG)
                row_max = jnp.max(last, axis=-1, keepdims=True)
                for s in scores:
                    row_max = jnp.maximum(row_max, jnp.max(s, axis=-1, keepdims=True))
                weights = jnp.exp2((last - row_max) * scale)
                total = jnp.sum(weights, axis=-1, keepdims=True)
                mixed = nn_dot(weights.astype(BF16), v_new[:, cols])
                for s, pool in zip(scores, pools):
                    weights = jnp.exp2((s - row_max) * scale)
                    total = total + jnp.sum(weights, axis=-1, keepdims=True)
                    mixed = mixed + nn_dot(weights.astype(BF16), pool[2 + head])
                mixed = mixed / total
                out[start : start + block, combo * 128 : (combo + 1) * 128] = mixed.astype(BF16)
                for base, stat in ((0, row_max), (4, total)):
                    for part in range(3):
                        piece = stat.astype(BF16).astype(F32)
                        stats = jnp.where(lane == 8 * part + base + combo, piece, stats)
                        stat = stat - piece
        out[start : start + block, 512:640] = stats.astype(BF16)


def attend(device, queries, pools, k_new, v_new):
    count = len(pools)
    rows = queries.shape[0]
    keys = count * pools[0].shape[1] + k_new.shape[0]
    return pl.pallas_call(
        lambda *refs: attend_body(count, *refs),
        out_shape=jax.ShapeDtypeStruct((rows, 640), BF16),
        in_specs=[pl.BlockSpec(memory_space=pltpu.SMEM)] + vmem(count + 3),
        out_specs=vmem(1)[0],
        compiler_params=pltpu.CompilerParams(vmem_limit_bytes=32 * MIB),
        cost_estimate=pl.CostEstimate(
            flops=4 * rows * keys * 512, bytes_accessed=2 * MIB, transcendentals=4 * rows * keys
        ),
        name="attend",
    )(device, queries, *pools, k_new, v_new)


def combine_body(parts, dec_out, lambdas, head_gain, out):
    scale = 0.125 * math.log2(math.e)
    members = parts.shape[0]
    rows = parts.shape[1]

    def whole(member):
        pieces = parts[member, :, 512:640].astype(F32)
        return pieces + pltpu.roll(pieces, 120, 1) + pltpu.roll(pieces, 112, 1)

    stats = [whole(member) for member in range(members)]
    top = stats[0]
    for s in stats[1:]:
        top = jnp.maximum(top, s)
    shares = [jnp.exp2((s - top) * scale) * pltpu.roll(s, 124, 1) for s in stats]
    total = shares[0]
    for s in shares[1:]:
        total = total + s
    sums = []
    for combo in range(4):
        acc = jnp.zeros((rows, 128), F32)
        for member in range(members):
            acc = acc + shares[member][:, combo : combo + 1] * parts[
                member, :, combo * 128 : (combo + 1) * 128
            ].astype(F32)
        sums.append(acc / total[:, combo : combo + 1])
    heads = []
    for head in range(2):
        attended = sums[2 * head] - lambdas[head] * sums[2 * head + 1]
        heads.append(rms(attended, head_gain[...]).astype(BF16))
    for copy in range(out.shape[0]):
        for head in range(2):
            out[copy, :rows, head * 128 : (head + 1) * 128] = heads[head]
        out[copy, rows:, :] = jnp.broadcast_to(dec_out[...], (out.shape[1] - rows, 256))


def combine(parts, dec_out, lambdas, head_gain, copies):
    return pl.pallas_call(
        combine_body,
        out_shape=jax.ShapeDtypeStruct((copies, parts.shape[1] + 8, 256), BF16),
        in_specs=vmem(2) + [pl.BlockSpec(memory_space=pltpu.SMEM)] + vmem(1),
        out_specs=vmem(1)[0],
        compiler_params=pltpu.CompilerParams(vmem_limit_bytes=16 * MIB),
        cost_estimate=pl.CostEstimate(flops=10**8, bytes_accessed=MIB, transcendentals=0),
        name="combine",
    )(parts, dec_out, lambdas, head_gain)


def out_body(heads, w, piece, dec):
    rows = piece.shape[0]
    acc = nn_dot(heads[0], w[:256])
    for copy in range(1, heads.shape[0]):
        acc = acc + nn_dot(heads[copy], w[copy * 256 : (copy + 1) * 256])
    piece[...] = acc[:rows].astype(BF16)
    dec[...] = acc[rows : rows + 1].astype(BF16)


def out_rows(heads, w, rows):
    return pl.pallas_call(
        out_body,
        out_shape=(
            jax.ShapeDtypeStruct((rows, w.shape[1]), BF16),
            jax.ShapeDtypeStruct((1, w.shape[1]), BF16),
        ),
        in_specs=vmem(2),
        out_specs=tuple(vmem(2)),
        compiler_params=pltpu.CompilerParams(vmem_limit_bytes=8 * MIB),
        cost_estimate=pl.CostEstimate(flops=10**8, bytes_accessed=MIB, transcendentals=0),
        name="out_rows",
    )(heads, w)


def shards(
    x_piece,
    x_decode,
    norm_gain,
    w_query,
    w_key,
    w_value,
    w_out,
    head_gain,
    lambdas,
    piece_keys,
    piece_values,
    cache_keys,
    cache_values,
    cache_lengths,
):
    kv_count = lax.axis_size("kv")
    tp_count = lax.axis_size("tp")
    members = kv_count // SHARE
    rows = x_piece.shape[0]
    groups = [[SHARE * m + e for m in range(members)] for e in range(SHARE)]
    gain = norm_gain.reshape(1, -1)
    head_gain = head_gain.reshape(1, -1)
    me = lax.axis_index("kv").reshape(1)

    def swap(array, bit):
        return lax.ppermute(array, "kv", [(i, i ^ bit) for i in range(kv_count)])

    pools = [prep(piece_keys.reshape(-1, 128), piece_values.reshape(-1, 128))]
    xs = [x_piece]
    bit = SHARE // 2
    while bit:
        pools, xs = (
            [p for pool in pools for p in (pool, swap(pool, bit))],
            [p for x in xs for p in (x, swap(x, bit))],
        )
        bit //= 2

    sent, q_dec = query_rows(x_piece, x_decode, gain, w_query, members)
    got = lax.all_to_all(sent, "kv", 0, 0, tiled=True, axis_index_groups=groups)
    k_new, v_new, dec_out = decode(
        xs,
        x_decode,
        gain,
        w_key,
        w_value,
        q_dec,
        cache_keys.reshape(-1, 128),
        cache_values.reshape(-1, 128),
        cache_lengths,
        lambdas,
        head_gain,
    )
    parts = attend(me, got.reshape(members * rows, 256), pools, k_new, v_new)
    parts = lax.all_to_all(
        parts.reshape(members, rows, 640), "kv", 0, 0, tiled=True, axis_index_groups=groups
    )
    heads = combine(parts, dec_out, lambdas, head_gain, tp_count)
    heads = lax.all_to_all(heads, "tp", 0, 0, tiled=True)
    return out_rows(heads, w_out, rows)


def solution(mesh):
    placed = (
        P("kv", None),
        P("kv", None),
        P(),
        P(None, "tp"),
        P(None, "tp"),
        P(None, "tp"),
        P(None, "tp"),
        P(),
        P("tp"),
        P("kv", "tp", None),
        P("kv", "tp", None),
        P("kv", None, "tp", None),
        P("kv", None, "tp", None),
        P("kv"),
    )
    return jax.shard_map(
        shards,
        mesh=mesh,
        in_specs=placed,
        out_specs=(P("kv", "tp"), P("kv", "tp")),
        check_vma=False,
    )
```

time: 148 us -> 72.5 us (0.49)
  local copies, waits for them, and re-layouts: 37.1 us -> 8.56 us
  blocking collectives: 9.63 us -> 35 us
  waiting for transfers between devices: 29.2 us -> 4.93 us
  other arithmetic: 20.6 us -> 0 us
  matrix products: 19.6 us -> 0 us
  starting transfers between devices: 28.3 us -> 12 us
  Pallas kernels: 0 us -> 10 us
    all_to_all x1 -> x2, blocking collectives: 9.63 us -> 35 us  [the longest x1 25.3 us: shards(): lax.all_to_all(parts.reshape(members, rows, 640), 'kv', 0, 0, tiled=True,...]
    all_to_all x3 -> x1, waiting for transfers between devices: 29.2 us -> 4.37 us  [shards(): got = lax.all_to_all(sent, 'kv', 0, 0, tiled=True, axis_index_groups=groups)]
    dot_general x16 -> x0, matrix products: 19.6 us -> none  [the longest x4 7.99 us: block_terms(): jnp.einsum('hqk,khd->qhd', weights.astype(jnp.bfloat16), values_all, pref...]
    all_to_all x3 -> x1, starting transfers between devices: 28.3 us -> 11.8 us  [shards(): got = lax.all_to_all(sent, 'kv', 0, 0, tiled=True, axis_index_groups=groups)]
    pallas_call x0 -> x6, Pallas kernels: none -> 10 us  [the longest x1 5.02 us: attend(): pl.pallas_call(lambda *refs: attend_body(count, *refs), out_shape=jax.Sha...]
    dynamic_update_slice x10 -> x0, local copies, waits for them, and re-layouts: 9.45 us -> none  [shards(): lax.map(lambda inputs: block_terms(inputs[0], inputs[1]), (blocks, starts))]
    reduce_sum x7 -> x0, other arithmetic: 7.5 us -> none  [the longest x1 3.94 us: shards(): jnp.sum(value_factor * weighted, axis=0)]
    dynamic_slice x6 -> x0, local copies, waits for them, and re-layouts: 6.17 us -> none  [shards(): lax.map(lambda inputs: block_terms(inputs[0], inputs[1]), (blocks, starts))]
  transfers between devices with their start and end apart: 3 -> 3, of which waited for: 2 -> 2; matrix products, arithmetic and copies ran while one was open for 17% -> 0% of each run, Pallas kernels for 0% -> 4%
where the time goes in v1:
time: 72.5 us; the launch traced here: 71.9 us
  blocking collectives  35 us (48%)
  starting transfers between devices  12 us (17%)
  Pallas kernels  10 us (14%)
  local copies, waits for them, and re-layouts  8.56 us (12%)
  waiting for transfers between devices  4.93 us (7%)
  between operations  1.43 us (2%)
    all_to_all x1, blocking collectives, shards(): lax.all_to_all(parts.reshape(members, rows, 640), 'kv', 0, 0, tiled=True,...  25.3 us
    all_to_all x1, starting transfers between devices, shards(): got = lax.all_to_all(sent, 'kv', 0, 0, tiled=True, axis_index_groups=groups)  11.8 us
    all_to_all x1, blocking collectives, shards(): heads = lax.all_to_all(heads, 'tp', 0, 0, tiled=True)  9.64 us
    unnamed x32, local copies, waits for them, and re-layouts  8.56 us
    pallas_call x1, Pallas kernels, attend(): pl.pallas_call(lambda *refs: attend_body(count, *refs), out_shape=jax.Sha...  5.02 us
    all_to_all x1, waiting for transfers between devices, shards(): got = lax.all_to_all(sent, 'kv', 0, 0, tiled=True, axis_index_groups=groups)  4.37 us
    pallas_call x1, Pallas kernels, decode(): pl.pallas_call(lambda *refs: decode_body(count, *refs), out_shape=(jax.Sh...  1.78 us
  transfers between devices with their start and end apart: 3, of which 2 were waited for; matrix products, arithmetic and copies ran while one was open for 0% of the time, Pallas kernels for 4%

profile of v1, /device:TPU:8, one launch (start us, length us, event | category | flops | bytes accessed | tf_op | source)
XLA Modules:
  0.0 71.9 jit_solution(17378729101113400397)
XLA Ops:
  0.6 0.0 copy-start
  0.6 0.0 copy-start.2
  0.7 1.0 %copy-done.2 = bf16[512,2,128]{2,1,0:T(2,128)(2,1)S(1)} copy-done((bf16[512,2,128]{2,1,0:T(2,128)(2,1)S(1)}, bf16[512,2,128]{2,1,0:T(2,128)(2,1)}, u32[]{:S(2)}) %copy-start.2) | copy-done | bytes 262168
  1.7 0.0 copy-start.3
  1.7 0.9 %copy-done.3 = bf16[512,2,128]{2,1,0:T(2,128)(2,1)S(1)} copy-done((bf16[512,2,128]{2,1,0:T(2,128)(2,1)S(1)}, bf16[512,2,128]{2,1,0:T(2,128)(2,1)}, u32[]{:S(2)}) %copy-start.3) | copy-done | bytes 262168
  2.6 0.1 prep.1.refs_2_
  2.8 0.1 collective-permute-start
  2.9 0.0 copy-done
  2.9 0.0 copy-start.4
  2.9 0.8 %copy-done.4 = bf16[16,2048]{1,0:T(8,128)(2,1)S(1)} copy-done((bf16[16,2048]{1,0:T(8,128)(2,1)S(1)}, bf16[16,2048]{1,0:T(8,128)(2,1)}, u32[]{:S(2)}) %copy-start.4) | copy-done | bytes 65560
  3.7 0.0 copy-start.6
  3.7 0.7 copy-done.6
  4.4 0.0 copy-start.8
  4.4 0.7 copy-done.8
  5.1 0.0 copy-start.12
  5.1 1.1 %query_rows.1 = (bf16[32,16,256]{2,1,0:T(8,128)(2,1)}, bf16[1,256]{1,0:T(2,128)(2,1)S(1)}) custom-call(bf16[16,2048]{1,0:T(8,128)(2,1)S(1)} %copy-done.4, bf16[1,2048]{1,0:T(2,128)(2,1)S(1)} %copy-done.6, f32[1,2048]{1,0:T(1,128)S(1)} %bitcast.13, bf16[2048,256]{1,0:T(8,128)(2,1)S(1)} %copy-done), custom_call_target="tpu_custom_call" | custom-call | flops 100000000 | bytes 1048576 | tf_op jit(solution)/shard_map/query_rows/pallas_call | solution.py:74
  6.2 0.0 copy-start.5
  6.2 11.8 %all-to-all-start = ((bf16[32,16,256]{2,1,0:T(8,128)(2,1)}), bf16[32,16,256]{2,1,0:T(8,128)(2,1)S(1)}, u32[]{:S(2)}, u32[]{:S(2)}) async-start(bf16[32,16,256]{2,1,0:T(8,128)(2,1)} %get-tuple-element.7), calls=%async_computation | async-start | bytes 524288 | tf_op jit(solution)/shard_map/all_to_all | solution.py:337
  18.0 0.0 copy-done.5
  18.0 0.1 collective-permute-start.1
  18.1 0.0 copy-start.9
  18.2 0.0 copy-start.7
  18.8 0.6 collective-permute-done.1.refs_1_
  19.4 0.0 copy-start.10
  19.4 0.0 copy-start.11
  19.4 0.0 copy-done.12
  19.4 0.0 copy-done.9
  19.4 0.0 copy-done.7
  19.4 0.6 copy-done.10
  20.0 0.0 copy-done.11
  20.1 0.0 copy-start.13
  20.1 1.2 %copy-done.13 = bf16[2048,256]{1,0:T(8,128)(2,1)S(1)} copy-done((bf16[2048,256]{1,0:T(8,128)(2,1)S(1)}, bf16[2048,256]{1,0:T(8,128)(2,1)}, u32[]{:S(2)}) %copy-start.13) | copy-done | bytes 1048600
  21.3 0.0 copy-start.14
  21.3 1.2 %copy-done.14 = bf16[1,2048,2,128]{3,2,1,0:T(2,128)(2,1)S(1)} copy-done((bf16[1,2048,2,128]{3,2,1,0:T(2,128)(2,1)S(1)}, bf16[1,2048,2,128]{3,2,1,0:T(2,128)(2,1)}, u32[]{:S(2)}) %copy-start.14) | copy-done | bytes 1048600
  22.5 0.0 copy-start.15
  22.5 1.2 %copy-done.15 = bf16[1,2048,2,128]{3,2,1,0:T(2,128)(2,1)S(1)} copy-done((bf16[1,2048,2,128]{3,2,1,0:T(2,128)(2,1)S(1)}, bf16[1,2048,2,128]{3,2,1,0:T(2,128)(2,1)}, u32[]{:S(2)}) %copy-start.15) | copy-done | bytes 1048600
  23.7 1.8 %decode.1 = (bf16[32,256]{1,0:T(8,128)(2,1)S(1)}, bf16[32,256]{1,0:T(8,128)(2,1)S(1)}, bf16[1,256]{1,0:T(2,128)(2,1)S(1)}) custom-call(bf16[16,2048]{1,0:T(8,128)(2,1)S(1)} %copy-done.5, bf16[16,2048]{1,0:T(8,128)(2,1)S(1)} %collective-permute-done.1.refs_1_, bf16[1,2048]{1,0:T(2,128)(2,1)S(1)} %copy-done.7, f32[1,2048]{1,0:T(1,128)S(1)} %bitcast.14, ...), custom_call_target="tpu_custom_call" | custom-call | flops 2000000000 | bytes 4194304 | tf_op jit(solution)/shard_map/decode/pallas_call | solution.py:146
  25.5 4.4 %all-to-all-done = bf16[32,16,256]{2,1,0:T(8,128)(2,1)S(1)} async-done(((bf16[32,16,256]{2,1,0:T(8,128)(2,1)}), bf16[32,16,256]{2,1,0:T(8,128)(2,1)S(1)}, u32[]{:S(2)}, u32[]{:S(2)}) %all-to-all-start) | async-done | bytes 262176 | tf_op jit(solution)/shard_map/all_to_all | solution.py:337
  29.9 0.0 collective-permute-done.refs_3_
  29.9 5.0 %attend.1 = bf16[512,640]{1,0:T(8,128)(2,1)S(1)} custom-call(s32[1]{0:T(128)} %bitcast.refs_0_, bf16[512,256]{1,0:T(8,128)(2,1)S(1)} %bitcast.10, bf16[4,512,128]{2,1,0:T(8,128)(2,1)S(1)} %prep.1.refs_2_, bf16[4,512,128]{2,1,0:T(8,128)(2,1)S(1)} %collective-permute-done.refs_3_, bf16[32,256]{1,0:T(8,128)(2,1)S(1)} %get-tuple-element.9.refs_4_, ...), custom_call_target="tpu_custom_call" | custom-call | flops 1107296256 | bytes 2097152 | tf_op jit(solution)/shard_map/attend/pallas_call | solution.py:214
  34.9 0.0 copy-start.1
  34.9 25.3 %all_to_all.15.parts = bf16[32,16,640]{2,1,0:T(8,128)(2,1)S(1)} all-to-all(bf16[32,16,640]{2,1,0:T(8,128)(2,1)S(1)} %bitcast.9), channel_id=1, replica_groups={{0,8,16,24,32,40,48,56,64,72,80,88,96,104,112,120,128,136,144,152,160,1..., dimensions={0} | all-to-all | bytes 1310720 | tf_op jit(solution)/shard_map/all_to_all | solution.py:352
  60.3 1.1 %combine.1 = bf16[4,24,256]{2,1,0:T(8,128)(2,1)S(1)} custom-call(bf16[32,16,640]{2,1,0:T(8,128)(2,1)S(1)} %all_to_all.15.parts, bf16[1,256]{1,0:T(2,128)(2,1)S(1)} %get-tuple-element.11.dec_out, f32[2]{0:T(128)S(1)} %copy-done.10, f32[1,128]{1,0:T(1,128)S(1)} %bitcast.16), custom_call_target="tpu_custom_call" | custom-call | flops 100000000 | bytes 1048576 | tf_op jit(solution)/shard_map/combine/pallas_call | solution.py:263
  61.4 9.6 %all_to_all.16.heads = bf16[4,24,256]{2,1,0:T(8,128)(2,1)S(1)} all-to-all(bf16[4,24,256]{2,1,0:T(8,128)(2,1)S(1)} %combine.1), channel_id=1, replica_groups=mesh['kv'=64,'tp'=4] {'tp'}, dimensions={0} | all-to-all | bytes 98304 | tf_op jit(solution)/shard_map/all_to_all | solution.py:356
  71.0 0.0 copy-done.1
  71.0 0.9 %out_rows.1 = (bf16[16,512]{1,0:T(8,128)(2,1)}, bf16[1,512]{1,0:T(2,128)(2,1)}) custom-call(bf16[4,24,256]{2,1,0:T(8,128)(2,1)S(1)} %all_to_all.16.heads, bf16[1024,512]{1,0:T(8,128)(2,1)S(1)} %copy-done.1), custom_call_target="tpu_custom_call" | custom-call | flops 100000000 | bytes 1048576 | tf_op jit(solution)/shard_map/out_rows/pallas_call | solution.py:284
Async XLA Ops:
  0.6 2.2 %copy-start = (bf16[2048,256]{1,0:T(8,128)(2,1)S(1)}, bf16[2048,256]{1,0:T(8,128)(2,1)}, u32[]{:S(2)}) copy-start(bf16[2048,256]{1,0:T(8,128)(2,1)} %w.2) | copy-start | bytes 3145732
  0.6 1.0 %copy-start.2 = (bf16[512,2,128]{2,1,0:T(2,128)(2,1)S(1)}, bf16[512,2,128]{2,1,0:T(2,128)(2,1)}, u32[]{:S(2)}) copy-start(bf16[512,2,128]{2,1,0:T(2,128)(2,1)} %param.23) | copy-start | bytes 786436
  1.7 0.9 %copy-start.3 = (bf16[512,2,128]{2,1,0:T(2,128)(2,1)S(1)}, bf16[512,2,128]{2,1,0:T(2,128)(2,1)}, u32[]{:S(2)}) copy-start(bf16[512,2,128]{2,1,0:T(2,128)(2,1)} %param.24) | copy-start | bytes 786436
  2.8 27.1 %collective-permute-start = (bf16[4,512,128]{2,1,0:T(8,128)(2,1)S(1)}, bf16[4,512,128]{2,1,0:T(8,128)(2,1)S(1)}, u32[]{:S(2)}, u32[]{:S(2)}) collective-permute-start(bf16[4,512,128]{2,1,0:T(8,128)(2,1)S(1)} %prep.1.refs_2_), channel_id=1, source_target_pairs={{0,4},{4,0},{8,12},{12,8},{16,20},{20,16},{24,28},{28,24},{32,36},... | collective-permute-start | bytes 1572872 | tf_op jit(solution)/shard_map/ppermute | solution.py:324
  2.9 0.8 %copy-start.4 = (bf16[16,2048]{1,0:T(8,128)(2,1)S(1)}, bf16[16,2048]{1,0:T(8,128)(2,1)}, u32[]{:S(2)}) copy-start(bf16[16,2048]{1,0:T(8,128)(2,1)} %refs_0_.1) | copy-start | bytes 196612
  3.7 0.7 copy-start.6
  4.4 0.7 copy-start.8
  5.1 14.3 %copy-start.12 = (bf16[2048,256]{1,0:T(8,128)(2,1)S(1)}, bf16[2048,256]{1,0:T(8,128)(2,1)}, u32[]{:S(2)}) copy-start(bf16[2048,256]{1,0:T(8,128)(2,1)} %refs_4_.1) | copy-start | bytes 3145732
  6.2 11.8 %copy-start.5 = (bf16[16,2048]{1,0:T(8,128)(2,1)S(1)}, bf16[16,2048]{1,0:T(8,128)(2,1)}, u32[]{:S(2)}) copy-start(bf16[16,2048]{1,0:T(8,128)(2,1)} %refs_0_.1) | copy-start | bytes 196612
  6.2 23.7 %all-to-all-start = ((bf16[32,16,256]{2,1,0:T(8,128)(2,1)}), bf16[32,16,256]{2,1,0:T(8,128)(2,1)S(1)}, u32[]{:S(2)}, u32[]{:S(2)}) async-start(bf16[32,16,256]{2,1,0:T(8,128)(2,1)} %get-tuple-element.7), calls=%async_computation | async-start | bytes 524288 | tf_op jit(solution)/shard_map/all_to_all | solution.py:337
  18.0 1.3 %collective-permute-start.1 = (bf16[16,2048]{1,0:T(8,128)(2,1)S(1)}, bf16[16,2048]{1,0:T(8,128)(2,1)S(1)}, u32[]{:S(2)}, u32[]{:S(2)}) collective-permute-start(bf16[16,2048]{1,0:T(8,128)(2,1)S(1)} %copy-done.5), channel_id=1, source_target_pairs={{0,4},{4,0},{8,12},{12,8},{16,20},{20,16},{24,28},{28,24},{32,36},... | collective-permute-start | bytes 196616 | tf_op jit(solution)/shard_map/ppermute | solution.py:324
  18.1 1.3 %copy-start.9 = (f32[2048]{0:T(1024)S(1)}, f32[2048]{0:T(1024)}, u32[]{:S(2)}) copy-start(f32[2048]{0:T(1024)} %param.16) | copy-start | bytes 24580
  18.2 1.2 %copy-start.7 = (bf16[1,2048]{1,0:T(2,128)(2,1)S(1)}, bf16[1,2048]{1,0:T(2,128)(2,1)}, u32[]{:S(2)}) copy-start(bf16[1,2048]{1,0:T(2,128)(2,1)} %refs_2_.1) | copy-start | bytes 12292
  19.4 0.7 copy-start.10
  19.4 0.7 copy-start.11
  20.1 1.2 %copy-start.13 = (bf16[2048,256]{1,0:T(8,128)(2,1)S(1)}, bf16[2048,256]{1,0:T(8,128)(2,1)}, u32[]{:S(2)}) copy-start(bf16[2048,256]{1,0:T(8,128)(2,1)} %refs_5_.1) | copy-start | bytes 3145732
  21.3 1.2 %copy-start.14 = (bf16[1,2048,2,128]{3,2,1,0:T(2,128)(2,1)S(1)}, bf16[1,2048,2,128]{3,2,1,0:T(2,128)(2,1)}, u32[]{:S(2)}) copy-start(bf16[1,2048,2,128]{3,2,1,0:T(2,128)(2,1)} %param.25) | copy-start | bytes 3145732
  22.5 1.2 %copy-start.15 = (bf16[1,2048,2,128]{3,2,1,0:T(2,128)(2,1)S(1)}, bf16[1,2048,2,128]{3,2,1,0:T(2,128)(2,1)}, u32[]{:S(2)}) copy-start(bf16[1,2048,2,128]{3,2,1,0:T(2,128)(2,1)} %param.26) | copy-start | bytes 3145732
  34.9 36.1 %copy-start.1 = (bf16[1024,512]{1,0:T(8,128)(2,1)S(1)}, bf16[1024,512]{1,0:T(8,128)(2,1)}, u32[]{:S(2)}) copy-start(bf16[1024,512]{1,0:T(8,128)(2,1)} %w.3) | copy-start | bytes 3145732

commit v2 on v1

--- a/solution.py
+++ b/solution.py
@@ -8,7 +8,7 @@
 from jax.sharding import PartitionSpec as P
 
 EPS = 1e-06
-SHARE = 2
+SHARE = 4
 NEG = -jnp.inf
 F32 = jnp.float32
 BF16 = jnp.bfloat16
@@ -35,74 +35,95 @@
     return [pl.BlockSpec(memory_space=pltpu.VMEM)] * count
 
 
-def prep_body(keys, values, out, wide):
+HBM = pl.BlockSpec(memory_space=pltpu.HBM)
+
+
+def fetch(pairs, sems):
+    copies = [pltpu.make_async_copy(a, b, sems.at[i]) for i, (a, b) in enumerate(pairs)]
+    for copy in copies:
+        copy.start()
+    return copies
+
+
+def opening_body(
+    keys, values, x, x_dec, gain, w, pool, out, out_dec, kv, xs, xd, g, wq, wide, normed, sems
+):
+    copies = fetch(
+        (
+            (x, xs),
+            (x_dec, xd),
+            (gain, g),
+            (keys, kv.at[0]),
+            (values, kv.at[1]),
+            (w, wq),
+        ),
+        sems,
+    )
     slots = keys.shape[0] // 2
-    for index, source in enumerate((keys, values)):
-        wide[index] = source[...].astype(F32)
+    rows = x.shape[0]
+    for copy in copies[:3]:
+        copy.wait()
+    normed[:rows] = rms(xs[...].astype(F32), g[...]).astype(BF16)
+    normed[rows:] = jnp.broadcast_to(
+        rms(xd[...].astype(F32), g[...]).astype(BF16), (16, x.shape[1])
+    )
+    for tile in range(x.shape[1] // 128):
+        at = slots + rows * (tile // 4)
+        pool[tile % 4, at : at + rows, :] = xs[:, tile * 128 : (tile + 1) * 128]
+    for index in range(2):
+        copies[3 + index].wait()
+        wide[index] = kv[index].astype(F32)
         for head in range(2):
-            out[2 * index + head] = wide[index, pl.ds(head, slots, stride=2), :].astype(BF16)
-
-
-def prep(keys, values):
-    rows = keys.shape[0]
-    return pl.pallas_call(
-        prep_body,
-        out_shape=jax.ShapeDtypeStruct((4, rows // 2, 128), BF16),
-        in_specs=vmem(2),
-        out_specs=vmem(1)[0],
-        scratch_shapes=[pltpu.VMEM((2, rows, 128), F32)],
-        compiler_params=pltpu.CompilerParams(vmem_limit_bytes=8 * MIB),
-        cost_estimate=pl.CostEstimate(flops=10**8, bytes_accessed=MIB, transcendentals=0),
-        name="prep",
-    )(keys, values)
-
-
-def query_body(x, x_dec, gain, w, out, out_dec, normed):
-    rows = x.shape[0]
-    normed[:rows] = rms(x[...].astype(F32), gain[...]).astype(BF16)
-    normed[rows:] = jnp.broadcast_to(
-        rms(x_dec[...].astype(F32), gain[...]).astype(BF16), (16, x.shape[1])
-    )
-    result = nn_dot(normed[...], w[...]).astype(BF16)
+            pool[2 * index + head, :slots] = wide[index, pl.ds(head, slots, stride=2), :].astype(
+                BF16
+            )
+    copies[5].wait()
+    result = nn_dot(normed[...], wq[...]).astype(BF16)
     for member in range(out.shape[0]):
         out[member] = result[:rows]
     out_dec[...] = result[rows : rows + 1]
 
 
-def query_rows(x, x_dec, gain, w, members):
+def opening(keys, values, x, x_dec, gain, w, members):
     rows, width = x.shape
-    return pl.pallas_call(
-        query_body,
+    slots = keys.shape[0] // 2
+    return pl.pallas_call(
+        opening_body,
         out_shape=(
+            jax.ShapeDtypeStruct((4, slots + rows * width // 512, 128), BF16),
             jax.ShapeDtypeStruct((members, rows, w.shape[1]), BF16),
             jax.ShapeDtypeStruct((1, w.shape[1]), BF16),
         ),
-        in_specs=vmem(4),
-        out_specs=tuple(vmem(2)),
-        scratch_shapes=[pltpu.VMEM((rows + 16, width), BF16)],
-        compiler_params=pltpu.CompilerParams(vmem_limit_bytes=8 * MIB),
-        cost_estimate=pl.CostEstimate(flops=10**8, bytes_accessed=MIB, transcendentals=0),
-        name="query_rows",
-    )(x, x_dec, gain, w)
-
-
-def decode_body(count, *refs):
-    xs = refs[:count]
-    (x_dec, gain, w_key, w_value, q_dec, keys, values, length, lambdas, head_gain) = refs[
-        count : count + 10
-    ]
-    k_out, v_out, head_out, normed = refs[count + 10 :]
-    rows = xs[0].shape[0]
-    for slot, x in enumerate(xs):
-        normed[slot * rows : (slot + 1) * rows] = rms(x[...].astype(F32), gain[...]).astype(BF16)
-    total = rows * count
-    normed[total:] = jnp.broadcast_to(
-        rms(x_dec[...].astype(F32), gain[...]).astype(BF16), (16, x_dec.shape[1])
-    )
-    new_keys = nn_dot(normed[...], w_key[...]).astype(BF16)
-    new_values = nn_dot(normed[...], w_value[...]).astype(BF16)
-    k_out[...] = new_keys[:total]
-    v_out[...] = new_values[:total]
+        in_specs=[HBM] * 6,
+        out_specs=tuple(vmem(3)),
+        scratch_shapes=[
+            pltpu.VMEM((2, 2 * slots, 128), BF16),
+            pltpu.VMEM((rows, width), BF16),
+            pltpu.VMEM((1, width), BF16),
+            pltpu.VMEM((1, width), F32),
+            pltpu.VMEM(w.shape, BF16),
+            pltpu.VMEM((2, 2 * slots, 128), F32),
+            pltpu.VMEM((rows + 16, width), BF16),
+            pltpu.SemaphoreType.DMA((6,)),
+        ],
+        compiler_params=pltpu.CompilerParams(vmem_limit_bytes=60 * 1024 * 1024),
+        cost_estimate=pl.CostEstimate(flops=10**9, bytes_accessed=2 * MIB, transcendentals=0),
+        name="opening",
+    )(keys, values, x, x_dec, gain, w)
+
+
+def decode_body(
+    x_dec, gain, w_key, w_value, q_dec, keys, values, length, lambdas, head_gain, head_out,
+    xd, g, wk, wv, kc, vc, sems
+):
+    copies = fetch(
+        ((x_dec, xd), (gain, g), (w_key, wk), (keys, kc), (w_value, wv), (values, vc)), sems
+    )
+    for copy in copies[:2]:
+        copy.wait()
+    normed = jnp.broadcast_to(rms(xd[...].astype(F32), g[...]).astype(BF16), (16, xd.shape[1]))
+    copies[2].wait()
+    new_keys = nn_dot(normed, wk[...]).astype(BF16)[:1]
 
     row = lax.broadcasted_iota(jnp.int32, (8, 128), 0)
     lane = lane_iota((8, 128))
@@ -118,10 +139,10 @@
 
     half = lane // 64 == row % 2
     queries = jnp.where(half, per_head(q_dec[...]), 0.0)
-    own_keys = per_head(new_keys[total : total + 1])
-    own_values = per_head(new_values[total : total + 1])
+    own_keys = per_head(new_keys)
     scale = 0.125 * math.log2(math.e)
-    scores = nt_dot(queries.astype(BF16), keys[...])
+    copies[3].wait()
+    scores = nt_dot(queries.astype(BF16), kc[...])
     width = keys.shape[0]
     column = lane_iota((8, width))
     wide_row = lax.broadcasted_iota(jnp.int32, (8, width), 0)
@@ -132,34 +153,79 @@
     weights = jnp.exp2((scores - row_max) * scale)
     own_weight = jnp.exp2((own_score - row_max) * scale)
     totals = jnp.sum(weights, axis=-1, keepdims=True) + own_weight
-    mixed = nn_dot(weights.astype(BF16), values[...])
+    copies[4].wait()
+    own_values = per_head(nn_dot(normed, wv[...]).astype(BF16)[:1])
+    copies[5].wait()
+    mixed = nn_dot(weights.astype(BF16), vc[...])
     mixed = (mixed + own_weight.astype(BF16).astype(F32) * own_values) / totals
     for head in range(2):
         attended = mixed[2 * head : 2 * head + 1] - lambdas[head] * mixed[2 * head + 1 : 2 * head + 2]
         head_out[:, head * 128 : (head + 1) * 128] = rms(attended, head_gain[...]).astype(BF16)
 
 
-def decode(xs, x_dec, gain, w_key, w_value, q_dec, keys, values, length, lambdas, head_gain):
-    count = len(xs)
-    rows, width = xs[0].shape
+def decode(x_dec, gain, w_key, w_value, q_dec, keys, values, length, lambdas, head_gain):
     smem = pl.BlockSpec(memory_space=pltpu.SMEM)
     return pl.pallas_call(
-        lambda *refs: decode_body(count, *refs),
-        out_shape=(
-            jax.ShapeDtypeStruct((count * rows, 256), BF16),
-            jax.ShapeDtypeStruct((count * rows, 256), BF16),
-            jax.ShapeDtypeStruct((1, 256), BF16),
-        ),
-        in_specs=vmem(count + 7) + [smem, smem] + vmem(1),
-        out_specs=tuple(vmem(3)),
-        scratch_shapes=[pltpu.VMEM((count * rows + 16, width), BF16)],
-        compiler_params=pltpu.CompilerParams(vmem_limit_bytes=16 * MIB),
+        decode_body,
+        out_shape=jax.ShapeDtypeStruct((1, 256), BF16),
+        in_specs=[HBM] * 4 + vmem(1) + [HBM] * 2 + [smem, smem] + vmem(1),
+        out_specs=vmem(1)[0],
+        scratch_shapes=[
+            pltpu.VMEM(x_dec.shape, BF16),
+            pltpu.VMEM(gain.shape, F32),
+            pltpu.VMEM(w_key.shape, BF16),
+            pltpu.VMEM(w_value.shape, BF16),
+            pltpu.VMEM(keys.shape, BF16),
+            pltpu.VMEM(values.shape, BF16),
+            pltpu.SemaphoreType.DMA((6,)),
+        ],
+        compiler_params=pltpu.CompilerParams(vmem_limit_bytes=60 * 1024 * 1024),
         cost_estimate=pl.CostEstimate(flops=2 * 10**9, bytes_accessed=4 * MIB, transcendentals=0),
         name="decode",
-    )(*xs, x_dec, gain, w_key, w_value, q_dec, keys, values, length, lambdas, head_gain)
-
-
-def attend_body(count, *refs):
+    )(x_dec, gain, w_key, w_value, q_dec, keys, values, length, lambdas, head_gain)
+
+
+def fresh_body(*refs):
+    (gain, w_key, w_value) = refs[:3]
+    pools = refs[3:-6]
+    (k_out, v_out, wk, wv, normed, sems) = refs[-6:]
+    copies = fetch(((w_key, wk), (w_value, wv)), sems)
+    rows = k_out.shape[0] // len(pools)
+    tiles = gain.shape[1] // 128
+    slots = pools[0].shape[1] - rows * tiles // 4
+    for slot, pool in enumerate(pools):
+        parts = []
+        for tile in range(tiles):
+            at = slots + rows * (tile // 4)
+            parts.append(pool[tile % 4, at : at + rows, :])
+        x = jnp.concatenate(parts, axis=1).astype(F32)
+        normed[slot * rows : (slot + 1) * rows] = rms(x, gain[...]).astype(BF16)
+    copies[0].wait()
+    k_out[...] = nn_dot(normed[...], wk[...]).astype(BF16)
+    copies[1].wait()
+    v_out[...] = nn_dot(normed[...], wv[...]).astype(BF16)
+
+
+def fresh(gain, w_key, w_value, pools, rows):
+    total = rows * len(pools)
+    return pl.pallas_call(
+        fresh_body,
+        out_shape=(jax.ShapeDtypeStruct((total, 256), BF16),) * 2,
+        in_specs=vmem(1) + [HBM] * 2 + vmem(len(pools)),
+        out_specs=tuple(vmem(2)),
+        scratch_shapes=[
+            pltpu.VMEM(w_key.shape, BF16),
+            pltpu.VMEM(w_value.shape, BF16),
+            pltpu.VMEM((total, gain.shape[1]), BF16),
+            pltpu.SemaphoreType.DMA((2,)),
+        ],
+        compiler_params=pltpu.CompilerParams(vmem_limit_bytes=8 * MIB),
+        cost_estimate=pl.CostEstimate(flops=10**9, bytes_accessed=2 * MIB, transcendentals=0),
+        name="fresh",
+    )(gain, w_key, w_value, *pools)
+
+
+def attend_body(count, slots, *refs):
     device, queries = refs[:2]
     pools = refs[2 : 2 + count]
     k_new, v_new, out = refs[2 + count :]
@@ -185,7 +251,7 @@
                 combo = 2 * head + which
                 kept = (lane < 64) if which == 0 else (lane >= 64)
                 masked = jnp.where(kept, q, 0.0).astype(BF16)
-                scores = [nt_dot(masked, pool[head]) for pool in pools]
+                scores = [nt_dot(masked, pool[head, :slots]) for pool in pools]
                 last = jnp.where(allowed, nt_dot(masked, k_new[:, cols]), NEG)
                 row_max = jnp.max(last, axis=-1, keepdims=True)
                 for s in scores:
@@ -196,7 +262,7 @@
                 for s, pool in zip(scores, pools):
                     weights = jnp.exp2((s - row_max) * scale)
                     total = total + jnp.sum(weights, axis=-1, keepdims=True)
-                    mixed = mixed + nn_dot(weights.astype(BF16), pool[2 + head])
+                    mixed = mixed + nn_dot(weights.astype(BF16), pool[2 + head, :slots])
                 mixed = mixed / total
                 out[start : start + block, combo * 128 : (combo + 1) * 128] = mixed.astype(BF16)
                 for base, stat in ((0, row_max), (4, total)):
@@ -207,12 +273,12 @@
         out[start : start + block, 512:640] = stats.astype(BF16)
 
 
-def attend(device, queries, pools, k_new, v_new):
+def attend(device, queries, pools, slots, k_new, v_new):
     count = len(pools)
     rows = queries.shape[0]
-    keys = count * pools[0].shape[1] + k_new.shape[0]
-    return pl.pallas_call(
-        lambda *refs: attend_body(count, *refs),
+    keys = count * slots + k_new.shape[0]
+    return pl.pallas_call(
+        lambda *refs: attend_body(count, slots, *refs),
         out_shape=jax.ShapeDtypeStruct((rows, 640), BF16),
         in_specs=[pl.BlockSpec(memory_space=pltpu.SMEM)] + vmem(count + 3),
         out_specs=vmem(1)[0],
@@ -295,7 +361,7 @@
     )(heads, w)
 
 
-def shards(
+def layer(
     x_piece,
     x_decode,
     norm_gain,
@@ -323,20 +389,25 @@
     def swap(array, bit):
         return lax.ppermute(array, "kv", [(i, i ^ bit) for i in range(kv_count)])
 
-    pools = [prep(piece_keys.reshape(-1, 128), piece_values.reshape(-1, 128))]
-    xs = [x_piece]
+    pool, sent, q_dec = opening(
+        piece_keys.reshape(-1, 128),
+        piece_values.reshape(-1, 128),
+        x_piece,
+        x_decode,
+        gain,
+        w_query,
+        members,
+    )
+    pools = [pool]
     bit = SHARE // 2
     while bit:
-        pools, xs = (
-            [p for pool in pools for p in (pool, swap(pool, bit))],
-            [p for x in xs for p in (x, swap(x, bit))],
-        )
+        swapped = []
+        for pool in pools:
+            swapped += [pool, swap(pool, bit)]
+        pools = swapped
         bit //= 2
-
-    sent, q_dec = query_rows(x_piece, x_decode, gain, w_query, members)
     got = lax.all_to_all(sent, "kv", 0, 0, tiled=True, axis_index_groups=groups)
-    k_new, v_new, dec_out = decode(
-        xs,
+    dec_out = decode(
         x_decode,
         gain,
         w_key,
@@ -348,7 +419,9 @@
         lambdas,
         head_gain,
     )
-    parts = attend(me, got.reshape(members * rows, 256), pools, k_new, v_new)
+    k_new, v_new = fresh(gain, w_key, w_value, pools, rows)
+    slots = piece_keys.shape[0]
+    parts = attend(me, got.reshape(members * rows, 256), pools, slots, k_new, v_new)
     parts = lax.all_to_all(
         parts.reshape(members, rows, 640), "kv", 0, 0, tiled=True, axis_index_groups=groups
     )
@@ -375,7 +448,7 @@
         P("kv"),
     )
     return jax.shard_map(
-        shards,
+        layer,
         mesh=mesh,
         in_specs=placed,
         out_specs=(P("kv", "tp"), P("kv", "tp")),

time: 72.5 us -> 79.5 us (1.097)
  blocking collectives: 35 us -> 9.63 us
  waiting for transfers between devices: 4.93 us -> 29.4 us
  Pallas kernels: 10 us -> 17.5 us
  starting transfers between devices: 12 us -> 16.2 us
  local copies, waits for them, and re-layouts: 8.56 us -> 4.72 us
    all_to_all x2 -> x1, blocking collectives: 35 us -> 9.63 us  [layer(): heads = lax.all_to_all(heads, 'tp', 0, 0, tiled=True)]
    ppermute x2 -> x3, waiting for transfers between devices: 0.56 us -> 13.1 us  [swap(): return lax.ppermute(array, 'kv', [(i, i ^ bit) for i in range(kv_count)])]
    all_to_all x1 -> x2, waiting for transfers between devices: 4.37 us -> 16.3 us  [the longest x1 9.24 us: layer(): lax.all_to_all(parts.reshape(members, rows, 640), 'kv', 0, 0, tiled=True,...]
    pallas_call x4, Pallas kernels: 8.01 us -> 15.7 us  [the longest x1 5.94 us: attend(): pl.pallas_call(lambda *refs: attend_body(count, slots, *refs), out_shape=...]
    unnamed x32 -> x24, local copies, waits for them, and re-layouts: 8.56 us -> 4.72 us
    all_to_all x1 -> x2, starting transfers between devices: 11.8 us -> 14 us  [the longest x1 10.4 us: layer(): got = lax.all_to_all(sent, 'kv', 0, 0, tiled=True, axis_index_groups=groups)]
    ppermute x2 -> x3, starting transfers between devices: 0.19 us -> 2.25 us  [swap(): return lax.ppermute(array, 'kv', [(i, i ^ bit) for i in range(kv_count)])]
  transfers between devices with their start and end apart: 3 -> 5, of which waited for: 2 -> 3; matrix products, arithmetic and copies ran while one was open for 0% -> 0% of each run, Pallas kernels for 4% -> 9%
where the time goes in v2:
time: 79.5 us; the launch traced here: 79 us
  waiting for transfers between devices  29.4 us (37%)
  Pallas kernels  17.5 us (22%)
  starting transfers between devices  16.2 us (20%)
  blocking collectives  9.63 us (12%)
  local copies, waits for them, and re-layouts  4.72 us (6%)
  between operations  1.43 us (2%)
    ppermute x3, waiting for transfers between devices, swap(): return lax.ppermute(array, 'kv', [(i, i ^ bit) for i in range(kv_count)])  13.1 us
    all_to_all x1, starting transfers between devices, layer(): got = lax.all_to_all(sent, 'kv', 0, 0, tiled=True, axis_index_groups=groups)  10.4 us
    all_to_all x1, blocking collectives, layer(): heads = lax.all_to_all(heads, 'tp', 0, 0, tiled=True)  9.63 us
    all_to_all x1, waiting for transfers between devices, layer(): lax.all_to_all(parts.reshape(members, rows, 640), 'kv', 0, 0, tiled=True,...  9.24 us
    all_to_all x1, waiting for transfers between devices, layer(): got = lax.all_to_all(sent, 'kv', 0, 0, tiled=True, axis_index_groups=groups)  7.08 us
    pallas_call x1, Pallas kernels, attend(): pl.pallas_call(lambda *refs: attend_body(count, slots, *refs), out_shape=...  5.94 us
    unnamed x24, local copies, waits for them, and re-layouts  4.72 us
    pallas_call x1, Pallas kernels, decode(): pl.pallas_call(decode_body, out_shape=jax.ShapeDtypeStruct((1, 256), BF16...  4.65 us
  transfers between devices with their start and end apart: 5, of which 3 were waited for; matrix products, arithmetic and copies ran while one was open for 0% of the time, Pallas kernels for 9%

profile of v2, /device:TPU:8, one launch (start us, length us, event | category | flops | bytes accessed | tf_op | source)
XLA Modules:
  0.0 79.0 jit_solution(3492328011609872937)
XLA Ops:
  0.6 0.0 copy-start
  0.6 0.0 copy-start.1
  0.7 2.6 %opening.1 = (bf16[4,576,128]{2,1,0:T(8,128)(2,1)}, bf16[16,16,256]{2,1,0:T(8,128)(2,1)}, bf16[1,256]{1,0:T(2,128)(2,1)}) custom-call(bf16[1024,128]{1,0:T(8,128)(2,1)} %bitcast.17, bf16[1024,128]{1,0:T(8,128)(2,1)} %bitcast.18, bf16[16,2048]{1,0:T(8,128)(2,1)} %x.1, bf16[1,2048]{1,0:T(2,128)(2,1)} %x_dec.3, f32[1,2048]{1,0:T(1,128)} %bitcast.10, ...), custom_call_target="tpu_custom_call" | custom-call | flops 1000000000 | bytes 2097152 | tf_op jit(solution)/shard_map/opening/pallas_call | solution.py:90
  3.3 2.2 %collective-permute-start.1 = (bf16[4,576,128]{2,1,0:T(8,128)(2,1)}, bf16[4,576,128]{2,1,0:T(8,128)(2,1)S(1)}, u32[]{:S(2)}, u32[]{:S(2)}) collective-permute-start(bf16[4,576,128]{2,1,0:T(8,128)(2,1)} %get-tuple-element.8.refs_3_.refs_2_), channel_id=1, source_target_pairs={{0,8},{4,12},{8,0},{12,4},{16,24},{20,28},{24,16},{28,20},{32,40},... | collective-permute-start | bytes 1769480 | tf_op jit(solution)/shard_map/ppermute | solution.py:390
  5.5 0.0 collective-permute-start
  5.5 13.1 %collective-permute-done.1.refs_5_.refs_4_ = bf16[4,576,128]{2,1,0:T(8,128)(2,1)S(1)} collective-permute-done((bf16[4,576,128]{2,1,0:T(8,128)(2,1)}, bf16[4,576,128]{2,1,0:T(8,128)(2,1)S(1)}, u32[]{:S(2)}, u32[]{:S(2)}) %collective-permute-start.1) | collective-permute-done | bytes 589856 | tf_op jit(solution)/shard_map/ppermute | solution.py:390
  18.6 0.0 collective-permute-start.2
  18.6 0.0 copy-start.5
  18.6 0.8 %copy-done.5 = bf16[4,576,128]{2,1,0:T(8,128)(2,1)} copy-done((bf16[4,576,128]{2,1,0:T(8,128)(2,1)}, bf16[4,576,128]{2,1,0:T(8,128)(2,1)S(1)}, u32[]{:S(2)}) %copy-start.5) | copy-done | bytes 589848
  19.4 0.0 copy-start.8
  19.4 10.4 %all-to-all-start = ((bf16[16,16,256]{2,1,0:T(8,128)(2,1)}), bf16[16,16,256]{2,1,0:T(8,128)(2,1)S(1)}, u32[]{:S(2)}, u32[]{:S(2)}) async-start(bf16[16,16,256]{2,1,0:T(8,128)(2,1)} %get-tuple-element.7), calls=%async_computation | async-start | bytes 262144 | tf_op jit(solution)/shard_map/all_to_all | solution.py:409
  29.9 0.0 collective-permute-done.refs_4_.refs_3_
  29.9 0.0 collective-permute-done.2.refs_6_.refs_5_
  29.9 0.0 copy-done
  29.9 0.0 copy-done.1
  29.9 0.0 copy-done.8
  29.9 0.0 copy-start.3
  30.0 1.1 %copy-done.3 = bf16[4,576,128]{2,1,0:T(8,128)(2,1)S(1)} copy-done((bf16[4,576,128]{2,1,0:T(8,128)(2,1)S(1)}, bf16[4,576,128]{2,1,0:T(8,128)(2,1)}, u32[]{:S(2)}) %copy-start.3) | copy-done | bytes 589848
  31.0 0.0 copy-start.6
  31.0 1.1 %copy-done.6 = bf16[4,576,128]{2,1,0:T(8,128)(2,1)S(1)} copy-done((bf16[4,576,128]{2,1,0:T(8,128)(2,1)S(1)}, bf16[4,576,128]{2,1,0:T(8,128)(2,1)}, u32[]{:S(2)}) %copy-start.6) | copy-done | bytes 589848
  32.1 0.0 copy-start.4
  32.1 2.5 %fresh.1 = (bf16[64,256]{1,0:T(8,128)(2,1)S(1)}, bf16[64,256]{1,0:T(8,128)(2,1)S(1)}) custom-call(f32[1,2048]{1,0:T(1,128)S(1)} %bitcast.12, bf16[2048,256]{1,0:T(8,128)(2,1)S(1)} %copy-done, bf16[2048,256]{1,0:T(8,128)(2,1)S(1)} %copy-done.1, bf16[4,576,128]{2,1,0:T(8,128)(2,1)S(1)} %copy-done.3, bf16[4,576,128]{2,1,0:T(8,128)(2,1)} %collective-permute-done.refs_4_.refs_3_, ...), custom_call_target="tpu_custom_call" | custom-call | flops 1000000000 | bytes 2097152 | tf_op jit(solution)/shard_map/fresh/pallas_call | solution.py:211
  34.5 7.1 %all-to-all-done = bf16[16,16,256]{2,1,0:T(8,128)(2,1)S(1)} async-done(((bf16[16,16,256]{2,1,0:T(8,128)(2,1)}), bf16[16,16,256]{2,1,0:T(8,128)(2,1)S(1)}, u32[]{:S(2)}, u32[]{:S(2)}) %all-to-all-start) | async-done | bytes 131104 | tf_op jit(solution)/shard_map/all_to_all | solution.py:409
  41.6 0.0 copy-done.4
  41.6 0.0 copy-start.7
  41.6 1.1 %copy-done.7 = bf16[4,576,128]{2,1,0:T(8,128)(2,1)S(1)} copy-done((bf16[4,576,128]{2,1,0:T(8,128)(2,1)S(1)}, bf16[4,576,128]{2,1,0:T(8,128)(2,1)}, u32[]{:S(2)}) %copy-start.7) | copy-done | bytes 589848
  42.7 5.9 %attend.1 = bf16[256,640]{1,0:T(8,128)(2,1)} custom-call(s32[1]{0:T(128)} %bitcast.refs_0_, bf16[256,256]{1,0:T(8,128)(2,1)S(1)} %bitcast.9, bf16[4,576,128]{2,1,0:T(8,128)(2,1)S(1)} %copy-done.4, bf16[4,576,128]{2,1,0:T(8,128)(2,1)} %collective-permute-done.refs_4_.refs_3_, bf16[4,576,128]{2,1,0:T(8,128)(2,1)S(1)} %copy-done.7, ...), custom_call_target="tpu_custom_call" | custom-call | flops 1107296256 | bytes 2097152 | tf_op jit(solution)/shard_map/attend/pallas_call | solution.py:280
  48.6 3.5 %all-to-all-start.1 = ((bf16[16,16,640]{2,1,0:T(8,128)(2,1)}), bf16[16,16,640]{2,1,0:T(8,128)(2,1)S(1)}, u32[]{:S(2)}, u32[]{:S(2)}) async-start(bf16[16,16,640]{2,1,0:T(8,128)(2,1)} %bitcast.5), calls=%async_computation.1 | async-start | bytes 655360 | tf_op jit(solution)/shard_map/all_to_all | solution.py:425
  52.8 0.0 copy-start.10
  52.8 0.0 copy-start.11
  52.8 0.0 copy-start.2
  52.9 4.7 %decode.1.dec_out = bf16[1,256]{1,0:T(2,128)(2,1)} custom-call(bf16[1,2048]{1,0:T(2,128)(2,1)} %x_dec.3, f32[1,2048]{1,0:T(1,128)} %bitcast.11, bf16[2048,256]{1,0:T(8,128)(2,1)} %w_key.1, bf16[2048,256]{1,0:T(8,128)(2,1)} %w_value.1, bf16[1,256]{1,0:T(2,128)(2,1)} %get-tuple-element.11.q_dec, bf16[4096,128]{1,0:T(8,128)(2,1)} %bitcast.15, ...), custom_call_target="tpu_custom_call" | custom-call | flops 2000000000 | bytes 4194304 | tf_op jit(solution)/shard_map/decode/pallas_call | solution.py:168
  57.5 9.2 %all-to-all-done.1.parts = bf16[16,16,640]{2,1,0:T(8,128)(2,1)S(1)} async-done(((bf16[16,16,640]{2,1,0:T(8,128)(2,1)}), bf16[16,16,640]{2,1,0:T(8,128)(2,1)S(1)}, u32[]{:S(2)}, u32[]{:S(2)}) %all-to-all-start.1) | async-done | bytes 327712 | tf_op jit(solution)/shard_map/all_to_all | solution.py:425
  66.8 0.0 copy-done.10
  66.8 0.0 copy-done.11
  66.8 0.0 copy-start.9
  66.8 0.7 copy-done.9
  67.5 1.0 %combine.1 = bf16[4,24,256]{2,1,0:T(8,128)(2,1)S(1)} custom-call(bf16[16,16,640]{2,1,0:T(8,128)(2,1)S(1)} %all-to-all-done.1.parts, bf16[1,256]{1,0:T(2,128)(2,1)S(1)} %copy-done.9, f32[2]{0:T(128)S(1)} %copy-done.10, f32[1,128]{1,0:T(1,128)S(1)} %bitcast.14), custom_call_target="tpu_custom_call" | custom-call | flops 100000000 | bytes 1048576 | tf_op jit(solution)/shard_map/combine/pallas_call | solution.py:329
  68.4 9.6 %all_to_all.15.heads = bf16[4,24,256]{2,1,0:T(8,128)(2,1)S(1)} all-to-all(bf16[4,24,256]{2,1,0:T(8,128)(2,1)S(1)} %combine.1), channel_id=1, replica_groups=mesh['kv'=64,'tp'=4] {'tp'}, dimensions={0} | all-to-all | bytes 98304 | tf_op jit(solution)/shard_map/all_to_all | solution.py:429
  78.1 0.0 copy-done.2
  78.1 0.9 %out_rows.1 = (bf16[16,512]{1,0:T(8,128)(2,1)}, bf16[1,512]{1,0:T(2,128)(2,1)}) custom-call(bf16[4,24,256]{2,1,0:T(8,128)(2,1)S(1)} %all_to_all.15.heads, bf16[1024,512]{1,0:T(8,128)(2,1)S(1)} %copy-done.2), custom_call_target="tpu_custom_call" | custom-call | flops 100000000 | bytes 1048576 | tf_op jit(solution)/shard_map/out_rows/pallas_call | solution.py:350
Async XLA Ops:
  0.6 29.3 %copy-start = (bf16[2048,256]{1,0:T(8,128)(2,1)S(1)}, bf16[2048,256]{1,0:T(8,128)(2,1)}, u32[]{:S(2)}) copy-start(bf16[2048,256]{1,0:T(8,128)(2,1)} %w_key.1) | copy-start | bytes 3145732
  0.6 29.3 %copy-start.1 = (bf16[2048,256]{1,0:T(8,128)(2,1)S(1)}, bf16[2048,256]{1,0:T(8,128)(2,1)}, u32[]{:S(2)}) copy-start(bf16[2048,256]{1,0:T(8,128)(2,1)} %w_value.1) | copy-start | bytes 3145732
  3.3 15.4 %collective-permute-start.1 = (bf16[4,576,128]{2,1,0:T(8,128)(2,1)}, bf16[4,576,128]{2,1,0:T(8,128)(2,1)S(1)}, u32[]{:S(2)}, u32[]{:S(2)}) collective-permute-start(bf16[4,576,128]{2,1,0:T(8,128)(2,1)} %get-tuple-element.8.refs_3_.refs_2_), channel_id=1, source_target_pairs={{0,8},{4,12},{8,0},{12,4},{16,24},{20,28},{24,16},{28,20},{32,40},... | collective-permute-start | bytes 1769480 | tf_op jit(solution)/shard_map/ppermute | solution.py:390
  5.5 24.4 %collective-permute-start = (bf16[4,576,128]{2,1,0:T(8,128)(2,1)}, bf16[4,576,128]{2,1,0:T(8,128)(2,1)}, u32[]{:S(2)}, u32[]{:S(2)}) collective-permute-start(bf16[4,576,128]{2,1,0:T(8,128)(2,1)} %get-tuple-element.8.refs_3_.refs_2_), channel_id=1, source_target_pairs={{0,4},{4,0},{8,12},{12,8},{16,20},{20,16},{24,28},{28,24},{32,36},... | collective-permute-start | bytes 1769480 | tf_op jit(solution)/shard_map/ppermute | solution.py:390
  18.6 11.3 %collective-permute-start.2 = (bf16[4,576,128]{2,1,0:T(8,128)(2,1)S(1)}, bf16[4,576,128]{2,1,0:T(8,128)(2,1)}, u32[]{:S(2)}, u32[]{:S(2)}) collective-permute-start(bf16[4,576,128]{2,1,0:T(8,128)(2,1)S(1)} %collective-permute-done.1.refs_5_.refs_4_), channel_id=1, source_target_pairs={{0,4},{4,0},{8,12},{12,8},{16,20},{20,16},{24,28},{28,24},{32,36},... | collective-permute-start | bytes 1769480 | tf_op jit(solution)/shard_map/ppermute | solution.py:390
  18.6 0.8 %copy-start.5 = (bf16[4,576,128]{2,1,0:T(8,128)(2,1)}, bf16[4,576,128]{2,1,0:T(8,128)(2,1)S(1)}, u32[]{:S(2)}) copy-start(bf16[4,576,128]{2,1,0:T(8,128)(2,1)S(1)} %collective-permute-done.1.refs_5_.refs_4_) | copy-start | bytes 1769476
  19.4 10.5 %copy-start.8 = (f32[2048]{0:T(1024)S(1)}, f32[2048]{0:T(1024)}, u32[]{:S(2)}) copy-start(f32[2048]{0:T(1024)} %param.16) | copy-start | bytes 24580
  19.4 22.2 %all-to-all-start = ((bf16[16,16,256]{2,1,0:T(8,128)(2,1)}), bf16[16,16,256]{2,1,0:T(8,128)(2,1)S(1)}, u32[]{:S(2)}, u32[]{:S(2)}) async-start(bf16[16,16,256]{2,1,0:T(8,128)(2,1)} %get-tuple-element.7), calls=%async_computation | async-start | bytes 262144 | tf_op jit(solution)/shard_map/all_to_all | solution.py:409
  29.9 1.1 %copy-start.3 = (bf16[4,576,128]{2,1,0:T(8,128)(2,1)S(1)}, bf16[4,576,128]{2,1,0:T(8,128)(2,1)}, u32[]{:S(2)}) copy-start(bf16[4,576,128]{2,1,0:T(8,128)(2,1)} %get-tuple-element.8.refs_3_.refs_2_) | copy-start | bytes 1769476
  31.0 1.1 %copy-start.6 = (bf16[4,576,128]{2,1,0:T(8,128)(2,1)S(1)}, bf16[4,576,128]{2,1,0:T(8,128)(2,1)}, u32[]{:S(2)}) copy-start(bf16[4,576,128]{2,1,0:T(8,128)(2,1)} %copy-done.5) | copy-start | bytes 1769476
  32.1 9.6 %copy-start.4 = (bf16[4,576,128]{2,1,0:T(8,128)(2,1)S(1)}, bf16[4,576,128]{2,1,0:T(8,128)(2,1)}, u32[]{:S(2)}) copy-start(bf16[4,576,128]{2,1,0:T(8,128)(2,1)} %get-tuple-element.8.refs_3_.refs_2_) | copy-start | bytes 1769476
  41.6 1.1 %copy-start.7 = (bf16[4,576,128]{2,1,0:T(8,128)(2,1)S(1)}, bf16[4,576,128]{2,1,0:T(8,128)(2,1)}, u32[]{:S(2)}) copy-start(bf16[4,576,128]{2,1,0:T(8,128)(2,1)} %copy-done.5) | copy-start | bytes 1769476
  48.6 18.1 %all-to-all-start.1 = ((bf16[16,16,640]{2,1,0:T(8,128)(2,1)}), bf16[16,16,640]{2,1,0:T(8,128)(2,1)S(1)}, u32[]{:S(2)}, u32[]{:S(2)}) async-start(bf16[16,16,640]{2,1,0:T(8,128)(2,1)} %bitcast.5), calls=%async_computation.1 | async-start | bytes 655360 | tf_op jit(solution)/shard_map/all_to_all | solution.py:425
  52.8 13.9 %copy-start.10 = (f32[2]{0:T(128)S(1)}, f32[2]{0:T(128)}, u32[]{:S(2)}) copy-start(f32[2]{0:T(128)} %lambdas.3) | copy-start | bytes 28
  52.8 13.9 %copy-start.11 = (f32[128]{0:T(128)S(1)}, f32[128]{0:T(128)}, u32[]{:S(2)}) copy-start(f32[128]{0:T(128)} %param.21) | copy-start | bytes 1540
  52.8 25.2 %copy-start.2 = (bf16[1024,512]{1,0:T(8,128)(2,1)S(1)}, bf16[1024,512]{1,0:T(8,128)(2,1)}, u32[]{:S(2)}) copy-start(bf16[1024,512]{1,0:T(8,128)(2,1)} %w.3) | copy-start | bytes 3145732
  66.8 0.7 copy-start.9

commit v3 on v2

--- a/solution.py
+++ b/solution.py
@@ -13,6 +13,7 @@
 F32 = jnp.float32
 BF16 = jnp.bfloat16
 MIB = 1024 * 1024
+ATT, FRE, DEC, OPN = 20, 8, 16, 60
 
 
 def nt_dot(a, b):
@@ -46,8 +47,9 @@
 
 
 def opening_body(
-    keys, values, x, x_dec, gain, w, pool, out, out_dec, kv, xs, xd, g, wq, wide, normed, sems
+    keys, values, x, x_dec, gain, w, pool0, pool1, out, out_dec, kv, xs, xd, g, wq, wide, normed, sems
 ):
+    pools = (pool0, pool1)
     copies = fetch(
         (
             (x, xs),
@@ -68,15 +70,14 @@
         rms(xd[...].astype(F32), g[...]).astype(BF16), (16, x.shape[1])
     )
     for tile in range(x.shape[1] // 128):
-        at = slots + rows * (tile // 4)
-        pool[tile % 4, at : at + rows, :] = xs[:, tile * 128 : (tile + 1) * 128]
+        at = slots + rows * (tile // 2)
+        for pool in pools:
+            pool[tile % 2, at : at + rows, :] = xs[:, tile * 128 : (tile + 1) * 128]
     for index in range(2):
         copies[3 + index].wait()
         wide[index] = kv[index].astype(F32)
         for head in range(2):
-            pool[2 * index + head, :slots] = wide[index, pl.ds(head, slots, stride=2), :].astype(
-                BF16
-            )
+            pools[head][index, :slots] = wide[index, pl.ds(head, slots, stride=2), :].astype(BF16)
     copies[5].wait()
     result = nn_dot(normed[...], wq[...]).astype(BF16)
     for member in range(out.shape[0]):
@@ -90,12 +91,13 @@
     return pl.pallas_call(
         opening_body,
         out_shape=(
-            jax.ShapeDtypeStruct((4, slots + rows * width // 512, 128), BF16),
+            jax.ShapeDtypeStruct((2, slots + rows * width // 256, 128), BF16),
+            jax.ShapeDtypeStruct((2, slots + rows * width // 256, 128), BF16),
             jax.ShapeDtypeStruct((members, rows, w.shape[1]), BF16),
             jax.ShapeDtypeStruct((1, w.shape[1]), BF16),
         ),
         in_specs=[HBM] * 6,
-        out_specs=tuple(vmem(3)),
+        out_specs=tuple(vmem(4)),
         scratch_shapes=[
             pltpu.VMEM((2, 2 * slots, 128), BF16),
             pltpu.VMEM((rows, width), BF16),
@@ -106,7 +108,7 @@
             pltpu.VMEM((rows + 16, width), BF16),
             pltpu.SemaphoreType.DMA((6,)),
         ],
-        compiler_params=pltpu.CompilerParams(vmem_limit_bytes=60 * 1024 * 1024),
+        compiler_params=pltpu.CompilerParams(vmem_limit_bytes=OPN * MIB),
         cost_estimate=pl.CostEstimate(flops=10**9, bytes_accessed=2 * MIB, transcendentals=0),
         name="opening",
     )(keys, values, x, x_dec, gain, w)
@@ -179,115 +181,113 @@
             pltpu.VMEM(values.shape, BF16),
             pltpu.SemaphoreType.DMA((6,)),
         ],
-        compiler_params=pltpu.CompilerParams(vmem_limit_bytes=60 * 1024 * 1024),
+        compiler_params=pltpu.CompilerParams(vmem_limit_bytes=DEC * MIB),
         cost_estimate=pl.CostEstimate(flops=2 * 10**9, bytes_accessed=4 * MIB, transcendentals=0),
         name="decode",
     )(x_dec, gain, w_key, w_value, q_dec, keys, values, length, lambdas, head_gain)
 
 
 def fresh_body(*refs):
-    (gain, w_key, w_value) = refs[:3]
-    pools = refs[3:-6]
-    (k_out, v_out, wk, wv, normed, sems) = refs[-6:]
-    copies = fetch(((w_key, wk), (w_value, wv)), sems)
-    rows = k_out.shape[0] // len(pools)
+    gain, w_key, w_value = refs[:3]
+    sources = refs[3:9]
+    k_out, v_out, normed = refs[9:]
+    rows = k_out.shape[0] // 4
     tiles = gain.shape[1] // 128
-    slots = pools[0].shape[1] - rows * tiles // 4
-    for slot, pool in enumerate(pools):
-        parts = []
-        for tile in range(tiles):
-            at = slots + rows * (tile // 4)
-            parts.append(pool[tile % 4, at : at + rows, :])
+    slots = sources[0].shape[1] - rows * tiles // 2
+    for index, source in enumerate(sources):
+        parts = [
+            source[tile % 2, slots + rows * (tile // 2) : slots + rows * (tile // 2 + 1), :]
+            for tile in range(tiles)
+        ]
         x = jnp.concatenate(parts, axis=1).astype(F32)
-        normed[slot * rows : (slot + 1) * rows] = rms(x, gain[...]).astype(BF16)
-    copies[0].wait()
-    k_out[...] = nn_dot(normed[...], wk[...]).astype(BF16)
-    copies[1].wait()
-    v_out[...] = nn_dot(normed[...], wv[...]).astype(BF16)
-
-
-def fresh(gain, w_key, w_value, pools, rows):
-    total = rows * len(pools)
+        normed[index * rows : (index + 1) * rows] = rms(x, gain[...]).astype(BF16)
+    for w, out in ((w_key, k_out), (w_value, v_out)):
+        result = nn_dot(normed[...], w[...]).astype(BF16)
+        out[:, :128] = result[: 4 * rows, :128]
+        out[: 2 * rows, 128:] = result[: 2 * rows, 128:]
+        out[2 * rows :, 128:] = result[4 * rows :, 128:]
+
+
+def fresh(gain, w_key, w_value, pools0, pools1, rows):
+    sources = [*pools0, *pools1[2:]]
+    width = gain.shape[1]
     return pl.pallas_call(
         fresh_body,
-        out_shape=(jax.ShapeDtypeStruct((total, 256), BF16),) * 2,
-        in_specs=vmem(1) + [HBM] * 2 + vmem(len(pools)),
+        out_shape=(jax.ShapeDtypeStruct((4 * rows, 256), BF16),) * 2,
+        in_specs=vmem(9),
         out_specs=tuple(vmem(2)),
-        scratch_shapes=[
-            pltpu.VMEM(w_key.shape, BF16),
-            pltpu.VMEM(w_value.shape, BF16),
-            pltpu.VMEM((total, gain.shape[1]), BF16),
-            pltpu.SemaphoreType.DMA((2,)),
-        ],
-        compiler_params=pltpu.CompilerParams(vmem_limit_bytes=8 * MIB),
+        scratch_shapes=[pltpu.VMEM((6 * rows, width), BF16)],
+        compiler_params=pltpu.CompilerParams(vmem_limit_bytes=FRE * MIB),
         cost_estimate=pl.CostEstimate(flops=10**9, bytes_accessed=2 * MIB, transcendentals=0),
         name="fresh",
-    )(gain, w_key, w_value, *pools)
-
-
-def attend_body(count, slots, *refs):
-    device, queries = refs[:2]
-    pools = refs[2 : 2 + count]
-    k_new, v_new, out = refs[2 + count :]
+    )(gain, w_key, w_value, *sources)
+
+
+def attend_body(slots, *refs):
+    ids, queries = refs[:2]
+    pool = refs[2:10]
+    k_new, v_new, out = refs[10:]
     rows = queries.shape[0]
-    fresh = k_new.shape[0]
-    each = fresh // count
+    fresh_rows = k_new.shape[0]
+    each = fresh_rows // 4
     scale = 0.125 * math.log2(math.e)
-    me = device[0]
-    block = min(256, rows)
-    key_lane = lane_iota((block, fresh))
-    key_pos = each * jnp.bitwise_xor(key_lane // each, me) + key_lane % each
-    row = lax.broadcasted_iota(jnp.int32, (block, fresh), 0)
-    lane = lane_iota((block, 128))
-    for start in range(0, rows, block):
-        at = row + start
-        row_pos = each * (count * (at // each) + lax.rem(me, count)) + at % each
-        allowed = key_pos <= row_pos
-        stats = jnp.zeros((block, 128), F32)
-        for head in range(2):
-            cols = slice(head * 128, (head + 1) * 128)
-            q = queries[start : start + block, cols].astype(F32)
-            for which in range(2):
-                combo = 2 * head + which
-                kept = (lane < 64) if which == 0 else (lane >= 64)
-                masked = jnp.where(kept, q, 0.0).astype(BF16)
-                scores = [nt_dot(masked, pool[head, :slots]) for pool in pools]
-                last = jnp.where(allowed, nt_dot(masked, k_new[:, cols]), NEG)
-                row_max = jnp.max(last, axis=-1, keepdims=True)
-                for s in scores:
-                    row_max = jnp.maximum(row_max, jnp.max(s, axis=-1, keepdims=True))
-                weights = jnp.exp2((last - row_max) * scale)
-                total = jnp.sum(weights, axis=-1, keepdims=True)
-                mixed = nn_dot(weights.astype(BF16), v_new[:, cols])
-                for s, pool in zip(scores, pools):
-                    weights = jnp.exp2((s - row_max) * scale)
-                    total = total + jnp.sum(weights, axis=-1, keepdims=True)
-                    mixed = mixed + nn_dot(weights.astype(BF16), pool[2 + head, :slots])
-                mixed = mixed / total
-                out[start : start + block, combo * 128 : (combo + 1) * 128] = mixed.astype(BF16)
-                for base, stat in ((0, row_max), (4, total)):
-                    for part in range(3):
-                        piece = stat.astype(BF16).astype(F32)
-                        stats = jnp.where(lane == 8 * part + base + combo, piece, stats)
-                        stat = stat - piece
-        out[start : start + block, 512:640] = stats.astype(BF16)
-
-
-def attend(device, queries, pools, slots, k_new, v_new):
-    count = len(pools)
+    me = ids[0]
+    chip = lax.rem(lax.div(me, 2), 4)
+    beyond = lax.rem(chip + 2 * lax.rem(chip, 2) + 3, 4)
+    partners = (jnp.bitwise_xor(me, 2), me + 2 * (beyond - chip))
+    key_lane = lane_iota((rows, fresh_rows))
+    row = lax.broadcasted_iota(jnp.int32, (rows, fresh_rows), 0)
+    row_pos = each * (4 * (row // each) + lax.rem(me, 4)) + row % each
+    lane = lane_iota((rows, 128))
+    stats = jnp.zeros((rows, 128), F32)
+    for head in range(2):
+        partner = partners[head]
+        slot = key_lane // each
+        owner = jnp.bitwise_xor(jnp.where(slot < 2, me, partner), slot % 2)
+        allowed = each * owner + key_lane % each <= row_pos
+        cols = slice(head * 128, (head + 1) * 128)
+        q = queries[:, cols].astype(F32)
+        places = range(4 * head, 4 * head + 4)
+        for which in range(2):
+            combo = 2 * head + which
+            kept = (lane < 64) if which == 0 else (lane >= 64)
+            masked = jnp.where(kept, q, 0.0).astype(BF16)
+            scores = [nt_dot(masked, pool[i][0, :slots]) for i in places]
+            last = jnp.where(allowed, nt_dot(masked, k_new[:, cols]), NEG)
+            row_max = jnp.max(last, axis=-1, keepdims=True)
+            for s in scores:
+                row_max = jnp.maximum(row_max, jnp.max(s, axis=-1, keepdims=True))
+            weights = jnp.exp2((last - row_max) * scale)
+            total = jnp.sum(weights, axis=-1, keepdims=True)
+            mixed = nn_dot(weights.astype(BF16), v_new[:, cols])
+            for s, i in zip(scores, places):
+                weights = jnp.exp2((s - row_max) * scale)
+                total = total + jnp.sum(weights, axis=-1, keepdims=True)
+                mixed = mixed + nn_dot(weights.astype(BF16), pool[i][1, :slots])
+            mixed = mixed / total
+            out[:, combo * 128 : (combo + 1) * 128] = mixed.astype(BF16)
+            for base, stat in ((0, row_max), (4, total)):
+                for part in range(3):
+                    piece = stat.astype(BF16).astype(F32)
+                    stats = jnp.where(lane == 8 * part + base + combo, piece, stats)
+                    stat = stat - piece
+    out[:, 512:640] = stats.astype(BF16)
+
+
+def attend(ids, queries, pools0, pools1, slots, k_new, v_new):
     rows = queries.shape[0]
-    keys = count * slots + k_new.shape[0]
-    return pl.pallas_call(
-        lambda *refs: attend_body(count, slots, *refs),
+    keys = 4 * slots + k_new.shape[0]
+    return pl.pallas_call(
+        lambda *refs: attend_body(slots, *refs),
         out_shape=jax.ShapeDtypeStruct((rows, 640), BF16),
-        in_specs=[pl.BlockSpec(memory_space=pltpu.SMEM)] + vmem(count + 3),
+        in_specs=[pl.BlockSpec(memory_space=pltpu.SMEM)] + vmem(11),
         out_specs=vmem(1)[0],
-        compiler_params=pltpu.CompilerParams(vmem_limit_bytes=32 * MIB),
+        compiler_params=pltpu.CompilerParams(vmem_limit_bytes=ATT * MIB),
         cost_estimate=pl.CostEstimate(
             flops=4 * rows * keys * 512, bytes_accessed=2 * MIB, transcendentals=4 * rows * keys
         ),
         name="attend",
-    )(device, queries, *pools, k_new, v_new)
+    )(ids, queries, *pools0, *pools1, k_new, v_new)
 
 
 def combine_body(parts, dec_out, lambdas, head_gain, out):
@@ -384,12 +384,18 @@
     groups = [[SHARE * m + e for m in range(members)] for e in range(SHARE)]
     gain = norm_gain.reshape(1, -1)
     head_gain = head_gain.reshape(1, -1)
-    me = lax.axis_index("kv").reshape(1)
-
-    def swap(array, bit):
-        return lax.ppermute(array, "kv", [(i, i ^ bit) for i in range(kv_count)])
-
-    pool, sent, q_dec = opening(
+    me = lax.axis_index("kv")
+
+    def across(i):
+        chip = i // 2 % 4
+        return i + 2 * ((chip + 2 * (chip % 2) + 3) % 4 - chip)
+
+    ids = me.reshape(1)
+
+    def move(array, target):
+        return lax.ppermute(array, "kv", [(i, target(i)) for i in range(kv_count)])
+
+    pool0, pool1, sent, q_dec = opening(
         piece_keys.reshape(-1, 128),
         piece_values.reshape(-1, 128),
         x_piece,
@@ -398,14 +404,12 @@
         w_query,
         members,
     )
-    pools = [pool]
-    bit = SHARE // 2
-    while bit:
-        swapped = []
-        for pool in pools:
-            swapped += [pool, swap(pool, bit)]
-        pools = swapped
-        bit //= 2
+    far0 = move(pool0, lambda i: i ^ 2)
+    far1 = move(pool1, across)
+    pools0 = [pool0, move(pool0, lambda i: i ^ 1), far0]
+    pools1 = [pool1, move(pool1, lambda i: i ^ 1), far1]
+    pools0.append(move(far0, lambda i: i ^ 1))
+    pools1.append(move(far1, lambda i: i ^ 1))
     got = lax.all_to_all(sent, "kv", 0, 0, tiled=True, axis_index_groups=groups)
     dec_out = decode(
         x_decode,
@@ -419,9 +423,11 @@
         lambdas,
         head_gain,
     )
-    k_new, v_new = fresh(gain, w_key, w_value, pools, rows)
+    k_new, v_new = fresh(gain, w_key, w_value, pools0, pools1, rows)
     slots = piece_keys.shape[0]
-    parts = attend(me, got.reshape(members * rows, 256), pools, slots, k_new, v_new)
+    parts = attend(
+        ids, got.reshape(members * rows, 256), pools0, pools1, slots, k_new, v_new
+    )
     parts = lax.all_to_all(
         parts.reshape(members, rows, 640), "kv", 0, 0, tiled=True, axis_index_groups=groups
     )

time: 79.5 us -> 75.2 us (0.946)
  waiting for transfers between devices: 29.4 us -> 22.9 us
  local copies, waits for them, and re-layouts: 4.72 us -> 7.73 us
  Pallas kernels: 17.5 us -> 14.9 us
  starting transfers between devices: 16.2 us -> 18 us
    ppermute x3 -> x6, waiting for transfers between devices: 13.1 us -> 7.64 us  [move(): return lax.ppermute(array, 'kv', [(i, target(i)) for i in range(kv_count)])]
    unnamed x24 -> x32, local copies, waits for them, and re-layouts: 4.72 us -> 7.73 us
    ppermute x3 -> x6, starting transfers between devices: 2.25 us -> 4.07 us  [move(): return lax.ppermute(array, 'kv', [(i, target(i)) for i in range(kv_count)])]
    pallas_call x1, Pallas kernels: 4.65 us -> 2.99 us  [decode(): pl.pallas_call(decode_body, out_shape=jax.ShapeDtypeStruct((1, 256), BF16...]
    all_to_all x1, waiting for transfers between devices: 9.24 us -> 7.78 us  [layer(): lax.all_to_all(parts.reshape(members, rows, 640), 'kv', 0, 0, tiled=True,...]
    pallas_call x3, Pallas kernels: 11 us -> 10 us  [the longest x1 5.85 us: attend(): pl.pallas_call(lambda *refs: attend_body(slots, *refs), out_shape=jax.Sha...]
  transfers between devices with their start and end apart: 5 -> 8, of which waited for: 3 -> 4; matrix products, arithmetic and copies ran while one was open for 0% -> 0% of each run, Pallas kernels for 9% -> 6%
where the time goes in v3:
time: 75.2 us; the launch traced here: 74.6 us
  waiting for transfers between devices  22.9 us (30%)
  starting transfers between devices  18 us (24%)
  Pallas kernels  14.9 us (20%)
  blocking collectives  9.63 us (13%)
  local copies, waits for them, and re-layouts  7.73 us (10%)
  between operations  1.45 us (2%)
    all_to_all x1, starting transfers between devices, layer(): got = lax.all_to_all(sent, 'kv', 0, 0, tiled=True, axis_index_groups=groups)  10.3 us
    all_to_all x1, blocking collectives, layer(): heads = lax.all_to_all(heads, 'tp', 0, 0, tiled=True)  9.63 us
    all_to_all x1, waiting for transfers between devices, layer(): lax.all_to_all(parts.reshape(members, rows, 640), 'kv', 0, 0, tiled=True,...  7.78 us
    unnamed x32, local copies, waits for them, and re-layouts  7.73 us
    ppermute x6, waiting for transfers between devices, move(): return lax.ppermute(array, 'kv', [(i, target(i)) for i in range(kv_count)])  7.64 us
    all_to_all x1, waiting for transfers between devices, layer(): got = lax.all_to_all(sent, 'kv', 0, 0, tiled=True, axis_index_groups=groups)  7.49 us
    pallas_call x1, Pallas kernels, attend(): pl.pallas_call(lambda *refs: attend_body(slots, *refs), out_shape=jax.Sha...  5.85 us
    ppermute x6, starting transfers between devices, move(): return lax.ppermute(array, 'kv', [(i, target(i)) for i in range(kv_count)])  4.07 us
  transfers between devices with their start and end apart: 8, of which 4 were waited for; matrix products, arithmetic and copies ran while one was open for 0% of the time, Pallas kernels for 6%

profile of v3, /device:TPU:8, one launch (start us, length us, event | category | flops | bytes accessed | tf_op | source)
XLA Modules:
  0.0 74.6 jit_solution(13142196864863229939)
XLA Ops:
  0.6 0.0 copy-start.1
  0.6 0.0 copy-start.2
  0.7 2.6 %opening.1 = (bf16[2,640,128]{2,1,0:T(8,128)(2,1)}, bf16[2,640,128]{2,1,0:T(8,128)(2,1)}, bf16[16,16,256]{2,1,0:T(8,128)(2,1)}, bf16[1,256]{1,0:T(2,128)(2,1)}) custom-call(bf16[1024,128]{1,0:T(8,128)(2,1)} %bitcast.16, bf16[1024,128]{1,0:T(8,128)(2,1)} %bitcast.17, bf16[16,2048]{1,0:T(8,128)(2,1)} %x.1, bf16[1,2048]{1,0:T(2,128)(2,1)} %x_dec.3, ...), custom_call_target="tpu_custom_call" | custom-call | flops 1000000000 | bytes 2097152 | tf_op jit(solution)/shard_map/opening/pallas_call | solution.py:91
  3.2 1.7 %collective-permute-start.4 = (bf16[2,640,128]{2,1,0:T(8,128)(2,1)}, bf16[2,640,128]{2,1,0:T(8,128)(2,1)S(1)}, u32[]{:S(2)}, u32[]{:S(2)}) collective-permute-start(bf16[2,640,128]{2,1,0:T(8,128)(2,1)} %get-tuple-element.10.refs_6_), channel_id=1, source_target_pairs={{0,24},{4,28},{8,16},{12,20},{16,8},{20,12},{24,0},{28,4},{32,56},... | collective-permute-start | bytes 983048 | tf_op jit(solution)/shard_map/ppermute | solution.py:396
  4.9 1.9 %collective-permute-start.1 = (bf16[2,640,128]{2,1,0:T(8,128)(2,1)}, bf16[2,640,128]{2,1,0:T(8,128)(2,1)S(1)}, u32[]{:S(2)}, u32[]{:S(2)}) collective-permute-start(bf16[2,640,128]{2,1,0:T(8,128)(2,1)} %get-tuple-element.9.refs_3_.refs_2_), channel_id=1, source_target_pairs={{0,8},{4,12},{8,0},{12,4},{16,24},{20,28},{24,16},{28,20},{32,40},... | collective-permute-start | bytes 983048 | tf_op jit(solution)/shard_map/ppermute | solution.py:396
  6.8 0.0 collective-permute-start
  6.8 6.2 %collective-permute-done.4.refs_7_.refs_8_ = bf16[2,640,128]{2,1,0:T(8,128)(2,1)S(1)} collective-permute-done((bf16[2,640,128]{2,1,0:T(8,128)(2,1)}, bf16[2,640,128]{2,1,0:T(8,128)(2,1)S(1)}, u32[]{:S(2)}, u32[]{:S(2)}) %collective-permute-start.4) | collective-permute-done | bytes 327712 | tf_op jit(solution)/shard_map/ppermute | solution.py:396
  13.0 0.0 collective-permute-start.5
  13.0 1.4 %collective-permute-done.1.refs_5_.refs_4_ = bf16[2,640,128]{2,1,0:T(8,128)(2,1)S(1)} collective-permute-done((bf16[2,640,128]{2,1,0:T(8,128)(2,1)}, bf16[2,640,128]{2,1,0:T(8,128)(2,1)S(1)}, u32[]{:S(2)}, u32[]{:S(2)}) %collective-permute-start.1) | collective-permute-done | bytes 327712 | tf_op jit(solution)/shard_map/ppermute | solution.py:396
  14.4 0.0 collective-permute-start.2
  14.4 0.5 collective-permute-start.3
  14.9 0.0 copy-start.8
  14.9 10.3 %all-to-all-start = ((bf16[16,16,256]{2,1,0:T(8,128)(2,1)}), bf16[16,16,256]{2,1,0:T(8,128)(2,1)}, u32[]{:S(2)}, u32[]{:S(2)}) async-start(bf16[16,16,256]{2,1,0:T(8,128)(2,1)} %get-tuple-element.8), calls=%async_computation | async-start | bytes 262144 | tf_op jit(solution)/shard_map/all_to_all | solution.py:413
  25.2 0.0 collective-permute-done.refs_4_.refs_3_
  25.2 0.0 collective-permute-done.5.refs_8_.refs_9_
  25.2 0.0 copy-start.5
  25.3 0.7 copy-done.5
  26.0 0.0 collective-permute-done.2.refs_6_.refs_5_
  26.0 0.0 copy-done.1
  26.0 0.0 copy-done.2
  26.0 0.0 copy-done.8
  26.0 0.0 copy-start.3
  26.0 1.0 %copy-done.3 = bf16[2,640,128]{2,1,0:T(8,128)(2,1)S(1)} copy-done((bf16[2,640,128]{2,1,0:T(8,128)(2,1)S(1)}, bf16[2,640,128]{2,1,0:T(8,128)(2,1)}, u32[]{:S(2)}) %copy-start.3) | copy-done | bytes 327704
  27.0 0.0 copy-start.6
  27.0 1.0 %copy-done.6 = bf16[2,640,128]{2,1,0:T(8,128)(2,1)S(1)} copy-done((bf16[2,640,128]{2,1,0:T(8,128)(2,1)S(1)}, bf16[2,640,128]{2,1,0:T(8,128)(2,1)}, u32[]{:S(2)}) %copy-start.6) | copy-done | bytes 327704
  28.0 1.6 %fresh.1 = (bf16[64,256]{1,0:T(8,128)(2,1)S(1)}, bf16[64,256]{1,0:T(8,128)(2,1)S(1)}) custom-call(f32[1,2048]{1,0:T(1,128)S(1)} %bitcast.10, bf16[2048,256]{1,0:T(8,128)(2,1)S(1)} %copy-done.1, bf16[2048,256]{1,0:T(8,128)(2,1)S(1)} %copy-done.2, bf16[2,640,128]{2,1,0:T(8,128)(2,1)S(1)} %copy-done.3, ...), custom_call_target="tpu_custom_call" | custom-call | flops 1000000000 | bytes 2097152 | tf_op jit(solution)/shard_map/fresh/pallas_call | solution.py:214
  29.5 7.5 %all-to-all-done = bf16[16,16,256]{2,1,0:T(8,128)(2,1)} async-done(((bf16[16,16,256]{2,1,0:T(8,128)(2,1)}), bf16[16,16,256]{2,1,0:T(8,128)(2,1)}, u32[]{:S(2)}, u32[]{:S(2)}) %all-to-all-start) | async-done | bytes 131104 | tf_op jit(solution)/shard_map/all_to_all | solution.py:413
  37.0 0.0 collective-permute-done.3.refs_7_
  37.0 0.0 copy-done.4
  37.0 1.0 %copy-done.7 = bf16[2,640,128]{2,1,0:T(8,128)(2,1)S(1)} copy-done((bf16[2,640,128]{2,1,0:T(8,128)(2,1)S(1)}, bf16[2,640,128]{2,1,0:T(8,128)(2,1)}, u32[]{:S(2)}) %copy-start.7) | copy-done | bytes 327704
  38.0 1.0 %copy-done.13 = bf16[2,640,128]{2,1,0:T(8,128)(2,1)S(1)} copy-done((bf16[2,640,128]{2,1,0:T(8,128)(2,1)S(1)}, bf16[2,640,128]{2,1,0:T(8,128)(2,1)}, u32[]{:S(2)}) %copy-start.13) | copy-done | bytes 327704
  39.0 5.9 %attend.1 = bf16[256,640]{1,0:T(8,128)(2,1)} custom-call(s32[1]{0:T(128)} %bitcast.refs_0_, bf16[256,256]{1,0:T(8,128)(2,1)} %bitcast.4.refs_1_, bf16[2,640,128]{2,1,0:T(8,128)(2,1)S(1)} %copy-done.4, bf16[2,640,128]{2,1,0:T(8,128)(2,1)S(1)} %collective-permute-done.refs_4_.refs_3_, bf16[2,640,128]{2,1,0:T(8,128)(2,1)S(1)} %collective-permute-done.1.refs_5_.refs_4_, ...), custom_call_target="tpu_custom_call" | custom-call | flops 1107296256 | bytes 2097152 | tf_op jit(solution)/shard_map/attend/pallas_call | solution.py:280
  44.8 3.7 %all-to-all-start.1 = ((bf16[16,16,640]{2,1,0:T(8,128)(2,1)}), bf16[16,16,640]{2,1,0:T(8,128)(2,1)S(1)}, u32[]{:S(2)}, u32[]{:S(2)}) async-start(bf16[16,16,640]{2,1,0:T(8,128)(2,1)} %bitcast.5), calls=%async_computation.1 | async-start | bytes 655360 | tf_op jit(solution)/shard_map/all_to_all | solution.py:431
  48.5 0.0 copy-start.14
  49.2 0.0 copy-start.9
  49.2 0.0 copy-start.10
  49.2 0.0 copy-done.15
  49.2 0.0 copy-done.14
  49.2 0.6 copy-done.9
  49.8 0.0 copy-done.10
  49.8 1.2 %copy-done.11 = bf16[1,2048,2,128]{3,2,1,0:T(2,128)(2,1)S(1)} copy-done((bf16[1,2048,2,128]{3,2,1,0:T(2,128)(2,1)S(1)}, bf16[1,2048,2,128]{3,2,1,0:T(2,128)(2,1)}, u32[]{:S(2)}) %copy-start.11) | copy-done | bytes 1048600
  51.1 1.2 %copy-done.12 = bf16[1,2048,2,128]{3,2,1,0:T(2,128)(2,1)S(1)} copy-done((bf16[1,2048,2,128]{3,2,1,0:T(2,128)(2,1)S(1)}, bf16[1,2048,2,128]{3,2,1,0:T(2,128)(2,1)}, u32[]{:S(2)}) %copy-start.12) | copy-done | bytes 1048600
  52.3 3.0 %decode.1.dec_out = bf16[1,256]{1,0:T(2,128)(2,1)S(1)} custom-call(bf16[1,2048]{1,0:T(2,128)(2,1)S(1)} %copy-done.14, f32[1,2048]{1,0:T(1,128)S(1)} %bitcast.11, bf16[2048,256]{1,0:T(8,128)(2,1)S(1)} %copy-done.1, bf16[2048,256]{1,0:T(8,128)(2,1)S(1)} %copy-done.2, bf16[1,256]{1,0:T(2,128)(2,1)S(1)} %copy-done.15, bf16[4096,128]{1,0:T(8,128)(2,1)S(1)} %bitcast.14, ...), custom_call_target="tpu_custom_call" | custom-call | flops 2000000000 | bytes 4194304 | tf_op jit(solution)/shard_map/decode/pallas_call | solution.py:170
  55.3 7.8 %all-to-all-done.1.parts = bf16[16,16,640]{2,1,0:T(8,128)(2,1)S(1)} async-done(((bf16[16,16,640]{2,1,0:T(8,128)(2,1)}), bf16[16,16,640]{2,1,0:T(8,128)(2,1)S(1)}, u32[]{:S(2)}, u32[]{:S(2)}) %all-to-all-start.1) | async-done | bytes 327712 | tf_op jit(solution)/shard_map/all_to_all | solution.py:431
  63.1 1.0 %combine.1 = bf16[4,24,256]{2,1,0:T(8,128)(2,1)S(1)} custom-call(bf16[16,16,640]{2,1,0:T(8,128)(2,1)S(1)} %all-to-all-done.1.parts, bf16[1,256]{1,0:T(2,128)(2,1)S(1)} %decode.1.dec_out, f32[2]{0:T(128)S(1)} %copy-done.9, f32[1,128]{1,0:T(1,128)S(1)} %bitcast.13), custom_call_target="tpu_custom_call" | custom-call | flops 100000000 | bytes 1048576 | tf_op jit(solution)/shard_map/combine/pallas_call | solution.py:329
  64.1 9.6 %all_to_all.15.heads = bf16[4,24,256]{2,1,0:T(8,128)(2,1)S(1)} all-to-all(bf16[4,24,256]{2,1,0:T(8,128)(2,1)S(1)} %combine.1), channel_id=1, replica_groups=mesh['kv'=64,'tp'=4] {'tp'}, dimensions={0} | all-to-all | bytes 98304 | tf_op jit(solution)/shard_map/all_to_all | solution.py:435
  73.7 0.0 copy-done
  73.7 0.9 %out_rows.1 = (bf16[16,512]{1,0:T(8,128)(2,1)}, bf16[1,512]{1,0:T(2,128)(2,1)}) custom-call(bf16[4,24,256]{2,1,0:T(8,128)(2,1)S(1)} %all_to_all.15.heads, bf16[1024,512]{1,0:T(8,128)(2,1)S(1)} %copy-done), custom_call_target="tpu_custom_call" | custom-call | flops 100000000 | bytes 1048576 | tf_op jit(solution)/shard_map/out_rows/pallas_call | solution.py:350
  (7 shorter events, 0.0 us)
Async XLA Ops:
  0.6 25.4 %copy-start.1 = (bf16[2048,256]{1,0:T(8,128)(2,1)S(1)}, bf16[2048,256]{1,0:T(8,128)(2,1)}, u32[]{:S(2)}) copy-start(bf16[2048,256]{1,0:T(8,128)(2,1)} %w_key.1) | copy-start | bytes 3145732
  0.6 25.3 %copy-start.2 = (bf16[2048,256]{1,0:T(8,128)(2,1)S(1)}, bf16[2048,256]{1,0:T(8,128)(2,1)}, u32[]{:S(2)}) copy-start(bf16[2048,256]{1,0:T(8,128)(2,1)} %w_value.1) | copy-start | bytes 3145732
  3.2 9.7 %collective-permute-start.4 = (bf16[2,640,128]{2,1,0:T(8,128)(2,1)}, bf16[2,640,128]{2,1,0:T(8,128)(2,1)S(1)}, u32[]{:S(2)}, u32[]{:S(2)}) collective-permute-start(bf16[2,640,128]{2,1,0:T(8,128)(2,1)} %get-tuple-element.10.refs_6_), channel_id=1, source_target_pairs={{0,24},{4,28},{8,16},{12,20},{16,8},{20,12},{24,0},{28,4},{32,56},... | collective-permute-start | bytes 983048 | tf_op jit(solution)/shard_map/ppermute | solution.py:396
  4.9 9.5 %collective-permute-start.1 = (bf16[2,640,128]{2,1,0:T(8,128)(2,1)}, bf16[2,640,128]{2,1,0:T(8,128)(2,1)S(1)}, u32[]{:S(2)}, u32[]{:S(2)}) collective-permute-start(bf16[2,640,128]{2,1,0:T(8,128)(2,1)} %get-tuple-element.9.refs_3_.refs_2_), channel_id=1, source_target_pairs={{0,8},{4,12},{8,0},{12,4},{16,24},{20,28},{24,16},{28,20},{32,40},... | collective-permute-start | bytes 983048 | tf_op jit(solution)/shard_map/ppermute | solution.py:396
  6.8 18.4 %collective-permute-start = (bf16[2,640,128]{2,1,0:T(8,128)(2,1)}, bf16[2,640,128]{2,1,0:T(8,128)(2,1)S(1)}, u32[]{:S(2)}, u32[]{:S(2)}) collective-permute-start(bf16[2,640,128]{2,1,0:T(8,128)(2,1)} %get-tuple-element.9.refs_3_.refs_2_), channel_id=1, source_target_pairs={{0,4},{4,0},{8,12},{12,8},{16,20},{20,16},{24,28},{28,24},{32,36},... | collective-permute-start | bytes 983048 | tf_op jit(solution)/shard_map/ppermute | solution.py:396
  13.0 12.2 %collective-permute-start.5 = (bf16[2,640,128]{2,1,0:T(8,128)(2,1)S(1)}, bf16[2,640,128]{2,1,0:T(8,128)(2,1)S(1)}, u32[]{:S(2)}, u32[]{:S(2)}) collective-permute-start(bf16[2,640,128]{2,1,0:T(8,128)(2,1)S(1)} %collective-permute-done.4.refs_7_.refs_8_), channel_id=1, source_target_pairs={{0,4},{4,0},{8,12},{12,8},{16,20},{20,16},{24,28},{28,24},{32,36},... | collective-permute-start | bytes 983048 | tf_op jit(solution)/shard_map/ppermute | solution.py:396
  14.4 11.5 %collective-permute-start.2 = (bf16[2,640,128]{2,1,0:T(8,128)(2,1)S(1)}, bf16[2,640,128]{2,1,0:T(8,128)(2,1)}, u32[]{:S(2)}, u32[]{:S(2)}) collective-permute-start(bf16[2,640,128]{2,1,0:T(8,128)(2,1)S(1)} %collective-permute-done.1.refs_5_.refs_4_), channel_id=1, source_target_pairs={{0,4},{4,0},{8,12},{12,8},{16,20},{20,16},{24,28},{28,24},{32,36},... | collective-permute-start | bytes 983048 | tf_op jit(solution)/shard_map/ppermute | solution.py:396
  14.4 22.6 %collective-permute-start.3 = (bf16[2,640,128]{2,1,0:T(8,128)(2,1)}, bf16[2,640,128]{2,1,0:T(8,128)(2,1)}, u32[]{:S(2)}, u32[]{:S(2)}) collective-permute-start(bf16[2,640,128]{2,1,0:T(8,128)(2,1)} %get-tuple-element.10.refs_6_), channel_id=1, source_target_pairs={{0,4},{4,0},{8,12},{12,8},{16,20},{20,16},{24,28},{28,24},{32,36},... | collective-permute-start | bytes 983048 | tf_op jit(solution)/shard_map/ppermute | solution.py:396
  14.9 11.0 %copy-start.8 = (f32[2048]{0:T(1024)S(1)}, f32[2048]{0:T(1024)}, u32[]{:S(2)}) copy-start(f32[2048]{0:T(1024)} %param.16) | copy-start | bytes 24580
  14.9 22.1 %all-to-all-start = ((bf16[16,16,256]{2,1,0:T(8,128)(2,1)}), bf16[16,16,256]{2,1,0:T(8,128)(2,1)}, u32[]{:S(2)}, u32[]{:S(2)}) async-start(bf16[16,16,256]{2,1,0:T(8,128)(2,1)} %get-tuple-element.8), calls=%async_computation | async-start | bytes 262144 | tf_op jit(solution)/shard_map/all_to_all | solution.py:413
  25.2 0.7 copy-start.5
  26.0 1.0 %copy-start.3 = (bf16[2,640,128]{2,1,0:T(8,128)(2,1)S(1)}, bf16[2,640,128]{2,1,0:T(8,128)(2,1)}, u32[]{:S(2)}) copy-start(bf16[2,640,128]{2,1,0:T(8,128)(2,1)} %get-tuple-element.9.refs_3_.refs_2_) | copy-start | bytes 983044
  27.0 1.0 %copy-start.6 = (bf16[2,640,128]{2,1,0:T(8,128)(2,1)S(1)}, bf16[2,640,128]{2,1,0:T(8,128)(2,1)}, u32[]{:S(2)}) copy-start(bf16[2,640,128]{2,1,0:T(8,128)(2,1)} %copy-done.5) | copy-start | bytes 983044
  28.0 9.1 %copy-start.4 = (bf16[2,640,128]{2,1,0:T(8,128)(2,1)S(1)}, bf16[2,640,128]{2,1,0:T(8,128)(2,1)}, u32[]{:S(2)}) copy-start(bf16[2,640,128]{2,1,0:T(8,128)(2,1)} %get-tuple-element.9.refs_3_.refs_2_) | copy-start | bytes 983044
  37.0 1.0 %copy-start.7 = (bf16[2,640,128]{2,1,0:T(8,128)(2,1)S(1)}, bf16[2,640,128]{2,1,0:T(8,128)(2,1)}, u32[]{:S(2)}) copy-start(bf16[2,640,128]{2,1,0:T(8,128)(2,1)} %copy-done.5) | copy-start | bytes 983044
  38.0 1.0 %copy-start.13 = (bf16[2,640,128]{2,1,0:T(8,128)(2,1)S(1)}, bf16[2,640,128]{2,1,0:T(8,128)(2,1)}, u32[]{:S(2)}) copy-start(bf16[2,640,128]{2,1,0:T(8,128)(2,1)} %get-tuple-element.10.refs_6_) | copy-start | bytes 983044
  44.8 4.4 %copy-start.15 = (bf16[1,256]{1,0:T(2,128)(2,1)S(1)}, bf16[1,256]{1,0:T(2,128)(2,1)}, u32[]{:S(2)}) copy-start(bf16[1,256]{1,0:T(2,128)(2,1)} %get-tuple-element.13.q_dec) | copy-start | bytes 1540
  44.8 18.3 %all-to-all-start.1 = ((bf16[16,16,640]{2,1,0:T(8,128)(2,1)}), bf16[16,16,640]{2,1,0:T(8,128)(2,1)S(1)}, u32[]{:S(2)}, u32[]{:S(2)}) async-start(bf16[16,16,640]{2,1,0:T(8,128)(2,1)} %bitcast.5), calls=%async_computation.1 | async-start | bytes 655360 | tf_op jit(solution)/shard_map/all_to_all | solution.py:431
  48.5 0.7 copy-start.14
  49.2 0.7 copy-start.9
  49.2 0.7 copy-start.10
  49.8 1.2 %copy-start.11 = (bf16[1,2048,2,128]{3,2,1,0:T(2,128)(2,1)S(1)}, bf16[1,2048,2,128]{3,2,1,0:T(2,128)(2,1)}, u32[]{:S(2)}) copy-start(bf16[1,2048,2,128]{3,2,1,0:T(2,128)(2,1)} %param.25) | copy-start | bytes 3145732
  51.1 1.2 %copy-start.12 = (bf16[1,2048,2,128]{3,2,1,0:T(2,128)(2,1)S(1)}, bf16[1,2048,2,128]{3,2,1,0:T(2,128)(2,1)}, u32[]{:S(2)}) copy-start(bf16[1,2048,2,128]{3,2,1,0:T(2,128)(2,1)} %param.26) | copy-start | bytes 3145732
  52.3 21.4 %copy-start = (bf16[1024,512]{1,0:T(8,128)(2,1)S(1)}, bf16[1024,512]{1,0:T(8,128)(2,1)}, u32[]{:S(2)}) copy-start(bf16[1024,512]{1,0:T(8,128)(2,1)} %w.3) | copy-start | bytes 3145732

commit v4 on v3

--- a/solution.py
+++ b/solution.py
@@ -91,9 +91,9 @@
     return pl.pallas_call(
         opening_body,
         out_shape=(
-            jax.ShapeDtypeStruct((2, slots + rows * width // 256, 128), BF16),
-            jax.ShapeDtypeStruct((2, slots + rows * width // 256, 128), BF16),
-            jax.ShapeDtypeStruct((members, rows, w.shape[1]), BF16),
+            pltpu.VMEM((2, slots + rows * width // 256, 128), BF16),
+            pltpu.VMEM((2, slots + rows * width // 256, 128), BF16),
+            pltpu.VMEM((members, rows, w.shape[1]), BF16),
             jax.ShapeDtypeStruct((1, w.shape[1]), BF16),
         ),
         in_specs=[HBM] * 6,
@@ -265,21 +265,26 @@
                 total = total + jnp.sum(weights, axis=-1, keepdims=True)
                 mixed = mixed + nn_dot(weights.astype(BF16), pool[i][1, :slots])
             mixed = mixed / total
-            out[:, combo * 128 : (combo + 1) * 128] = mixed.astype(BF16)
+            out[:, combo * each : (combo + 1) * each, :] = mixed.astype(BF16).reshape(
+                rows // each, each, 128
+            )
             for base, stat in ((0, row_max), (4, total)):
                 for part in range(3):
                     piece = stat.astype(BF16).astype(F32)
-                    stats = jnp.where(lane == 8 * part + base + combo, piece, stats)
+                    stats = jnp.where(lane % 64 == 8 * part + base + combo, piece, stats)
                     stat = stat - piece
-    out[:, 512:640] = stats.astype(BF16)
+    stats = stats.reshape(rows // each, 2, each // 2, 128)
+    low = lane_iota((rows // each, each // 2, 128)) < 64
+    out[:, 4 * each :, :] = jnp.where(low, stats[:, 0], stats[:, 1]).astype(BF16)
 
 
 def attend(ids, queries, pools0, pools1, slots, k_new, v_new):
     rows = queries.shape[0]
     keys = 4 * slots + k_new.shape[0]
+    each = k_new.shape[0] // 4
     return pl.pallas_call(
         lambda *refs: attend_body(slots, *refs),
-        out_shape=jax.ShapeDtypeStruct((rows, 640), BF16),
+        out_shape=pltpu.HBM((rows // each, 4 * each + each // 2, 128), BF16),
         in_specs=[pl.BlockSpec(memory_space=pltpu.SMEM)] + vmem(11),
         out_specs=vmem(1)[0],
         compiler_params=pltpu.CompilerParams(vmem_limit_bytes=ATT * MIB),
@@ -293,10 +298,11 @@
 def combine_body(parts, dec_out, lambdas, head_gain, out):
     scale = 0.125 * math.log2(math.e)
     members = parts.shape[0]
-    rows = parts.shape[1]
+    rows = parts.shape[1] * 2 // 9
 
     def whole(member):
-        pieces = parts[member, :, 512:640].astype(F32)
+        pieces = parts[member, 4 * rows :, :].astype(F32)
+        pieces = jnp.concatenate([pieces, pltpu.roll(pieces, 64, 1)], axis=0)
         return pieces + pltpu.roll(pieces, 120, 1) + pltpu.roll(pieces, 112, 1)
 
     stats = [whole(member) for member in range(members)]
@@ -312,7 +318,7 @@
         acc = jnp.zeros((rows, 128), F32)
         for member in range(members):
             acc = acc + shares[member][:, combo : combo + 1] * parts[
-                member, :, combo * 128 : (combo + 1) * 128
+                member, combo * rows : (combo + 1) * rows, :
             ].astype(F32)
         sums.append(acc / total[:, combo : combo + 1])
     heads = []
@@ -326,9 +332,10 @@
 
 
 def combine(parts, dec_out, lambdas, head_gain, copies):
+    rows = parts.shape[1] * 2 // 9
     return pl.pallas_call(
         combine_body,
-        out_shape=jax.ShapeDtypeStruct((copies, parts.shape[1] + 8, 256), BF16),
+        out_shape=jax.ShapeDtypeStruct((copies, rows + 8, 256), BF16),
         in_specs=vmem(2) + [pl.BlockSpec(memory_space=pltpu.SMEM)] + vmem(1),
         out_specs=vmem(1)[0],
         compiler_params=pltpu.CompilerParams(vmem_limit_bytes=16 * MIB),
@@ -337,28 +344,48 @@
     )(parts, dec_out, lambdas, head_gain)
 
 
-def out_body(heads, w, piece, dec):
+def own_body(place, heads, w, out):
+    start = pl.multiple_of(place[0] * 256, 256)
+    out[...] = nn_dot(heads[0], w[pl.ds(start, 256), :])
+
+
+def own_rows(place, heads, w):
+    return pl.pallas_call(
+        own_body,
+        out_shape=jax.ShapeDtypeStruct((heads.shape[1], w.shape[1]), F32),
+        in_specs=[pl.BlockSpec(memory_space=pltpu.SMEM)] + vmem(2),
+        out_specs=vmem(1)[0],
+        compiler_params=pltpu.CompilerParams(vmem_limit_bytes=8 * MIB),
+        cost_estimate=pl.CostEstimate(flops=10**9, bytes_accessed=MIB, transcendentals=0),
+        name="own_rows",
+    )(place, heads, w)
+
+
+def out_body(place, own, heads, w, piece, dec):
     rows = piece.shape[0]
-    acc = nn_dot(heads[0], w[:256])
-    for copy in range(1, heads.shape[0]):
-        acc = acc + nn_dot(heads[copy], w[copy * 256 : (copy + 1) * 256])
+    count = heads.shape[0]
+    acc = own[...]
+    for step in range(1, count):
+        other = lax.rem(place[0] + step, count)
+        start = pl.multiple_of(other * 256, 256)
+        acc = acc + nn_dot(heads[other], w[pl.ds(start, 256), :])
     piece[...] = acc[:rows].astype(BF16)
     dec[...] = acc[rows : rows + 1].astype(BF16)
 
 
-def out_rows(heads, w, rows):
+def out_rows(place, own, heads, w, rows):
     return pl.pallas_call(
         out_body,
         out_shape=(
             jax.ShapeDtypeStruct((rows, w.shape[1]), BF16),
             jax.ShapeDtypeStruct((1, w.shape[1]), BF16),
         ),
-        in_specs=vmem(2),
+        in_specs=[pl.BlockSpec(memory_space=pltpu.SMEM)] + vmem(3),
         out_specs=tuple(vmem(2)),
         compiler_params=pltpu.CompilerParams(vmem_limit_bytes=8 * MIB),
         cost_estimate=pl.CostEstimate(flops=10**8, bytes_accessed=MIB, transcendentals=0),
         name="out_rows",
-    )(heads, w)
+    )(place, own, heads, w)
 
 
 def layer(
@@ -429,11 +456,13 @@
         ids, got.reshape(members * rows, 256), pools0, pools1, slots, k_new, v_new
     )
     parts = lax.all_to_all(
-        parts.reshape(members, rows, 640), "kv", 0, 0, tiled=True, axis_index_groups=groups
+        parts, "kv", 0, 0, tiled=True, axis_index_groups=groups
     )
     heads = combine(parts, dec_out, lambdas, head_gain, tp_count)
+    place = lax.axis_index("tp").reshape(1)
+    own = own_rows(place, heads, w_out)
     heads = lax.all_to_all(heads, "tp", 0, 0, tiled=True)
-    return out_rows(heads, w_out, rows)
+    return out_rows(place, own, heads, w_out, rows)
 
 
 def solution(mesh):

time: 75.2 us -> 73.6 us (0.979)
  blocking collectives: 9.63 us -> 0 us
  waiting for transfers between devices: 22.9 us -> 29 us
  local copies, waits for them, and re-layouts: 7.73 us -> 3.11 us
  starting transfers between devices: 18 us -> 22.5 us
  Pallas kernels: 14.9 us -> 16.9 us
    all_to_all x1 -> x0, blocking collectives: 9.63 us -> none  [layer(): heads = lax.all_to_all(heads, 'tp', 0, 0, tiled=True)]
    unnamed x32 -> x20, local copies, waits for them, and re-layouts: 7.73 us -> 3.11 us
    all_to_all x1 -> x2, starting transfers between devices: 3.67 us -> 7.96 us  [the longest x1 4.3 us: layer(): heads = lax.all_to_all(heads, 'tp', 0, 0, tiled=True)]
    all_to_all x1 -> x2, waiting for transfers between devices: 7.78 us -> 11.7 us  [the longest x1 7.1 us: layer(): lax.all_to_all(parts, 'kv', 0, 0, tiled=True, axis_index_groups=groups)]
    all_to_all x1, waiting for transfers between devices: 7.49 us -> 9.94 us  [layer(): got = lax.all_to_all(sent, 'kv', 0, 0, tiled=True, axis_index_groups=groups)]
    pallas_call x3 -> x4, Pallas kernels: 9.42 us -> 11.3 us  [the longest x1 6.08 us: attend(): pl.pallas_call(lambda *refs: attend_body(slots, *refs), out_shape=pltpu.H...]
  transfers between devices with their start and end apart: 8 -> 9, of which waited for: 4 -> 5; matrix products, arithmetic and copies ran while one was open for 0% -> 0% of each run, Pallas kernels for 6% -> 8%
where the time goes in v4:
time: 73.6 us; the launch traced here: 72.9 us
  waiting for transfers between devices  29 us (39%)
  starting transfers between devices  22.5 us (31%)
  Pallas kernels  16.9 us (23%)
  local copies, waits for them, and re-layouts  3.11 us (4%)
  between operations  1.45 us (2%)
    all_to_all x1, starting transfers between devices, layer(): got = lax.all_to_all(sent, 'kv', 0, 0, tiled=True, axis_index_groups=groups)  10.4 us
    all_to_all x1, waiting for transfers between devices, layer(): got = lax.all_to_all(sent, 'kv', 0, 0, tiled=True, axis_index_groups=groups)  9.94 us
    ppermute x6, waiting for transfers between devices, move(): return lax.ppermute(array, 'kv', [(i, target(i)) for i in range(kv_count)])  7.43 us
    all_to_all x1, waiting for transfers between devices, layer(): lax.all_to_all(parts, 'kv', 0, 0, tiled=True, axis_index_groups=groups)  7.1 us
    pallas_call x1, Pallas kernels, attend(): pl.pallas_call(lambda *refs: attend_body(slots, *refs), out_shape=pltpu.H...  6.08 us
    all_to_all x1, waiting for transfers between devices, layer(): heads = lax.all_to_all(heads, 'tp', 0, 0, tiled=True)  4.57 us
    all_to_all x1, starting transfers between devices, layer(): heads = lax.all_to_all(heads, 'tp', 0, 0, tiled=True)  4.3 us
    ppermute x6, starting transfers between devices, move(): return lax.ppermute(array, 'kv', [(i, target(i)) for i in range(kv_count)])  4.07 us
  transfers between devices with their start and end apart: 9, of which 5 were waited for; matrix products, arithmetic and copies ran while one was open for 0% of the time, Pallas kernels for 8%

profile of v4, /device:TPU:8, one launch (start us, length us, event | category | flops | bytes accessed | tf_op | source)
XLA Modules:
  0.0 72.9 jit_solution(6115190270879073308)
XLA Ops:
  0.6 0.0 copy-start.1
  0.6 0.0 copy-start.2
  0.7 2.6 %opening.1 = (bf16[2,640,128]{2,1,0:T(8,128)(2,1)S(1)}, bf16[2,640,128]{2,1,0:T(8,128)(2,1)}, bf16[16,16,256]{2,1,0:T(8,128)(2,1)}, bf16[1,256]{1,0:T(2,128)(2,1)}) custom-call(bf16[1024,128]{1,0:T(8,128)(2,1)} %bitcast.17, bf16[1024,128]{1,0:T(8,128)(2,1)} %bitcast.18, bf16[16,2048]{1,0:T(8,128)(2,1)} %x.1, bf16[1,2048]{1,0:T(2,128)(2,1)} %x_dec.3, ...), custom_call_target="tpu_custom_call" | custom-call | flops 1000000000 | bytes 2097152 | tf_op jit(solution)/shard_map/opening/pallas_call | solution.py:91
  3.2 1.7 %collective-permute-start.4 = (bf16[2,640,128]{2,1,0:T(8,128)(2,1)}, bf16[2,640,128]{2,1,0:T(8,128)(2,1)S(1)}, u32[]{:S(2)}, u32[]{:S(2)}) collective-permute-start(bf16[2,640,128]{2,1,0:T(8,128)(2,1)} %get-tuple-element.10.refs_6_), channel_id=1, source_target_pairs={{0,24},{4,28},{8,16},{12,20},{16,8},{20,12},{24,0},{28,4},{32,56},... | collective-permute-start | bytes 983048 | tf_op jit(solution)/shard_map/ppermute | solution.py:423
  4.9 1.9 %collective-permute-start.1 = (bf16[2,640,128]{2,1,0:T(8,128)(2,1)S(1)}, bf16[2,640,128]{2,1,0:T(8,128)(2,1)S(1)}, u32[]{:S(2)}, u32[]{:S(2)}) collective-permute-start(bf16[2,640,128]{2,1,0:T(8,128)(2,1)S(1)} %get-tuple-element.9.refs_3_.refs_2_), channel_id=1, source_target_pairs={{0,8},{4,12},{8,0},{12,4},{16,24},{20,28},{24,16},{28,20},{32,40},... | collective-permute-start | bytes 983048 | tf_op jit(solution)/shard_map/ppermute | solution.py:423
  6.8 0.0 collective-permute-start
  6.8 6.2 %collective-permute-done.4.refs_7_.refs_8_ = bf16[2,640,128]{2,1,0:T(8,128)(2,1)S(1)} collective-permute-done((bf16[2,640,128]{2,1,0:T(8,128)(2,1)}, bf16[2,640,128]{2,1,0:T(8,128)(2,1)S(1)}, u32[]{:S(2)}, u32[]{:S(2)}) %collective-permute-start.4) | collective-permute-done | bytes 327712 | tf_op jit(solution)/shard_map/ppermute | solution.py:423
  13.0 0.0 collective-permute-start.5
  13.0 1.2 %collective-permute-done.1.refs_5_.refs_4_ = bf16[2,640,128]{2,1,0:T(8,128)(2,1)S(1)} collective-permute-done((bf16[2,640,128]{2,1,0:T(8,128)(2,1)S(1)}, bf16[2,640,128]{2,1,0:T(8,128)(2,1)S(1)}, u32[]{:S(2)}, u32[]{:S(2)}) %collective-permute-start.1) | collective-permute-done | bytes 327712 | tf_op jit(solution)/shard_map/ppermute | solution.py:423
  14.2 0.0 collective-permute-start.2
  14.2 0.5 collective-permute-start.3
  14.7 0.0 copy-start.3
  14.7 10.4 %all-to-all-start = ((bf16[16,16,256]{2,1,0:T(8,128)(2,1)}), bf16[16,16,256]{2,1,0:T(8,128)(2,1)S(1)}, u32[]{:S(2)}, u32[]{:S(2)}) async-start(bf16[16,16,256]{2,1,0:T(8,128)(2,1)} %get-tuple-element.8), calls=%async_computation | async-start | bytes 262144 | tf_op jit(solution)/shard_map/all_to_all | solution.py:440
  25.2 0.0 collective-permute-done.refs_4_.refs_3_
  25.2 0.0 collective-permute-done.5.refs_8_.refs_9_
  25.2 0.0 collective-permute-done.2.refs_6_.refs_5_
  25.2 0.0 copy-done.1
  25.2 0.0 copy-done.2
  25.2 0.0 copy-done.3
  25.2 1.7 %fresh.1 = (bf16[64,256]{1,0:T(8,128)(2,1)S(1)}, bf16[64,256]{1,0:T(8,128)(2,1)S(1)}) custom-call(f32[1,2048]{1,0:T(1,128)S(1)} %bitcast.11, bf16[2048,256]{1,0:T(8,128)(2,1)S(1)} %copy-done.1, bf16[2048,256]{1,0:T(8,128)(2,1)S(1)} %copy-done.2, bf16[2,640,128]{2,1,0:T(8,128)(2,1)S(1)} %get-tuple-element.9.refs_3_.refs_2_, ...), custom_call_target="tpu_custom_call" | custom-call | flops 1000000000 | bytes 2097152 | tf_op jit(solution)/shard_map/fresh/pallas_call | solution.py:214
  27.0 9.9 %all-to-all-done = bf16[16,16,256]{2,1,0:T(8,128)(2,1)S(1)} async-done(((bf16[16,16,256]{2,1,0:T(8,128)(2,1)}), bf16[16,16,256]{2,1,0:T(8,128)(2,1)S(1)}, u32[]{:S(2)}, u32[]{:S(2)}) %all-to-all-start) | async-done | bytes 131104 | tf_op jit(solution)/shard_map/all_to_all | solution.py:440
  36.9 0.0 collective-permute-done.3.refs_7_
  36.9 6.1 %attend.1 = bf16[16,72,128]{2,1,0:T(8,128)(2,1)} custom-call(s32[1]{0:T(128)} %bitcast.1.refs_0_, bf16[256,256]{1,0:T(8,128)(2,1)S(1)} %bitcast.9, bf16[2,640,128]{2,1,0:T(8,128)(2,1)S(1)} %get-tuple-element.9.refs_3_.refs_2_, bf16[2,640,128]{2,1,0:T(8,128)(2,1)} %collective-permute-done.refs_4_.refs_3_, ...), custom_call_target="tpu_custom_call" | custom-call | flops 1107296256 | bytes 2097152 | tf_op jit(solution)/shard_map/attend/pallas_call | solution.py:285
  43.0 0.0 copy-start.9
  43.0 3.7 %all-to-all-start.1 = ((bf16[16,72,128]{2,1,0:T(8,128)(2,1)}), bf16[16,72,128]{2,1,0:T(8,128)(2,1)S(1)}, u32[]{:S(2)}, u32[]{:S(2)}) async-start(bf16[16,72,128]{2,1,0:T(8,128)(2,1)} %attend.1), calls=%async_computation.1 | async-start | bytes 589824 | tf_op jit(solution)/shard_map/all_to_all | solution.py:458
  46.7 0.0 copy-start.6
  47.3 0.0 copy-start.7
  47.3 0.0 copy-start.8
  47.4 0.0 copy-done.9
  47.4 0.0 copy-done.6
  47.4 0.6 copy-done.7
  48.0 0.0 copy-done.8
  48.0 0.0 copy-start.4
  48.0 1.2 %copy-done.4 = bf16[1,2048,2,128]{3,2,1,0:T(2,128)(2,1)S(1)} copy-done((bf16[1,2048,2,128]{3,2,1,0:T(2,128)(2,1)S(1)}, bf16[1,2048,2,128]{3,2,1,0:T(2,128)(2,1)}, u32[]{:S(2)}) %copy-start.4) | copy-done | bytes 1048600
  49.2 0.0 copy-start.5
  49.2 1.2 %copy-done.5 = bf16[1,2048,2,128]{3,2,1,0:T(2,128)(2,1)S(1)} copy-done((bf16[1,2048,2,128]{3,2,1,0:T(2,128)(2,1)S(1)}, bf16[1,2048,2,128]{3,2,1,0:T(2,128)(2,1)}, u32[]{:S(2)}) %copy-start.5) | copy-done | bytes 1048600
  50.5 0.0 copy-start
  50.5 3.0 %decode.1.dec_out = bf16[1,256]{1,0:T(2,128)(2,1)S(1)} custom-call(bf16[1,2048]{1,0:T(2,128)(2,1)S(1)} %copy-done.6, f32[1,2048]{1,0:T(1,128)S(1)} %bitcast.12, bf16[2048,256]{1,0:T(8,128)(2,1)S(1)} %copy-done.1, bf16[2048,256]{1,0:T(8,128)(2,1)S(1)} %copy-done.2, bf16[1,256]{1,0:T(2,128)(2,1)S(1)} %copy-done.9, bf16[4096,128]{1,0:T(8,128)(2,1)S(1)} %bitcast.13, ...), custom_call_target="tpu_custom_call" | custom-call | flops 2000000000 | bytes 4194304 | tf_op jit(solution)/shard_map/decode/pallas_call | solution.py:170
  53.5 7.1 %all-to-all-done.1.parts = bf16[16,72,128]{2,1,0:T(8,128)(2,1)S(1)} async-done(((bf16[16,72,128]{2,1,0:T(8,128)(2,1)}), bf16[16,72,128]{2,1,0:T(8,128)(2,1)S(1)}, u32[]{:S(2)}, u32[]{:S(2)}) %all-to-all-start.1) | async-done | bytes 294944 | tf_op jit(solution)/shard_map/all_to_all | solution.py:458
  60.6 1.7 %combine.1.heads = bf16[4,24,256]{2,1,0:T(8,128)(2,1)} custom-call(bf16[16,72,128]{2,1,0:T(8,128)(2,1)S(1)} %all-to-all-done.1.parts, bf16[1,256]{1,0:T(2,128)(2,1)S(1)} %decode.1.dec_out, f32[2]{0:T(128)S(1)} %copy-done.7, f32[1,128]{1,0:T(1,128)S(1)} %bitcast.16), custom_call_target="tpu_custom_call" | custom-call | flops 100000000 | bytes 1048576 | tf_op jit(solution)/shard_map/combine/pallas_call | solution.py:336
  62.2 4.3 %all-to-all-start.2 = ((bf16[4,24,256]{2,1,0:T(8,128)(2,1)}), bf16[4,24,256]{2,1,0:T(8,128)(2,1)S(1)}, u32[]{:S(2)}, u32[]{:S(2)}) async-start(bf16[4,24,256]{2,1,0:T(8,128)(2,1)} %combine.1.heads), calls=%async_computation.2 | async-start | bytes 98304 | tf_op jit(solution)/shard_map/all_to_all | solution.py:464
  66.5 0.0 copy-done
  66.5 1.0 %own_rows.1.own = f32[24,512]{1,0:T(8,128)S(1)} custom-call(s32[1]{0:T(128)} %bitcast.place, bf16[4,24,256]{2,1,0:T(8,128)(2,1)} %combine.1.heads, bf16[1024,512]{1,0:T(8,128)(2,1)S(1)} %copy-done), custom_call_target="tpu_custom_call" | custom-call | flops 1000000000 | bytes 1048576 | tf_op jit(solution)/shard_map/own_rows/pallas_call | solution.py:353
  67.5 4.6 %all-to-all-done.2.heads = bf16[4,24,256]{2,1,0:T(8,128)(2,1)S(1)} async-done(((bf16[4,24,256]{2,1,0:T(8,128)(2,1)}), bf16[4,24,256]{2,1,0:T(8,128)(2,1)S(1)}, u32[]{:S(2)}, u32[]{:S(2)}) %all-to-all-start.2) | async-done | bytes 49184 | tf_op jit(solution)/shard_map/all_to_all | solution.py:464
  72.1 0.9 %out_rows.1 = (bf16[16,512]{1,0:T(8,128)(2,1)}, bf16[1,512]{1,0:T(2,128)(2,1)}) custom-call(s32[1]{0:T(128)} %bitcast.place, f32[24,512]{1,0:T(8,128)S(1)} %own_rows.1.own, bf16[4,24,256]{2,1,0:T(8,128)(2,1)S(1)} %all-to-all-done.2.heads, bf16[1024,512]{1,0:T(8,128)(2,1)S(1)} %copy-done), custom_call_target="tpu_custom_call" | custom-call | flops 100000000 | bytes 1048576 | tf_op jit(solution)/shard_map/out_rows/pallas_call | solution.py:377
Async XLA Ops:
  0.6 24.6 %copy-start.1 = (bf16[2048,256]{1,0:T(8,128)(2,1)S(1)}, bf16[2048,256]{1,0:T(8,128)(2,1)}, u32[]{:S(2)}) copy-start(bf16[2048,256]{1,0:T(8,128)(2,1)} %w_key.1) | copy-start | bytes 3145732
  0.6 24.6 %copy-start.2 = (bf16[2048,256]{1,0:T(8,128)(2,1)S(1)}, bf16[2048,256]{1,0:T(8,128)(2,1)}, u32[]{:S(2)}) copy-start(bf16[2048,256]{1,0:T(8,128)(2,1)} %w_value.1) | copy-start | bytes 3145732
  3.2 9.7 %collective-permute-start.4 = (bf16[2,640,128]{2,1,0:T(8,128)(2,1)}, bf16[2,640,128]{2,1,0:T(8,128)(2,1)S(1)}, u32[]{:S(2)}, u32[]{:S(2)}) collective-permute-start(bf16[2,640,128]{2,1,0:T(8,128)(2,1)} %get-tuple-element.10.refs_6_), channel_id=1, source_target_pairs={{0,24},{4,28},{8,16},{12,20},{16,8},{20,12},{24,0},{28,4},{32,56},... | collective-permute-start | bytes 983048 | tf_op jit(solution)/shard_map/ppermute | solution.py:423
  4.9 9.3 %collective-permute-start.1 = (bf16[2,640,128]{2,1,0:T(8,128)(2,1)S(1)}, bf16[2,640,128]{2,1,0:T(8,128)(2,1)S(1)}, u32[]{:S(2)}, u32[]{:S(2)}) collective-permute-start(bf16[2,640,128]{2,1,0:T(8,128)(2,1)S(1)} %get-tuple-element.9.refs_3_.refs_2_), channel_id=1, source_target_pairs={{0,8},{4,12},{8,0},{12,4},{16,24},{20,28},{24,16},{28,20},{32,40},... | collective-permute-start | bytes 983048 | tf_op jit(solution)/shard_map/ppermute | solution.py:423
  6.8 18.4 %collective-permute-start = (bf16[2,640,128]{2,1,0:T(8,128)(2,1)S(1)}, bf16[2,640,128]{2,1,0:T(8,128)(2,1)}, u32[]{:S(2)}, u32[]{:S(2)}) collective-permute-start(bf16[2,640,128]{2,1,0:T(8,128)(2,1)S(1)} %get-tuple-element.9.refs_3_.refs_2_), channel_id=1, source_target_pairs={{0,4},{4,0},{8,12},{12,8},{16,20},{20,16},{24,28},{28,24},{32,36},... | collective-permute-start | bytes 983048 | tf_op jit(solution)/shard_map/ppermute | solution.py:423
  13.0 12.2 %collective-permute-start.5 = (bf16[2,640,128]{2,1,0:T(8,128)(2,1)S(1)}, bf16[2,640,128]{2,1,0:T(8,128)(2,1)}, u32[]{:S(2)}, u32[]{:S(2)}) collective-permute-start(bf16[2,640,128]{2,1,0:T(8,128)(2,1)S(1)} %collective-permute-done.4.refs_7_.refs_8_), channel_id=1, source_target_pairs={{0,4},{4,0},{8,12},{12,8},{16,20},{20,16},{24,28},{28,24},{32,36},... | collective-permute-start | bytes 983048 | tf_op jit(solution)/shard_map/ppermute | solution.py:423
  14.2 11.0 %collective-permute-start.2 = (bf16[2,640,128]{2,1,0:T(8,128)(2,1)S(1)}, bf16[2,640,128]{2,1,0:T(8,128)(2,1)}, u32[]{:S(2)}, u32[]{:S(2)}) collective-permute-start(bf16[2,640,128]{2,1,0:T(8,128)(2,1)S(1)} %collective-permute-done.1.refs_5_.refs_4_), channel_id=1, source_target_pairs={{0,4},{4,0},{8,12},{12,8},{16,20},{20,16},{24,28},{28,24},{32,36},... | collective-permute-start | bytes 983048 | tf_op jit(solution)/shard_map/ppermute | solution.py:423
  14.2 22.7 %collective-permute-start.3 = (bf16[2,640,128]{2,1,0:T(8,128)(2,1)}, bf16[2,640,128]{2,1,0:T(8,128)(2,1)}, u32[]{:S(2)}, u32[]{:S(2)}) collective-permute-start(bf16[2,640,128]{2,1,0:T(8,128)(2,1)} %get-tuple-element.10.refs_6_), channel_id=1, source_target_pairs={{0,4},{4,0},{8,12},{12,8},{16,20},{20,16},{24,28},{28,24},{32,36},... | collective-permute-start | bytes 983048 | tf_op jit(solution)/shard_map/ppermute | solution.py:423
  14.7 10.5 %copy-start.3 = (f32[2048]{0:T(1024)S(1)}, f32[2048]{0:T(1024)}, u32[]{:S(2)}) copy-start(f32[2048]{0:T(1024)} %param.16) | copy-start | bytes 24580
  14.7 22.2 %all-to-all-start = ((bf16[16,16,256]{2,1,0:T(8,128)(2,1)}), bf16[16,16,256]{2,1,0:T(8,128)(2,1)S(1)}, u32[]{:S(2)}, u32[]{:S(2)}) async-start(bf16[16,16,256]{2,1,0:T(8,128)(2,1)} %get-tuple-element.8), calls=%async_computation | async-start | bytes 262144 | tf_op jit(solution)/shard_map/all_to_all | solution.py:440
  43.0 4.4 %copy-start.9 = (bf16[1,256]{1,0:T(2,128)(2,1)S(1)}, bf16[1,256]{1,0:T(2,128)(2,1)}, u32[]{:S(2)}) copy-start(bf16[1,256]{1,0:T(2,128)(2,1)} %get-tuple-element.13.q_dec) | copy-start | bytes 1540
  43.0 17.6 %all-to-all-start.1 = ((bf16[16,72,128]{2,1,0:T(8,128)(2,1)}), bf16[16,72,128]{2,1,0:T(8,128)(2,1)S(1)}, u32[]{:S(2)}, u32[]{:S(2)}) async-start(bf16[16,72,128]{2,1,0:T(8,128)(2,1)} %attend.1), calls=%async_computation.1 | async-start | bytes 589824 | tf_op jit(solution)/shard_map/all_to_all | solution.py:458
  46.7 0.7 copy-start.6
  47.3 0.7 copy-start.7
  47.3 0.7 copy-start.8
  48.0 1.2 %copy-start.4 = (bf16[1,2048,2,128]{3,2,1,0:T(2,128)(2,1)S(1)}, bf16[1,2048,2,128]{3,2,1,0:T(2,128)(2,1)}, u32[]{:S(2)}) copy-start(bf16[1,2048,2,128]{3,2,1,0:T(2,128)(2,1)} %param.25) | copy-start | bytes 3145732
  49.2 1.2 %copy-start.5 = (bf16[1,2048,2,128]{3,2,1,0:T(2,128)(2,1)S(1)}, bf16[1,2048,2,128]{3,2,1,0:T(2,128)(2,1)}, u32[]{:S(2)}) copy-start(bf16[1,2048,2,128]{3,2,1,0:T(2,128)(2,1)} %param.26) | copy-start | bytes 3145732
  50.5 16.1 %copy-start = (bf16[1024,512]{1,0:T(8,128)(2,1)S(1)}, bf16[1024,512]{1,0:T(8,128)(2,1)}, u32[]{:S(2)}) copy-start(bf16[1024,512]{1,0:T(8,128)(2,1)} %w.5) | copy-start | bytes 3145732
  62.2 9.8 %all-to-all-start.2 = ((bf16[4,24,256]{2,1,0:T(8,128)(2,1)}), bf16[4,24,256]{2,1,0:T(8,128)(2,1)S(1)}, u32[]{:S(2)}, u32[]{:S(2)}) async-start(bf16[4,24,256]{2,1,0:T(8,128)(2,1)} %combine.1.heads), calls=%async_computation.2 | async-start | bytes 98304 | tf_op jit(solution)/shard_map/all_to_all | solution.py:464

commit v5 on v3

--- a/solution.py
+++ b/solution.py
@@ -13,7 +13,7 @@
 F32 = jnp.float32
 BF16 = jnp.bfloat16
 MIB = 1024 * 1024
-ATT, FRE, DEC, OPN = 20, 8, 16, 60
+ATT, FRE, DEC, OPN = 20, 8, 60, 60
 
 
 def nt_dot(a, b):
@@ -47,7 +47,8 @@
 
 
 def opening_body(
-    keys, values, x, x_dec, gain, w, pool0, pool1, out, out_dec, kv, xs, xd, g, wq, wide, normed, sems
+    keys, values, x, x_dec, gain, w, pool0, pool1, out, out_dec, row_dec, kv, xs, xd, g, wq, wide, normed,
+    sems
 ):
     pools = (pool0, pool1)
     copies = fetch(
@@ -69,10 +70,11 @@
     normed[rows:] = jnp.broadcast_to(
         rms(xd[...].astype(F32), g[...]).astype(BF16), (16, x.shape[1])
     )
+    row_dec[...] = normed[rows : rows + 1]
     for tile in range(x.shape[1] // 128):
         at = slots + rows * (tile // 2)
         for pool in pools:
-            pool[tile % 2, at : at + rows, :] = xs[:, tile * 128 : (tile + 1) * 128]
+            pool[tile % 2, at : at + rows, :] = normed[:rows, tile * 128 : (tile + 1) * 128]
     for index in range(2):
         copies[3 + index].wait()
         wide[index] = kv[index].astype(F32)
@@ -91,13 +93,14 @@
     return pl.pallas_call(
         opening_body,
         out_shape=(
-            jax.ShapeDtypeStruct((2, slots + rows * width // 256, 128), BF16),
-            jax.ShapeDtypeStruct((2, slots + rows * width // 256, 128), BF16),
-            jax.ShapeDtypeStruct((members, rows, w.shape[1]), BF16),
+            pltpu.VMEM((2, slots + rows * width // 256, 128), BF16),
+            pltpu.VMEM((2, slots + rows * width // 256, 128), BF16),
+            pltpu.VMEM((members, rows, w.shape[1]), BF16),
             jax.ShapeDtypeStruct((1, w.shape[1]), BF16),
+            jax.ShapeDtypeStruct((1, width), BF16),
         ),
         in_specs=[HBM] * 6,
-        out_specs=tuple(vmem(4)),
+        out_specs=tuple(vmem(5)),
         scratch_shapes=[
             pltpu.VMEM((2, 2 * slots, 128), BF16),
             pltpu.VMEM((rows, width), BF16),
@@ -115,17 +118,9 @@
 
 
 def decode_body(
-    x_dec, gain, w_key, w_value, q_dec, keys, values, length, lambdas, head_gain, head_out,
-    xd, g, wk, wv, kc, vc, sems
+    q_dec, k_dec, v_dec, keys, values, length, lambdas, head_gain, head_out, kc, vc, sems
 ):
-    copies = fetch(
-        ((x_dec, xd), (gain, g), (w_key, wk), (keys, kc), (w_value, wv), (values, vc)), sems
-    )
-    for copy in copies[:2]:
-        copy.wait()
-    normed = jnp.broadcast_to(rms(xd[...].astype(F32), g[...]).astype(BF16), (16, xd.shape[1]))
-    copies[2].wait()
-    new_keys = nn_dot(normed, wk[...]).astype(BF16)[:1]
+    copies = fetch(((keys, kc), (values, vc)), sems)
 
     row = lax.broadcasted_iota(jnp.int32, (8, 128), 0)
     lane = lane_iota((8, 128))
@@ -141,9 +136,10 @@
 
     half = lane // 64 == row % 2
     queries = jnp.where(half, per_head(q_dec[...]), 0.0)
-    own_keys = per_head(new_keys)
+    own_keys = per_head(k_dec[...])
+    own_values = per_head(v_dec[...])
     scale = 0.125 * math.log2(math.e)
-    copies[3].wait()
+    copies[0].wait()
     scores = nt_dot(queries.astype(BF16), kc[...])
     width = keys.shape[0]
     column = lane_iota((8, width))
@@ -155,9 +151,7 @@
     weights = jnp.exp2((scores - row_max) * scale)
     own_weight = jnp.exp2((own_score - row_max) * scale)
     totals = jnp.sum(weights, axis=-1, keepdims=True) + own_weight
-    copies[4].wait()
-    own_values = per_head(nn_dot(normed, wv[...]).astype(BF16)[:1])
-    copies[5].wait()
+    copies[1].wait()
     mixed = nn_dot(weights.astype(BF16), vc[...])
     mixed = (mixed + own_weight.astype(BF16).astype(F32) * own_values) / totals
     for head in range(2):
@@ -165,68 +159,76 @@
         head_out[:, head * 128 : (head + 1) * 128] = rms(attended, head_gain[...]).astype(BF16)
 
 
-def decode(x_dec, gain, w_key, w_value, q_dec, keys, values, length, lambdas, head_gain):
+def decode(q_dec, k_dec, v_dec, keys, values, length, lambdas, head_gain):
     smem = pl.BlockSpec(memory_space=pltpu.SMEM)
     return pl.pallas_call(
         decode_body,
-        out_shape=jax.ShapeDtypeStruct((1, 256), BF16),
-        in_specs=[HBM] * 4 + vmem(1) + [HBM] * 2 + [smem, smem] + vmem(1),
+        out_shape=pltpu.VMEM((1, 256), BF16),
+        in_specs=vmem(3) + [HBM] * 2 + [smem, smem] + vmem(1),
         out_specs=vmem(1)[0],
         scratch_shapes=[
-            pltpu.VMEM(x_dec.shape, BF16),
-            pltpu.VMEM(gain.shape, F32),
-            pltpu.VMEM(w_key.shape, BF16),
-            pltpu.VMEM(w_value.shape, BF16),
             pltpu.VMEM(keys.shape, BF16),
             pltpu.VMEM(values.shape, BF16),
-            pltpu.SemaphoreType.DMA((6,)),
+            pltpu.SemaphoreType.DMA((2,)),
         ],
         compiler_params=pltpu.CompilerParams(vmem_limit_bytes=DEC * MIB),
-        cost_estimate=pl.CostEstimate(flops=2 * 10**9, bytes_accessed=4 * MIB, transcendentals=0),
+        cost_estimate=pl.CostEstimate(flops=2 * 10**9, bytes_accessed=2 * MIB, transcendentals=0),
         name="decode",
-    )(x_dec, gain, w_key, w_value, q_dec, keys, values, length, lambdas, head_gain)
+    )(q_dec, k_dec, v_dec, keys, values, length, lambdas, head_gain)
 
 
 def fresh_body(*refs):
-    gain, w_key, w_value = refs[:3]
+    row_dec, w_key, w_value = refs[:3]
     sources = refs[3:9]
-    k_out, v_out, normed = refs[9:]
+    k_out, v_out, k_dec, v_dec, xs, normed, sems = refs[9:]
     rows = k_out.shape[0] // 4
-    tiles = gain.shape[1] // 128
+    tiles = row_dec.shape[1] // 128
     slots = sources[0].shape[1] - rows * tiles // 2
-    for index, source in enumerate(sources):
-        parts = [
-            source[tile % 2, slots + rows * (tile // 2) : slots + rows * (tile // 2 + 1), :]
-            for tile in range(tiles)
-        ]
-        x = jnp.concatenate(parts, axis=1).astype(F32)
-        normed[index * rows : (index + 1) * rows] = rms(x, gain[...]).astype(BF16)
-    for w, out in ((w_key, k_out), (w_value, v_out)):
+    copies = fetch([(s.at[:, slots:], xs.at[i]) for i, s in enumerate(sources)], sems)
+    normed[6 * rows :] = jnp.broadcast_to(row_dec[...], (16, row_dec.shape[1]))
+    for index in range(6):
+        copies[index].wait()
+        for tile in range(tiles):
+            normed[index * rows : (index + 1) * rows, tile * 128 : (tile + 1) * 128] = xs[
+                index, tile % 2, rows * (tile // 2) : rows * (tile // 2 + 1), :
+            ]
+    for w, out, out_dec in ((w_key, k_out, k_dec), (w_value, v_out, v_dec)):
         result = nn_dot(normed[...], w[...]).astype(BF16)
         out[:, :128] = result[: 4 * rows, :128]
         out[: 2 * rows, 128:] = result[: 2 * rows, 128:]
-        out[2 * rows :, 128:] = result[4 * rows :, 128:]
-
-
-def fresh(gain, w_key, w_value, pools0, pools1, rows):
+        out[2 * rows :, 128:] = result[4 * rows : 6 * rows, 128:]
+        out_dec[...] = result[6 * rows : 6 * rows + 1]
+
+
+def fresh(row_dec, w_key, w_value, pools0, pools1, rows):
     sources = [*pools0, *pools1[2:]]
-    width = gain.shape[1]
+    width = row_dec.shape[1]
     return pl.pallas_call(
         fresh_body,
-        out_shape=(jax.ShapeDtypeStruct((4 * rows, 256), BF16),) * 2,
-        in_specs=vmem(9),
-        out_specs=tuple(vmem(2)),
-        scratch_shapes=[pltpu.VMEM((6 * rows, width), BF16)],
+        out_shape=(
+            jax.ShapeDtypeStruct((4 * rows, 256), BF16),
+            jax.ShapeDtypeStruct((4 * rows, 256), BF16),
+            jax.ShapeDtypeStruct((1, 256), BF16),
+            jax.ShapeDtypeStruct((1, 256), BF16),
+        ),
+        in_specs=vmem(3) + [HBM] * 6,
+        out_specs=tuple(vmem(4)),
+        scratch_shapes=[
+            pltpu.VMEM((6, 2, rows * width // 256, 128), BF16),
+            pltpu.VMEM((6 * rows + 16, width), BF16),
+            pltpu.SemaphoreType.DMA((6,)),
+        ],
         compiler_params=pltpu.CompilerParams(vmem_limit_bytes=FRE * MIB),
         cost_estimate=pl.CostEstimate(flops=10**9, bytes_accessed=2 * MIB, transcendentals=0),
         name="fresh",
-    )(gain, w_key, w_value, *sources)
+    )(row_dec, w_key, w_value, *sources)
 
 
 def attend_body(slots, *refs):
     ids, queries = refs[:2]
-    pool = refs[2:10]
-    k_new, v_new, out = refs[10:]
+    sources = refs[2:10]
+    k_new, v_new, out, pool, sems = refs[10:]
+    copies = fetch([(s.at[:, :slots], pool.at[i]) for i, s in enumerate(sources)], sems)
     rows = queries.shape[0]
     fresh_rows = k_new.shape[0]
     each = fresh_rows // 4
@@ -248,11 +250,13 @@
         cols = slice(head * 128, (head + 1) * 128)
         q = queries[:, cols].astype(F32)
         places = range(4 * head, 4 * head + 4)
+        for i in places:
+            copies[i].wait()
         for which in range(2):
             combo = 2 * head + which
             kept = (lane < 64) if which == 0 else (lane >= 64)
             masked = jnp.where(kept, q, 0.0).astype(BF16)
-            scores = [nt_dot(masked, pool[i][0, :slots]) for i in places]
+            scores = [nt_dot(masked, pool[i, 0]) for i in places]
             last = jnp.where(allowed, nt_dot(masked, k_new[:, cols]), NEG)
             row_max = jnp.max(last, axis=-1, keepdims=True)
             for s in scores:
@@ -263,25 +267,34 @@
             for s, i in zip(scores, places):
                 weights = jnp.exp2((s - row_max) * scale)
                 total = total + jnp.sum(weights, axis=-1, keepdims=True)
-                mixed = mixed + nn_dot(weights.astype(BF16), pool[i][1, :slots])
+                mixed = mixed + nn_dot(weights.astype(BF16), pool[i, 1])
             mixed = mixed / total
-            out[:, combo * 128 : (combo + 1) * 128] = mixed.astype(BF16)
+            out[:, combo * each : (combo + 1) * each, :] = mixed.astype(BF16).reshape(
+                rows // each, each, 128
+            )
             for base, stat in ((0, row_max), (4, total)):
                 for part in range(3):
                     piece = stat.astype(BF16).astype(F32)
-                    stats = jnp.where(lane == 8 * part + base + combo, piece, stats)
+                    stats = jnp.where(lane % 64 == 8 * part + base + combo, piece, stats)
                     stat = stat - piece
-    out[:, 512:640] = stats.astype(BF16)
+    stats = stats.reshape(rows // each, 2, each // 2, 128)
+    low = lane_iota((rows // each, each // 2, 128)) < 64
+    out[:, 4 * each :, :] = jnp.where(low, stats[:, 0], stats[:, 1]).astype(BF16)
 
 
 def attend(ids, queries, pools0, pools1, slots, k_new, v_new):
     rows = queries.shape[0]
     keys = 4 * slots + k_new.shape[0]
+    each = k_new.shape[0] // 4
     return pl.pallas_call(
         lambda *refs: attend_body(slots, *refs),
-        out_shape=jax.ShapeDtypeStruct((rows, 640), BF16),
-        in_specs=[pl.BlockSpec(memory_space=pltpu.SMEM)] + vmem(11),
+        out_shape=pltpu.HBM((rows // each, 4 * each + each // 2, 128), BF16),
+        in_specs=[pl.BlockSpec(memory_space=pltpu.SMEM)] + vmem(1) + [HBM] * 8 + vmem(2),
         out_specs=vmem(1)[0],
+        scratch_shapes=[
+            pltpu.VMEM((8, 2, slots, 128), BF16),
+            pltpu.SemaphoreType.DMA((8,)),
+        ],
         compiler_params=pltpu.CompilerParams(vmem_limit_bytes=ATT * MIB),
         cost_estimate=pl.CostEstimate(
             flops=4 * rows * keys * 512, bytes_accessed=2 * MIB, transcendentals=4 * rows * keys
@@ -293,10 +306,11 @@
 def combine_body(parts, dec_out, lambdas, head_gain, out):
     scale = 0.125 * math.log2(math.e)
     members = parts.shape[0]
-    rows = parts.shape[1]
+    rows = parts.shape[1] * 2 // 9
 
     def whole(member):
-        pieces = parts[member, :, 512:640].astype(F32)
+        pieces = parts[member, 4 * rows :, :].astype(F32)
+        pieces = jnp.concatenate([pieces, pltpu.roll(pieces, 64, 1)], axis=0)
         return pieces + pltpu.roll(pieces, 120, 1) + pltpu.roll(pieces, 112, 1)
 
     stats = [whole(member) for member in range(members)]
@@ -312,7 +326,7 @@
         acc = jnp.zeros((rows, 128), F32)
         for member in range(members):
             acc = acc + shares[member][:, combo : combo + 1] * parts[
-                member, :, combo * 128 : (combo + 1) * 128
+                member, combo * rows : (combo + 1) * rows, :
             ].astype(F32)
         sums.append(acc / total[:, combo : combo + 1])
     heads = []
@@ -326,9 +340,10 @@
 
 
 def combine(parts, dec_out, lambdas, head_gain, copies):
+    rows = parts.shape[1] * 2 // 9
     return pl.pallas_call(
         combine_body,
-        out_shape=jax.ShapeDtypeStruct((copies, parts.shape[1] + 8, 256), BF16),
+        out_shape=jax.ShapeDtypeStruct((copies, rows + 8, 256), BF16),
         in_specs=vmem(2) + [pl.BlockSpec(memory_space=pltpu.SMEM)] + vmem(1),
         out_specs=vmem(1)[0],
         compiler_params=pltpu.CompilerParams(vmem_limit_bytes=16 * MIB),
@@ -395,7 +410,7 @@
     def move(array, target):
         return lax.ppermute(array, "kv", [(i, target(i)) for i in range(kv_count)])
 
-    pool0, pool1, sent, q_dec = opening(
+    pool0, pool1, sent, q_dec, row_dec = opening(
         piece_keys.reshape(-1, 128),
         piece_values.reshape(-1, 128),
         x_piece,
@@ -411,25 +426,23 @@
     pools0.append(move(far0, lambda i: i ^ 1))
     pools1.append(move(far1, lambda i: i ^ 1))
     got = lax.all_to_all(sent, "kv", 0, 0, tiled=True, axis_index_groups=groups)
+    k_new, v_new, k_dec, v_dec = fresh(row_dec, w_key, w_value, pools0, pools1, rows)
     dec_out = decode(
-        x_decode,
-        gain,
-        w_key,
-        w_value,
         q_dec,
+        k_dec,
+        v_dec,
         cache_keys.reshape(-1, 128),
         cache_values.reshape(-1, 128),
         cache_lengths,
         lambdas,
         head_gain,
     )
-    k_new, v_new = fresh(gain, w_key, w_value, pools0, pools1, rows)
     slots = piece_keys.shape[0]
     parts = attend(
         ids, got.reshape(members * rows, 256), pools0, pools1, slots, k_new, v_new
     )
     parts = lax.all_to_all(
-        parts.reshape(members, rows, 640), "kv", 0, 0, tiled=True, axis_index_groups=groups
+        parts, "kv", 0, 0, tiled=True, axis_index_groups=groups
     )
     heads = combine(parts, dec_out, lambdas, head_gain, tp_count)
     heads = lax.all_to_all(heads, "tp", 0, 0, tiled=True)

time: 75.2 us -> 72.4 us (0.963)
  local copies, waits for them, and re-layouts: 7.73 us -> 0.67 us
  waiting for transfers between devices: 22.9 us -> 27.2 us
    unnamed x32 -> x16, local copies, waits for them, and re-layouts: 7.73 us -> 0.67 us
    all_to_all x1, waiting for transfers between devices: 7.78 us -> 10.2 us  [layer(): lax.all_to_all(parts, 'kv', 0, 0, tiled=True, axis_index_groups=groups)]
    all_to_all x1, waiting for transfers between devices: 7.49 us -> 9.53 us  [layer(): got = lax.all_to_all(sent, 'kv', 0, 0, tiled=True, axis_index_groups=groups)]
where the time goes in v5:
time: 72.4 us; the launch traced here: 71.9 us
  waiting for transfers between devices  27.2 us (38%)
  starting transfers between devices  17.9 us (25%)
  Pallas kernels  15.1 us (21%)
  blocking collectives  9.64 us (13%)
  between operations  1.45 us (2%)
    all_to_all x1, starting transfers between devices, layer(): got = lax.all_to_all(sent, 'kv', 0, 0, tiled=True, axis_index_groups=groups)  10.3 us
    all_to_all x1, waiting for transfers between devices, layer(): lax.all_to_all(parts, 'kv', 0, 0, tiled=True, axis_index_groups=groups)  10.2 us
    all_to_all x1, blocking collectives, layer(): heads = lax.all_to_all(heads, 'tp', 0, 0, tiled=True)  9.64 us
    all_to_all x1, waiting for transfers between devices, layer(): got = lax.all_to_all(sent, 'kv', 0, 0, tiled=True, axis_index_groups=groups)  9.53 us
    ppermute x6, waiting for transfers between devices, move(): return lax.ppermute(array, 'kv', [(i, target(i)) for i in range(kv_count)])  7.43 us
    pallas_call x1, Pallas kernels, attend(): pl.pallas_call(lambda *refs: attend_body(slots, *refs), out_shape=pltpu.H...  6.06 us
    ppermute x6, starting transfers between devices, move(): return lax.ppermute(array, 'kv', [(i, target(i)) for i in range(kv_count)])  4.07 us
    all_to_all x1, starting transfers between devices, layer(): lax.all_to_all(parts, 'kv', 0, 0, tiled=True, axis_index_groups=groups)  3.55 us
  transfers between devices with their start and end apart: 8, of which 4 were waited for; matrix products, arithmetic and copies ran while one was open for 0% of the time, Pallas kernels for 6%

profile of v5, /device:TPU:8, one launch (start us, length us, event | category | flops | bytes accessed | tf_op | source)
XLA Modules:
  0.0 71.9 jit_solution(7597163441070945836)
XLA Ops:
  0.6 0.0 copy-start.1
  0.6 0.0 copy-start.2
  0.7 2.6 %opening.1 = (bf16[2,640,128]{2,1,0:T(8,128)(2,1)S(1)}, bf16[2,640,128]{2,1,0:T(8,128)(2,1)}, bf16[16,16,256]{2,1,0:T(8,128)(2,1)}, bf16[1,256]{1,0:T(2,128)(2,1)}, bf16[1,2048]{1,0:T(2,128)(2,1)}) custom-call(bf16[1024,128]{1,0:T(8,128)(2,1)} %bitcast.13, bf16[1024,128]{1,0:T(8,128)(2,1)} %bitcast.14, bf16[16,2048]{1,0:T(8,128)(2,1)} %x.1, ...), custom_call_target="tpu_custom_call" | custom-call | flops 1000000000 | bytes 2097152 | tf_op jit(solution)/shard_map/opening/pallas_call | solution.py:93
  3.3 1.7 %collective-permute-start.4 = (bf16[2,640,128]{2,1,0:T(8,128)(2,1)}, bf16[2,640,128]{2,1,0:T(8,128)(2,1)S(1)}, u32[]{:S(2)}, u32[]{:S(2)}) collective-permute-start(bf16[2,640,128]{2,1,0:T(8,128)(2,1)} %get-tuple-element.13.refs_6_), channel_id=1, source_target_pairs={{0,24},{4,28},{8,16},{12,20},{16,8},{20,12},{24,0},{28,4},{32,56},... | collective-permute-start | bytes 983048 | tf_op jit(solution)/shard_map/ppermute | solution.py:411
  4.9 1.9 %collective-permute-start.1 = (bf16[2,640,128]{2,1,0:T(8,128)(2,1)S(1)}, bf16[2,640,128]{2,1,0:T(8,128)(2,1)S(1)}, u32[]{:S(2)}, u32[]{:S(2)}) collective-permute-start(bf16[2,640,128]{2,1,0:T(8,128)(2,1)S(1)} %get-tuple-element.12.refs_3_.refs_2_), channel_id=1, source_target_pairs={{0,8},{4,12},{8,0},{12,4},{16,24},{20,28},{24,16},{28,20},{32,40},... | collective-permute-start | bytes 983048 | tf_op jit(solution)/shard_map/ppermute | solution.py:411
  6.8 0.0 collective-permute-start
  6.8 6.2 %collective-permute-done.4.refs_7_.refs_8_ = bf16[2,640,128]{2,1,0:T(8,128)(2,1)S(1)} collective-permute-done((bf16[2,640,128]{2,1,0:T(8,128)(2,1)}, bf16[2,640,128]{2,1,0:T(8,128)(2,1)S(1)}, u32[]{:S(2)}, u32[]{:S(2)}) %collective-permute-start.4) | collective-permute-done | bytes 327712 | tf_op jit(solution)/shard_map/ppermute | solution.py:411
  13.0 0.0 collective-permute-start.5
  13.0 1.2 %collective-permute-done.1.refs_5_.refs_4_ = bf16[2,640,128]{2,1,0:T(8,128)(2,1)S(1)} collective-permute-done((bf16[2,640,128]{2,1,0:T(8,128)(2,1)S(1)}, bf16[2,640,128]{2,1,0:T(8,128)(2,1)S(1)}, u32[]{:S(2)}, u32[]{:S(2)}) %collective-permute-start.1) | collective-permute-done | bytes 327712 | tf_op jit(solution)/shard_map/ppermute | solution.py:411
  14.2 0.0 collective-permute-start.2
  14.2 0.5 collective-permute-start.3
  14.7 10.3 %all-to-all-start = ((bf16[16,16,256]{2,1,0:T(8,128)(2,1)}), bf16[16,16,256]{2,1,0:T(8,128)(2,1)S(1)}, u32[]{:S(2)}, u32[]{:S(2)}) async-start(bf16[16,16,256]{2,1,0:T(8,128)(2,1)} %get-tuple-element.11), calls=%async_computation | async-start | bytes 262144 | tf_op jit(solution)/shard_map/all_to_all | solution.py:428
  25.0 0.0 copy-start.3
  25.1 0.0 collective-permute-done.refs_4_.refs_3_
  25.1 0.0 collective-permute-done.5.refs_8_.refs_9_
  25.1 0.0 collective-permute-done.2.refs_6_.refs_5_
  25.1 0.0 copy-done.1
  25.1 0.0 copy-done.2
  25.1 0.6 copy-done.3
  25.7 1.5 %fresh.1 = (bf16[64,256]{1,0:T(8,128)(2,1)S(1)}, bf16[64,256]{1,0:T(8,128)(2,1)S(1)}, bf16[1,256]{1,0:T(2,128)(2,1)S(1)}, bf16[1,256]{1,0:T(2,128)(2,1)S(1)}) custom-call(bf16[1,2048]{1,0:T(2,128)(2,1)S(1)} %copy-done.3, bf16[2048,256]{1,0:T(8,128)(2,1)S(1)} %copy-done.1, bf16[2048,256]{1,0:T(8,128)(2,1)S(1)} %copy-done.2, ...), custom_call_target="tpu_custom_call" | custom-call | flops 1000000000 | bytes 2097152 | tf_op jit(solution)/shard_map/fresh/pallas_call | solution.py:206
  27.2 0.0 copy-start.4
  27.2 0.0 copy-start.5
  27.2 9.5 %all-to-all-done = bf16[16,16,256]{2,1,0:T(8,128)(2,1)S(1)} async-done(((bf16[16,16,256]{2,1,0:T(8,128)(2,1)}), bf16[16,16,256]{2,1,0:T(8,128)(2,1)S(1)}, u32[]{:S(2)}, u32[]{:S(2)}) %all-to-all-start) | async-done | bytes 131104 | tf_op jit(solution)/shard_map/all_to_all | solution.py:428
  36.8 0.0 collective-permute-done.3.refs_7_
  36.8 0.0 copy-done.4
  36.8 0.0 copy-done.5
  36.8 6.1 %attend.1 = bf16[16,72,128]{2,1,0:T(8,128)(2,1)} custom-call(s32[1]{0:T(128)} %bitcast.refs_0_, bf16[256,256]{1,0:T(8,128)(2,1)S(1)} %bitcast.8, bf16[2,640,128]{2,1,0:T(8,128)(2,1)S(1)} %get-tuple-element.12.refs_3_.refs_2_, bf16[2,640,128]{2,1,0:T(8,128)(2,1)} %collective-permute-done.refs_4_.refs_3_, ...), custom_call_target="tpu_custom_call" | custom-call | flops 1107296256 | bytes 2097152 | tf_op jit(solution)/shard_map/attend/pallas_call | solution.py:289
  42.9 3.5 %all-to-all-start.1 = ((bf16[16,72,128]{2,1,0:T(8,128)(2,1)}), bf16[16,72,128]{2,1,0:T(8,128)(2,1)S(1)}, u32[]{:S(2)}, u32[]{:S(2)}) async-start(bf16[16,72,128]{2,1,0:T(8,128)(2,1)} %attend.1), calls=%async_computation.1 | async-start | bytes 589824 | tf_op jit(solution)/shard_map/all_to_all | solution.py:444
  47.1 0.0 copy-start.6
  47.1 0.0 copy-start.7
  47.1 0.0 copy-start
  47.1 3.0 %decode.1.dec_out = bf16[1,256]{1,0:T(2,128)(2,1)S(1)} custom-call(bf16[1,256]{1,0:T(2,128)(2,1)} %get-tuple-element.17.q_dec, bf16[1,256]{1,0:T(2,128)(2,1)} %copy-done.4, bf16[1,256]{1,0:T(2,128)(2,1)} %copy-done.5, bf16[4096,128]{1,0:T(8,128)(2,1)} %bitcast.11, bf16[4096,128]{1,0:T(8,128)(2,1)} %bitcast.12, s32[1]{0:T(128)S(6)} %copy.16.length, ...), custom_call_target="tpu_custom_call" | custom-call | flops 2000000000 | bytes 2097152 | tf_op jit(solution)/shard_map/decode/pallas_call | solution.py:164
  50.1 10.2 %all-to-all-done.1.parts = bf16[16,72,128]{2,1,0:T(8,128)(2,1)S(1)} async-done(((bf16[16,72,128]{2,1,0:T(8,128)(2,1)}), bf16[16,72,128]{2,1,0:T(8,128)(2,1)S(1)}, u32[]{:S(2)}, u32[]{:S(2)}) %all-to-all-start.1) | async-done | bytes 294944 | tf_op jit(solution)/shard_map/all_to_all | solution.py:444
  60.3 0.0 copy-done.6
  60.3 0.0 copy-done.7
  60.3 1.1 %combine.1 = bf16[4,24,256]{2,1,0:T(8,128)(2,1)S(1)} custom-call(bf16[16,72,128]{2,1,0:T(8,128)(2,1)S(1)} %all-to-all-done.1.parts, bf16[1,256]{1,0:T(2,128)(2,1)S(1)} %decode.1.dec_out, f32[2]{0:T(128)S(1)} %copy-done.6, f32[1,128]{1,0:T(1,128)S(1)} %bitcast.10), custom_call_target="tpu_custom_call" | custom-call | flops 100000000 | bytes 1048576 | tf_op jit(solution)/shard_map/combine/pallas_call | solution.py:344
  61.4 9.6 %all_to_all.15.heads = bf16[4,24,256]{2,1,0:T(8,128)(2,1)S(1)} all-to-all(bf16[4,24,256]{2,1,0:T(8,128)(2,1)S(1)} %combine.1), channel_id=1, replica_groups=mesh['kv'=64,'tp'=4] {'tp'}, dimensions={0} | all-to-all | bytes 98304 | tf_op jit(solution)/shard_map/all_to_all | solution.py:448
  71.0 0.0 copy-done
  71.0 0.9 %out_rows.1 = (bf16[16,512]{1,0:T(8,128)(2,1)}, bf16[1,512]{1,0:T(2,128)(2,1)}) custom-call(bf16[4,24,256]{2,1,0:T(8,128)(2,1)S(1)} %all_to_all.15.heads, bf16[1024,512]{1,0:T(8,128)(2,1)S(1)} %copy-done), custom_call_target="tpu_custom_call" | custom-call | flops 100000000 | bytes 1048576 | tf_op jit(solution)/shard_map/out_rows/pallas_call | solution.py:365
Async XLA Ops:
  0.6 24.5 %copy-start.1 = (bf16[2048,256]{1,0:T(8,128)(2,1)S(1)}, bf16[2048,256]{1,0:T(8,128)(2,1)}, u32[]{:S(2)}) copy-start(bf16[2048,256]{1,0:T(8,128)(2,1)} %refs_1_.1) | copy-start | bytes 3145732
  0.6 24.5 %copy-start.2 = (bf16[2048,256]{1,0:T(8,128)(2,1)S(1)}, bf16[2048,256]{1,0:T(8,128)(2,1)}, u32[]{:S(2)}) copy-start(bf16[2048,256]{1,0:T(8,128)(2,1)} %refs_2_.1) | copy-start | bytes 3145732
  3.3 9.7 %collective-permute-start.4 = (bf16[2,640,128]{2,1,0:T(8,128)(2,1)}, bf16[2,640,128]{2,1,0:T(8,128)(2,1)S(1)}, u32[]{:S(2)}, u32[]{:S(2)}) collective-permute-start(bf16[2,640,128]{2,1,0:T(8,128)(2,1)} %get-tuple-element.13.refs_6_), channel_id=1, source_target_pairs={{0,24},{4,28},{8,16},{12,20},{16,8},{20,12},{24,0},{28,4},{32,56},... | collective-permute-start | bytes 983048 | tf_op jit(solution)/shard_map/ppermute | solution.py:411
  4.9 9.3 %collective-permute-start.1 = (bf16[2,640,128]{2,1,0:T(8,128)(2,1)S(1)}, bf16[2,640,128]{2,1,0:T(8,128)(2,1)S(1)}, u32[]{:S(2)}, u32[]{:S(2)}) collective-permute-start(bf16[2,640,128]{2,1,0:T(8,128)(2,1)S(1)} %get-tuple-element.12.refs_3_.refs_2_), channel_id=1, source_target_pairs={{0,8},{4,12},{8,0},{12,4},{16,24},{20,28},{24,16},{28,20},{32,40},... | collective-permute-start | bytes 983048 | tf_op jit(solution)/shard_map/ppermute | solution.py:411
  6.8 18.3 %collective-permute-start = (bf16[2,640,128]{2,1,0:T(8,128)(2,1)S(1)}, bf16[2,640,128]{2,1,0:T(8,128)(2,1)}, u32[]{:S(2)}, u32[]{:S(2)}) collective-permute-start(bf16[2,640,128]{2,1,0:T(8,128)(2,1)S(1)} %get-tuple-element.12.refs_3_.refs_2_), channel_id=1, source_target_pairs={{0,4},{4,0},{8,12},{12,8},{16,20},{20,16},{24,28},{28,24},{32,36},... | collective-permute-start | bytes 983048 | tf_op jit(solution)/shard_map/ppermute | solution.py:411
  13.0 12.1 %collective-permute-start.5 = (bf16[2,640,128]{2,1,0:T(8,128)(2,1)S(1)}, bf16[2,640,128]{2,1,0:T(8,128)(2,1)}, u32[]{:S(2)}, u32[]{:S(2)}) collective-permute-start(bf16[2,640,128]{2,1,0:T(8,128)(2,1)S(1)} %collective-permute-done.4.refs_7_.refs_8_), channel_id=1, source_target_pairs={{0,4},{4,0},{8,12},{12,8},{16,20},{20,16},{24,28},{28,24},{32,36},... | collective-permute-start | bytes 983048 | tf_op jit(solution)/shard_map/ppermute | solution.py:411
  14.2 10.8 %collective-permute-start.2 = (bf16[2,640,128]{2,1,0:T(8,128)(2,1)S(1)}, bf16[2,640,128]{2,1,0:T(8,128)(2,1)}, u32[]{:S(2)}, u32[]{:S(2)}) collective-permute-start(bf16[2,640,128]{2,1,0:T(8,128)(2,1)S(1)} %collective-permute-done.1.refs_5_.refs_4_), channel_id=1, source_target_pairs={{0,4},{4,0},{8,12},{12,8},{16,20},{20,16},{24,28},{28,24},{32,36},... | collective-permute-start | bytes 983048 | tf_op jit(solution)/shard_map/ppermute | solution.py:411
  14.2 22.5 %collective-permute-start.3 = (bf16[2,640,128]{2,1,0:T(8,128)(2,1)}, bf16[2,640,128]{2,1,0:T(8,128)(2,1)}, u32[]{:S(2)}, u32[]{:S(2)}) collective-permute-start(bf16[2,640,128]{2,1,0:T(8,128)(2,1)} %get-tuple-element.13.refs_6_), channel_id=1, source_target_pairs={{0,4},{4,0},{8,12},{12,8},{16,20},{20,16},{24,28},{28,24},{32,36},... | collective-permute-start | bytes 983048 | tf_op jit(solution)/shard_map/ppermute | solution.py:411
  14.7 22.0 %all-to-all-start = ((bf16[16,16,256]{2,1,0:T(8,128)(2,1)}), bf16[16,16,256]{2,1,0:T(8,128)(2,1)S(1)}, u32[]{:S(2)}, u32[]{:S(2)}) async-start(bf16[16,16,256]{2,1,0:T(8,128)(2,1)} %get-tuple-element.11), calls=%async_computation | async-start | bytes 262144 | tf_op jit(solution)/shard_map/all_to_all | solution.py:428
  25.0 0.7 copy-start.3
  27.2 9.6 %copy-start.4 = (bf16[1,256]{1,0:T(2,128)(2,1)}, bf16[1,256]{1,0:T(2,128)(2,1)S(1)}, u32[]{:S(2)}) copy-start(bf16[1,256]{1,0:T(2,128)(2,1)S(1)} %get-tuple-element.18.k_dec) | copy-start | bytes 1540
  27.2 9.6 %copy-start.5 = (bf16[1,256]{1,0:T(2,128)(2,1)}, bf16[1,256]{1,0:T(2,128)(2,1)S(1)}, u32[]{:S(2)}) copy-start(bf16[1,256]{1,0:T(2,128)(2,1)S(1)} %get-tuple-element.19.v_dec) | copy-start | bytes 1540
  42.9 17.5 %all-to-all-start.1 = ((bf16[16,72,128]{2,1,0:T(8,128)(2,1)}), bf16[16,72,128]{2,1,0:T(8,128)(2,1)S(1)}, u32[]{:S(2)}, u32[]{:S(2)}) async-start(bf16[16,72,128]{2,1,0:T(8,128)(2,1)} %attend.1), calls=%async_computation.1 | async-start | bytes 589824 | tf_op jit(solution)/shard_map/all_to_all | solution.py:444
  47.1 13.3 %copy-start.6 = (f32[2]{0:T(128)S(1)}, f32[2]{0:T(128)}, u32[]{:S(2)}) copy-start(f32[2]{0:T(128)} %lambdas.3) | copy-start | bytes 28
  47.1 13.2 %copy-start.7 = (f32[128]{0:T(128)S(1)}, f32[128]{0:T(128)}, u32[]{:S(2)}) copy-start(f32[128]{0:T(128)} %param.21) | copy-start | bytes 1540
  47.1 23.9 %copy-start = (bf16[1024,512]{1,0:T(8,128)(2,1)S(1)}, bf16[1024,512]{1,0:T(8,128)(2,1)}, u32[]{:S(2)}) copy-start(bf16[1024,512]{1,0:T(8,128)(2,1)} %w.3) | copy-start | bytes 3145732

commit v6 on v5

--- a/solution.py
+++ b/solution.py
@@ -47,10 +47,10 @@
 
 
 def opening_body(
-    keys, values, x, x_dec, gain, w, pool0, pool1, out, out_dec, row_dec, kv, xs, xd, g, wq, wide, normed,
+    keys, values, x, x_dec, gain, w, pool, out, out_dec, row_dec, kv, xs, xd, g, wq, wide, normed,
     sems
 ):
-    pools = (pool0, pool1)
+
     copies = fetch(
         (
             (x, xs),
@@ -72,14 +72,15 @@
     )
     row_dec[...] = normed[rows : rows + 1]
     for tile in range(x.shape[1] // 128):
-        at = slots + rows * (tile // 2)
-        for pool in pools:
-            pool[tile % 2, at : at + rows, :] = normed[:rows, tile * 128 : (tile + 1) * 128]
+        at = slots + rows * (tile // 4)
+        pool[tile % 4, at : at + rows, :] = normed[:rows, tile * 128 : (tile + 1) * 128]
     for index in range(2):
         copies[3 + index].wait()
         wide[index] = kv[index].astype(F32)
         for head in range(2):
-            pools[head][index, :slots] = wide[index, pl.ds(head, slots, stride=2), :].astype(BF16)
+            pool[2 * head + index, :slots] = wide[index, pl.ds(head, slots, stride=2), :].astype(
+                BF16
+            )
     copies[5].wait()
     result = nn_dot(normed[...], wq[...]).astype(BF16)
     for member in range(out.shape[0]):
@@ -93,14 +94,13 @@
     return pl.pallas_call(
         opening_body,
         out_shape=(
-            pltpu.VMEM((2, slots + rows * width // 256, 128), BF16),
-            pltpu.VMEM((2, slots + rows * width // 256, 128), BF16),
+            pltpu.VMEM((4, slots + rows * width // 512, 128), BF16),
             pltpu.VMEM((members, rows, w.shape[1]), BF16),
             jax.ShapeDtypeStruct((1, w.shape[1]), BF16),
             jax.ShapeDtypeStruct((1, width), BF16),
         ),
         in_specs=[HBM] * 6,
-        out_specs=tuple(vmem(5)),
+        out_specs=tuple(vmem(4)),
         scratch_shapes=[
             pltpu.VMEM((2, 2 * slots, 128), BF16),
             pltpu.VMEM((rows, width), BF16),
@@ -179,29 +179,27 @@
 
 def fresh_body(*refs):
     row_dec, w_key, w_value = refs[:3]
-    sources = refs[3:9]
-    k_out, v_out, k_dec, v_dec, xs, normed, sems = refs[9:]
-    rows = k_out.shape[0] // 4
+    pools = refs[3:7]
+    k_out, v_out, k_dec, v_dec, xs, normed, sems = refs[7:]
+    total = k_out.shape[0]
+    rows = total // 4
     tiles = row_dec.shape[1] // 128
-    slots = sources[0].shape[1] - rows * tiles // 2
-    copies = fetch([(s.at[:, slots:], xs.at[i]) for i, s in enumerate(sources)], sems)
-    normed[6 * rows :] = jnp.broadcast_to(row_dec[...], (16, row_dec.shape[1]))
-    for index in range(6):
+    slots = pools[0].shape[1] - rows * tiles // 4
+    copies = fetch([(s.at[:, slots:], xs.at[i]) for i, s in enumerate(pools)], sems)
+    normed[total:] = jnp.broadcast_to(row_dec[...], (16, row_dec.shape[1]))
+    for index in range(4):
         copies[index].wait()
         for tile in range(tiles):
             normed[index * rows : (index + 1) * rows, tile * 128 : (tile + 1) * 128] = xs[
-                index, tile % 2, rows * (tile // 2) : rows * (tile // 2 + 1), :
+                index, tile % 4, rows * (tile // 4) : rows * (tile // 4 + 1), :
             ]
     for w, out, out_dec in ((w_key, k_out, k_dec), (w_value, v_out, v_dec)):
         result = nn_dot(normed[...], w[...]).astype(BF16)
-        out[:, :128] = result[: 4 * rows, :128]
-        out[: 2 * rows, 128:] = result[: 2 * rows, 128:]
-        out[2 * rows :, 128:] = result[4 * rows : 6 * rows, 128:]
-        out_dec[...] = result[6 * rows : 6 * rows + 1]
-
-
-def fresh(row_dec, w_key, w_value, pools0, pools1, rows):
-    sources = [*pools0, *pools1[2:]]
+        out[...] = result[:total]
+        out_dec[...] = result[total : total + 1]
+
+
+def fresh(row_dec, w_key, w_value, pools, rows):
     width = row_dec.shape[1]
     return pl.pallas_call(
         fresh_body,
@@ -211,88 +209,119 @@
             jax.ShapeDtypeStruct((1, 256), BF16),
             jax.ShapeDtypeStruct((1, 256), BF16),
         ),
-        in_specs=vmem(3) + [HBM] * 6,
+        in_specs=vmem(3) + [HBM] * 4,
         out_specs=tuple(vmem(4)),
         scratch_shapes=[
-            pltpu.VMEM((6, 2, rows * width // 256, 128), BF16),
-            pltpu.VMEM((6 * rows + 16, width), BF16),
-            pltpu.SemaphoreType.DMA((6,)),
+            pltpu.VMEM((4, 4, rows * width // 512, 128), BF16),
+            pltpu.VMEM((4 * rows + 16, width), BF16),
+            pltpu.SemaphoreType.DMA((4,)),
         ],
         compiler_params=pltpu.CompilerParams(vmem_limit_bytes=FRE * MIB),
         cost_estimate=pl.CostEstimate(flops=10**9, bytes_accessed=2 * MIB, transcendentals=0),
         name="fresh",
-    )(row_dec, w_key, w_value, *sources)
+    )(row_dec, w_key, w_value, *pools)
 
 
 def attend_body(slots, *refs):
     ids, queries = refs[:2]
-    sources = refs[2:10]
-    k_new, v_new, out, pool, sems = refs[10:]
-    copies = fetch([(s.at[:, :slots], pool.at[i]) for i, s in enumerate(sources)], sems)
+    sources = refs[2:6]
+    k_new, v_new, out, pool, sems = refs[6:]
+    copies = fetch(
+        [
+            (source.at[2 * head : 2 * head + 2, :slots], pool.at[i, 2 * head : 2 * head + 2])
+            for head in range(2)
+            for i, source in enumerate(sources)
+        ],
+        sems,
+    )
     rows = queries.shape[0]
     fresh_rows = k_new.shape[0]
     each = fresh_rows // 4
     scale = 0.125 * math.log2(math.e)
+    block = min(128, rows)
     me = ids[0]
+    core = lax.rem(me, 2)
     chip = lax.rem(lax.div(me, 2), 4)
     beyond = lax.rem(chip + 2 * lax.rem(chip, 2) + 3, 4)
-    partners = (jnp.bitwise_xor(me, 2), me + 2 * (beyond - chip))
-    key_lane = lane_iota((rows, fresh_rows))
-    row = lax.broadcasted_iota(jnp.int32, (rows, fresh_rows), 0)
-    row_pos = each * (4 * (row // each) + lax.rem(me, 4)) + row % each
-    lane = lane_iota((rows, 128))
-    stats = jnp.zeros((rows, 128), F32)
-    for head in range(2):
-        partner = partners[head]
-        slot = key_lane // each
-        owner = jnp.bitwise_xor(jnp.where(slot < 2, me, partner), slot % 2)
-        allowed = each * owner + key_lane % each <= row_pos
+    first = jnp.bitwise_xor(me - core, 2)
+    second = me - core + 1 + 2 * (beyond - chip)
+    key_lane = lane_iota((block, fresh_rows))
+    slot = key_lane // each
+    owner = jnp.where(
+        slot < 2,
+        jnp.bitwise_xor(me, slot % 2),
+        jnp.where(jnp.bitwise_xor(core, slot % 2) == 0, first, second),
+    )
+    key_pos = each * owner + key_lane % each
+    row = lax.broadcasted_iota(jnp.int32, (block, fresh_rows), 0)
+    lane = lane_iota((block, 128))
+
+    def score(task):
+        head, which, start = task
+        if which == 0 and start == 0:
+            for copy in copies[4 * head : 4 * head + 4]:
+                copy.wait()
         cols = slice(head * 128, (head + 1) * 128)
-        q = queries[:, cols].astype(F32)
-        places = range(4 * head, 4 * head + 4)
-        for i in places:
-            copies[i].wait()
-        for which in range(2):
-            combo = 2 * head + which
-            kept = (lane < 64) if which == 0 else (lane >= 64)
-            masked = jnp.where(kept, q, 0.0).astype(BF16)
-            scores = [nt_dot(masked, pool[i, 0]) for i in places]
-            last = jnp.where(allowed, nt_dot(masked, k_new[:, cols]), NEG)
-            row_max = jnp.max(last, axis=-1, keepdims=True)
-            for s in scores:
-                row_max = jnp.maximum(row_max, jnp.max(s, axis=-1, keepdims=True))
-            weights = jnp.exp2((last - row_max) * scale)
-            total = jnp.sum(weights, axis=-1, keepdims=True)
-            mixed = nn_dot(weights.astype(BF16), v_new[:, cols])
-            for s, i in zip(scores, places):
-                weights = jnp.exp2((s - row_max) * scale)
-                total = total + jnp.sum(weights, axis=-1, keepdims=True)
-                mixed = mixed + nn_dot(weights.astype(BF16), pool[i, 1])
-            mixed = mixed / total
-            out[:, combo * each : (combo + 1) * each, :] = mixed.astype(BF16).reshape(
-                rows // each, each, 128
-            )
-            for base, stat in ((0, row_max), (4, total)):
-                for part in range(3):
-                    piece = stat.astype(BF16).astype(F32)
-                    stats = jnp.where(lane % 64 == 8 * part + base + combo, piece, stats)
-                    stat = stat - piece
-    stats = stats.reshape(rows // each, 2, each // 2, 128)
-    low = lane_iota((rows // each, each // 2, 128)) < 64
-    out[:, 4 * each :, :] = jnp.where(low, stats[:, 0], stats[:, 1]).astype(BF16)
-
-
-def attend(ids, queries, pools0, pools1, slots, k_new, v_new):
+        q = queries[start : start + block, cols].astype(F32)
+        kept = (lane < 64) if which == 0 else (lane >= 64)
+        masked = jnp.where(kept, q, 0.0).astype(BF16)
+        at = row + start
+        row_pos = each * (4 * (at // each) + lax.rem(me, 4)) + at % each
+        last = jnp.where(key_pos <= row_pos, nt_dot(masked, k_new[:, cols]), NEG)
+        return [nt_dot(masked, pool[i, 2 * head]) for i in range(4)], last
+
+    stats = {start: jnp.zeros((block, 128), F32) for start in range(0, rows, block)}
+
+    def finish(task, scores, last):
+        head, which, start = task
+        combo = 2 * head + which
+        row_max = jnp.max(last, axis=-1, keepdims=True)
+        for s in scores:
+            row_max = jnp.maximum(row_max, jnp.max(s, axis=-1, keepdims=True))
+        weights = jnp.exp2((last - row_max) * scale)
+        total = jnp.sum(weights, axis=-1, keepdims=True)
+        mixed = nn_dot(weights.astype(BF16), v_new[:, head * 128 : (head + 1) * 128])
+        for i, s in enumerate(scores):
+            weights = jnp.exp2((s - row_max) * scale)
+            total = total + jnp.sum(weights, axis=-1, keepdims=True)
+            mixed = mixed + nn_dot(weights.astype(BF16), pool[i, 2 * head + 1])
+        mixed = mixed / total
+        place = slice(start // each, (start + block) // each)
+        out[place, combo * each : (combo + 1) * each, :] = mixed.astype(BF16).reshape(
+            block // each, each, 128
+        )
+        for base, stat in ((0, row_max), (4, total)):
+            for part in range(3):
+                piece = stat.astype(BF16).astype(F32)
+                at = lane % 64 == 8 * part + base + combo
+                stats[start] = jnp.where(at, piece, stats[start])
+                stat = stat - piece
+
+    tasks = [(h, w, start) for h in range(2) for w in range(2) for start in range(0, rows, block)]
+    ahead = score(tasks[0])
+    for index, task in enumerate(tasks):
+        ready = ahead
+        if index + 1 < len(tasks):
+            ahead = score(tasks[index + 1])
+        finish(task, *ready)
+    low = lane_iota((block // each, each // 2, 128)) < 64
+    for start in range(0, rows, block):
+        pair = stats[start].reshape(block // each, 2, each // 2, 128)
+        place = slice(start // each, (start + block) // each)
+        out[place, 4 * each :, :] = jnp.where(low, pair[:, 0], pair[:, 1]).astype(BF16)
+
+
+def attend(ids, queries, pools, slots, k_new, v_new):
     rows = queries.shape[0]
     keys = 4 * slots + k_new.shape[0]
     each = k_new.shape[0] // 4
     return pl.pallas_call(
         lambda *refs: attend_body(slots, *refs),
         out_shape=pltpu.HBM((rows // each, 4 * each + each // 2, 128), BF16),
-        in_specs=[pl.BlockSpec(memory_space=pltpu.SMEM)] + vmem(1) + [HBM] * 8 + vmem(2),
+        in_specs=[pl.BlockSpec(memory_space=pltpu.SMEM)] + vmem(1) + [HBM] * 4 + vmem(2),
         out_specs=vmem(1)[0],
         scratch_shapes=[
-            pltpu.VMEM((8, 2, slots, 128), BF16),
+            pltpu.VMEM((4, 4, slots, 128), BF16),
             pltpu.SemaphoreType.DMA((8,)),
         ],
         compiler_params=pltpu.CompilerParams(vmem_limit_bytes=ATT * MIB),
@@ -300,7 +329,7 @@
             flops=4 * rows * keys * 512, bytes_accessed=2 * MIB, transcendentals=4 * rows * keys
         ),
         name="attend",
-    )(ids, queries, *pools0, *pools1, k_new, v_new)
+    )(ids, queries, *pools, k_new, v_new)
 
 
 def combine_body(parts, dec_out, lambdas, head_gain, out):
@@ -403,6 +432,8 @@
 
     def across(i):
         chip = i // 2 % 4
+        if i % 2 == 0:
+            return i ^ 2
         return i + 2 * ((chip + 2 * (chip % 2) + 3) % 4 - chip)
 
     ids = me.reshape(1)
@@ -410,7 +441,7 @@
     def move(array, target):
         return lax.ppermute(array, "kv", [(i, target(i)) for i in range(kv_count)])
 
-    pool0, pool1, sent, q_dec, row_dec = opening(
+    pool, sent, q_dec, row_dec = opening(
         piece_keys.reshape(-1, 128),
         piece_values.reshape(-1, 128),
         x_piece,
@@ -419,14 +450,10 @@
         w_query,
         members,
     )
-    far0 = move(pool0, lambda i: i ^ 2)
-    far1 = move(pool1, across)
-    pools0 = [pool0, move(pool0, lambda i: i ^ 1), far0]
-    pools1 = [pool1, move(pool1, lambda i: i ^ 1), far1]
-    pools0.append(move(far0, lambda i: i ^ 1))
-    pools1.append(move(far1, lambda i: i ^ 1))
+    far = move(pool, across)
+    pools = [pool, move(pool, lambda i: i ^ 1), far, move(far, lambda i: i ^ 1)]
     got = lax.all_to_all(sent, "kv", 0, 0, tiled=True, axis_index_groups=groups)
-    k_new, v_new, k_dec, v_dec = fresh(row_dec, w_key, w_value, pools0, pools1, rows)
+    k_new, v_new, k_dec, v_dec = fresh(row_dec, w_key, w_value, pools, rows)
     dec_out = decode(
         q_dec,
         k_dec,
@@ -438,9 +465,7 @@
         head_gain,
     )
     slots = piece_keys.shape[0]
-    parts = attend(
-        ids, got.reshape(members * rows, 256), pools0, pools1, slots, k_new, v_new
-    )
+    parts = attend(ids, got.reshape(members * rows, 256), pools, slots, k_new, v_new)
     parts = lax.all_to_all(
         parts, "kv", 0, 0, tiled=True, axis_index_groups=groups
     )

time: 72.4 us -> 70.2 us (0.970)
  starting transfers between devices: 17.9 us -> 16 us
    ppermute x6 -> x3, starting transfers between devices: 4.07 us -> 2.25 us  [move(): return lax.ppermute(array, 'kv', [(i, target(i)) for i in range(kv_count)])]
    ppermute x6 -> x3, waiting for transfers between devices: 7.43 us -> 7.86 us  [move(): return lax.ppermute(array, 'kv', [(i, target(i)) for i in range(kv_count)])]
  transfers between devices with their start and end apart: 8 -> 5, of which waited for: 4 -> 3; matrix products, arithmetic and copies ran while one was open for 0% -> 0% of each run, Pallas kernels for 6% -> 6%
where the time goes in v6:
time: 70.2 us; the launch traced here: 69.8 us
  waiting for transfers between devices  27.7 us (39%)
  starting transfers between devices  16 us (23%)
  Pallas kernels  14.4 us (21%)
  blocking collectives  9.64 us (14%)
  between operations  1.44 us (2%)
    all_to_all x1, waiting for transfers between devices, layer(): lax.all_to_all(parts, 'kv', 0, 0, tiled=True, axis_index_groups=groups)  10.2 us
    all_to_all x1, starting transfers between devices, layer(): got = lax.all_to_all(sent, 'kv', 0, 0, tiled=True, axis_index_groups=groups)  10.2 us
    all_to_all x1, blocking collectives, layer(): heads = lax.all_to_all(heads, 'tp', 0, 0, tiled=True)  9.64 us
    all_to_all x1, waiting for transfers between devices, layer(): got = lax.all_to_all(sent, 'kv', 0, 0, tiled=True, axis_index_groups=groups)  9.59 us
    ppermute x3, waiting for transfers between devices, move(): return lax.ppermute(array, 'kv', [(i, target(i)) for i in range(kv_count)])  7.86 us
    pallas_call x1, Pallas kernels, attend(): pl.pallas_call(lambda *refs: attend_body(slots, *refs), out_shape=pltpu.H...  5.4 us
    all_to_all x1, starting transfers between devices, layer(): lax.all_to_all(parts, 'kv', 0, 0, tiled=True, axis_index_groups=groups)  3.55 us
    pallas_call x1, Pallas kernels, decode(): pl.pallas_call(decode_body, out_shape=pltpu.VMEM((1, 256), BF16), in_spec...  2.98 us
  transfers between devices with their start and end apart: 5, of which 3 were waited for; matrix products, arithmetic and copies ran while one was open for 0% of the time, Pallas kernels for 6%

profile of v6, /device:TPU:8, one launch (start us, length us, event | category | flops | bytes accessed | tf_op | source)
XLA Modules:
  0.0 69.8 jit_solution(11785529798430661726)
XLA Ops:
  0.6 0.0 copy-start
  0.6 0.0 copy-start.1
  0.7 2.6 %opening.1 = (bf16[4,576,128]{2,1,0:T(8,128)(2,1)S(1)}, bf16[16,16,256]{2,1,0:T(8,128)(2,1)}, bf16[1,256]{1,0:T(2,128)(2,1)}, bf16[1,2048]{1,0:T(2,128)(2,1)}) custom-call(bf16[1024,128]{1,0:T(8,128)(2,1)} %bitcast.13, bf16[1024,128]{1,0:T(8,128)(2,1)} %bitcast.14, bf16[16,2048]{1,0:T(8,128)(2,1)} %x.1, bf16[1,2048]{1,0:T(2,128)(2,1)} %x_dec.1, ...), custom_call_target="tpu_custom_call" | custom-call | flops 1000000000 | bytes 2097152 | tf_op jit(solution)/shard_map/opening/pallas_call | solution.py:94
  3.3 2.2 %collective-permute-start.1 = (bf16[4,576,128]{2,1,0:T(8,128)(2,1)S(1)}, bf16[4,576,128]{2,1,0:T(8,128)(2,1)S(1)}, u32[]{:S(2)}, u32[]{:S(2)}) collective-permute-start(bf16[4,576,128]{2,1,0:T(8,128)(2,1)S(1)} %get-tuple-element.11.refs_3_.refs_2_), channel_id=1, source_target_pairs={{0,8},{4,28},{8,0},{12,20},{16,24},{20,12},{24,16},{28,4},{32,40},... | collective-permute-start | bytes 1769480 | tf_op jit(solution)/shard_map/ppermute | solution.py:442
  5.5 0.0 collective-permute-start
  5.5 7.9 %collective-permute-done.1.refs_5_.refs_4_ = bf16[4,576,128]{2,1,0:T(8,128)(2,1)S(1)} collective-permute-done((bf16[4,576,128]{2,1,0:T(8,128)(2,1)S(1)}, bf16[4,576,128]{2,1,0:T(8,128)(2,1)S(1)}, u32[]{:S(2)}, u32[]{:S(2)}) %collective-permute-start.1) | collective-permute-done | bytes 589856 | tf_op jit(solution)/shard_map/ppermute | solution.py:442
  13.4 0.0 collective-permute-start.2
  13.4 10.2 %all-to-all-start = ((bf16[16,16,256]{2,1,0:T(8,128)(2,1)}), bf16[16,16,256]{2,1,0:T(8,128)(2,1)S(1)}, u32[]{:S(2)}, u32[]{:S(2)}) async-start(bf16[16,16,256]{2,1,0:T(8,128)(2,1)} %get-tuple-element.10), calls=%async_computation | async-start | bytes 262144 | tf_op jit(solution)/shard_map/all_to_all | solution.py:455
  23.5 0.0 copy-start.3
  23.6 0.0 collective-permute-done.refs_4_.refs_3_
  23.6 0.0 collective-permute-done.2.refs_6_.refs_5_
  23.6 0.0 copy-done
  23.6 0.0 copy-done.1
  23.6 0.6 copy-done.3
  24.2 1.4 %fresh.1 = (bf16[64,256]{1,0:T(8,128)(2,1)S(1)}, bf16[64,256]{1,0:T(8,128)(2,1)S(1)}, bf16[1,256]{1,0:T(2,128)(2,1)S(1)}, bf16[1,256]{1,0:T(2,128)(2,1)S(1)}) custom-call(bf16[1,2048]{1,0:T(2,128)(2,1)S(1)} %copy-done.3, bf16[2048,256]{1,0:T(8,128)(2,1)S(1)} %copy-done, bf16[2048,256]{1,0:T(8,128)(2,1)S(1)} %copy-done.1, ...), custom_call_target="tpu_custom_call" | custom-call | flops 1000000000 | bytes 2097152 | tf_op jit(solution)/shard_map/fresh/pallas_call | solution.py:204
  25.7 0.0 copy-start.4
  25.7 0.0 copy-start.5
  25.7 9.6 %all-to-all-done = bf16[16,16,256]{2,1,0:T(8,128)(2,1)S(1)} async-done(((bf16[16,16,256]{2,1,0:T(8,128)(2,1)}), bf16[16,16,256]{2,1,0:T(8,128)(2,1)S(1)}, u32[]{:S(2)}, u32[]{:S(2)}) %all-to-all-start) | async-done | bytes 131104 | tf_op jit(solution)/shard_map/all_to_all | solution.py:455
  35.3 0.0 copy-done.4
  35.3 0.0 copy-done.5
  35.3 5.4 %attend.1 = bf16[16,72,128]{2,1,0:T(8,128)(2,1)} custom-call(s32[1]{0:T(128)} %bitcast.refs_0_, bf16[256,256]{1,0:T(8,128)(2,1)S(1)} %bitcast.8, bf16[4,576,128]{2,1,0:T(8,128)(2,1)S(1)} %get-tuple-element.11.refs_3_.refs_2_, bf16[4,576,128]{2,1,0:T(8,128)(2,1)} %collective-permute-done.refs_4_.refs_3_, ...), custom_call_target="tpu_custom_call" | custom-call | flops 1107296256 | bytes 2097152 | tf_op jit(solution)/shard_map/attend/pallas_call | solution.py:318
  40.7 3.5 %all-to-all-start.1 = ((bf16[16,72,128]{2,1,0:T(8,128)(2,1)}), bf16[16,72,128]{2,1,0:T(8,128)(2,1)S(1)}, u32[]{:S(2)}, u32[]{:S(2)}) async-start(bf16[16,72,128]{2,1,0:T(8,128)(2,1)} %attend.1), calls=%async_computation.1 | async-start | bytes 589824 | tf_op jit(solution)/shard_map/all_to_all | solution.py:469
  44.9 0.0 copy-start.6
  44.9 0.0 copy-start.7
  44.9 0.0 copy-start.2
  44.9 3.0 %decode.1.dec_out = bf16[1,256]{1,0:T(2,128)(2,1)S(1)} custom-call(bf16[1,256]{1,0:T(2,128)(2,1)} %get-tuple-element.15.q_dec, bf16[1,256]{1,0:T(2,128)(2,1)} %copy-done.4, bf16[1,256]{1,0:T(2,128)(2,1)} %copy-done.5, bf16[4096,128]{1,0:T(8,128)(2,1)} %bitcast.11, bf16[4096,128]{1,0:T(8,128)(2,1)} %bitcast.12, s32[1]{0:T(128)S(6)} %copy.16.length, ...), custom_call_target="tpu_custom_call" | custom-call | flops 2000000000 | bytes 2097152 | tf_op jit(solution)/shard_map/decode/pallas_call | solution.py:164
  47.9 10.2 %all-to-all-done.1.parts = bf16[16,72,128]{2,1,0:T(8,128)(2,1)S(1)} async-done(((bf16[16,72,128]{2,1,0:T(8,128)(2,1)}), bf16[16,72,128]{2,1,0:T(8,128)(2,1)S(1)}, u32[]{:S(2)}, u32[]{:S(2)}) %all-to-all-start.1) | async-done | bytes 294944 | tf_op jit(solution)/shard_map/all_to_all | solution.py:469
  58.2 0.0 copy-done.6
  58.2 0.0 copy-done.7
  58.2 1.1 %combine.1 = bf16[4,24,256]{2,1,0:T(8,128)(2,1)S(1)} custom-call(bf16[16,72,128]{2,1,0:T(8,128)(2,1)S(1)} %all-to-all-done.1.parts, bf16[1,256]{1,0:T(2,128)(2,1)S(1)} %decode.1.dec_out, f32[2]{0:T(128)S(1)} %copy-done.6, f32[1,128]{1,0:T(1,128)S(1)} %bitcast.10), custom_call_target="tpu_custom_call" | custom-call | flops 100000000 | bytes 1048576 | tf_op jit(solution)/shard_map/combine/pallas_call | solution.py:373
  59.2 9.6 %all_to_all.15.heads = bf16[4,24,256]{2,1,0:T(8,128)(2,1)S(1)} all-to-all(bf16[4,24,256]{2,1,0:T(8,128)(2,1)S(1)} %combine.1), channel_id=1, replica_groups=mesh['kv'=64,'tp'=4] {'tp'}, dimensions={0} | all-to-all | bytes 98304 | tf_op jit(solution)/shard_map/all_to_all | solution.py:473
  68.9 0.0 copy-done.2
  68.9 0.9 %out_rows.1 = (bf16[16,512]{1,0:T(8,128)(2,1)}, bf16[1,512]{1,0:T(2,128)(2,1)}) custom-call(bf16[4,24,256]{2,1,0:T(8,128)(2,1)S(1)} %all_to_all.15.heads, bf16[1024,512]{1,0:T(8,128)(2,1)S(1)} %copy-done.2), custom_call_target="tpu_custom_call" | custom-call | flops 100000000 | bytes 1048576 | tf_op jit(solution)/shard_map/out_rows/pallas_call | solution.py:394
Async XLA Ops:
  0.6 23.0 %copy-start = (bf16[2048,256]{1,0:T(8,128)(2,1)S(1)}, bf16[2048,256]{1,0:T(8,128)(2,1)}, u32[]{:S(2)}) copy-start(bf16[2048,256]{1,0:T(8,128)(2,1)} %refs_1_.1) | copy-start | bytes 3145732
  0.6 23.0 %copy-start.1 = (bf16[2048,256]{1,0:T(8,128)(2,1)S(1)}, bf16[2048,256]{1,0:T(8,128)(2,1)}, u32[]{:S(2)}) copy-start(bf16[2048,256]{1,0:T(8,128)(2,1)} %refs_2_.1) | copy-start | bytes 3145732
  3.3 10.1 %collective-permute-start.1 = (bf16[4,576,128]{2,1,0:T(8,128)(2,1)S(1)}, bf16[4,576,128]{2,1,0:T(8,128)(2,1)S(1)}, u32[]{:S(2)}, u32[]{:S(2)}) collective-permute-start(bf16[4,576,128]{2,1,0:T(8,128)(2,1)S(1)} %get-tuple-element.11.refs_3_.refs_2_), channel_id=1, source_target_pairs={{0,8},{4,28},{8,0},{12,20},{16,24},{20,12},{24,16},{28,4},{32,40},... | collective-permute-start | bytes 1769480 | tf_op jit(solution)/shard_map/ppermute | solution.py:442
  5.5 18.1 %collective-permute-start = (bf16[4,576,128]{2,1,0:T(8,128)(2,1)S(1)}, bf16[4,576,128]{2,1,0:T(8,128)(2,1)}, u32[]{:S(2)}, u32[]{:S(2)}) collective-permute-start(bf16[4,576,128]{2,1,0:T(8,128)(2,1)S(1)} %get-tuple-element.11.refs_3_.refs_2_), channel_id=1, source_target_pairs={{0,4},{4,0},{8,12},{12,8},{16,20},{20,16},{24,28},{28,24},{32,36},... | collective-permute-start | bytes 1769480 | tf_op jit(solution)/shard_map/ppermute | solution.py:442
  13.4 10.2 %collective-permute-start.2 = (bf16[4,576,128]{2,1,0:T(8,128)(2,1)S(1)}, bf16[4,576,128]{2,1,0:T(8,128)(2,1)}, u32[]{:S(2)}, u32[]{:S(2)}) collective-permute-start(bf16[4,576,128]{2,1,0:T(8,128)(2,1)S(1)} %collective-permute-done.1.refs_5_.refs_4_), channel_id=1, source_target_pairs={{0,4},{4,0},{8,12},{12,8},{16,20},{20,16},{24,28},{28,24},{32,36},... | collective-permute-start | bytes 1769480 | tf_op jit(solution)/shard_map/ppermute | solution.py:442
  13.4 21.9 %all-to-all-start = ((bf16[16,16,256]{2,1,0:T(8,128)(2,1)}), bf16[16,16,256]{2,1,0:T(8,128)(2,1)S(1)}, u32[]{:S(2)}, u32[]{:S(2)}) async-start(bf16[16,16,256]{2,1,0:T(8,128)(2,1)} %get-tuple-element.10), calls=%async_computation | async-start | bytes 262144 | tf_op jit(solution)/shard_map/all_to_all | solution.py:455
  23.5 0.7 %copy-start.3 = (bf16[1,2048]{1,0:T(2,128)(2,1)S(1)}, bf16[1,2048]{1,0:T(2,128)(2,1)}, u32[]{:S(2)}) copy-start(bf16[1,2048]{1,0:T(2,128)(2,1)} %get-tuple-element.12.refs_0_) | copy-start | bytes 12292
  25.7 9.6 %copy-start.4 = (bf16[1,256]{1,0:T(2,128)(2,1)}, bf16[1,256]{1,0:T(2,128)(2,1)S(1)}, u32[]{:S(2)}) copy-start(bf16[1,256]{1,0:T(2,128)(2,1)S(1)} %get-tuple-element.16.k_dec) | copy-start | bytes 1540
  25.7 9.6 %copy-start.5 = (bf16[1,256]{1,0:T(2,128)(2,1)}, bf16[1,256]{1,0:T(2,128)(2,1)S(1)}, u32[]{:S(2)}) copy-start(bf16[1,256]{1,0:T(2,128)(2,1)S(1)} %get-tuple-element.17.v_dec) | copy-start | bytes 1540
  40.7 17.5 %all-to-all-start.1 = ((bf16[16,72,128]{2,1,0:T(8,128)(2,1)}), bf16[16,72,128]{2,1,0:T(8,128)(2,1)S(1)}, u32[]{:S(2)}, u32[]{:S(2)}) async-start(bf16[16,72,128]{2,1,0:T(8,128)(2,1)} %attend.1), calls=%async_computation.1 | async-start | bytes 589824 | tf_op jit(solution)/shard_map/all_to_all | solution.py:469
  44.9 13.3 %copy-start.6 = (f32[2]{0:T(128)S(1)}, f32[2]{0:T(128)}, u32[]{:S(2)}) copy-start(f32[2]{0:T(128)} %lambdas.3) | copy-start | bytes 28
  44.9 13.2 %copy-start.7 = (f32[128]{0:T(128)S(1)}, f32[128]{0:T(128)}, u32[]{:S(2)}) copy-start(f32[128]{0:T(128)} %param.21) | copy-start | bytes 1540
  44.9 23.9 %copy-start.2 = (bf16[1024,512]{1,0:T(8,128)(2,1)S(1)}, bf16[1024,512]{1,0:T(8,128)(2,1)}, u32[]{:S(2)}) copy-start(bf16[1024,512]{1,0:T(8,128)(2,1)} %w.3) | copy-start | bytes 3145732

commit v7 on v6

--- a/solution.py
+++ b/solution.py
@@ -241,17 +241,13 @@
     block = min(128, rows)
     me = ids[0]
     core = lax.rem(me, 2)
-    chip = lax.rem(lax.div(me, 2), 4)
-    beyond = lax.rem(chip + 2 * lax.rem(chip, 2) + 3, 4)
-    first = jnp.bitwise_xor(me - core, 2)
-    second = me - core + 1 + 2 * (beyond - chip)
+    y = lax.rem(lax.div(me, 2), 4)
+    z = lax.div(me, 8)
     key_lane = lane_iota((block, fresh_rows))
     slot = key_lane // each
-    owner = jnp.where(
-        slot < 2,
-        jnp.bitwise_xor(me, slot % 2),
-        jnp.where(jnp.bitwise_xor(core, slot % 2) == 0, first, second),
-    )
+    of = jnp.bitwise_xor(core, slot % 2)
+    z_of = jnp.where(of == 0, jnp.bitwise_xor(z, 1), lax.rem(z + 2 * lax.rem(z, 2) + 7, 8))
+    owner = of + 2 * y + 8 * jnp.where(slot < 2, z, z_of)
     key_pos = each * owner + key_lane % each
     row = lax.broadcasted_iota(jnp.int32, (block, fresh_rows), 0)
     lane = lane_iota((block, 128))
@@ -266,7 +262,9 @@
         kept = (lane < 64) if which == 0 else (lane >= 64)
         masked = jnp.where(kept, q, 0.0).astype(BF16)
         at = row + start
-        row_pos = each * (4 * (at // each) + lax.rem(me, 4)) + at % each
+        member = at // each
+        place = 8 * (2 * (member // 4) + lax.rem(z, 2)) + 2 * (member % 4) + core
+        row_pos = each * place + at % each
         last = jnp.where(key_pos <= row_pos, nt_dot(masked, k_new[:, cols]), NEG)
         return [nt_dot(masked, pool[i, 2 * head]) for i in range(4)], last
 
@@ -425,16 +423,19 @@
     tp_count = lax.axis_size("tp")
     members = kv_count // SHARE
     rows = x_piece.shape[0]
-    groups = [[SHARE * m + e for m in range(members)] for e in range(SHARE)]
+    groups = [
+        [z * 8 + y * 2 + core for z in range(parity, 8, 2) for y in range(4)]
+        for parity in range(2)
+        for core in range(2)
+    ]
     gain = norm_gain.reshape(1, -1)
     head_gain = head_gain.reshape(1, -1)
     me = lax.axis_index("kv")
 
     def across(i):
-        chip = i // 2 % 4
-        if i % 2 == 0:
-            return i ^ 2
-        return i + 2 * ((chip + 2 * (chip % 2) + 3) % 4 - chip)
+        z, y, core = i // 8, i // 2 % 4, i % 2
+        z = z ^ 1 if core == 0 else (z + 2 * (z % 2) + 7) % 8
+        return z * 8 + y * 2 + core
 
     ids = me.reshape(1)
 

time: 70.2 us -> 68.4 us (0.974)
  the two profiles are of different devices: /device:TPU:8 before, /device:TPU:32 now
where the time goes in v7:
time: 68.4 us; the launch traced here: 68 us
  waiting for transfers between devices  26.1 us (38%)
  starting transfers between devices  15.8 us (23%)
  Pallas kernels  14.3 us (21%)
  blocking collectives  9.64 us (14%)
  between operations  1.44 us (2%)
    all_to_all x1, starting transfers between devices, layer(): got = lax.all_to_all(sent, 'kv', 0, 0, tiled=True, axis_index_groups=groups)  10.3 us
    all_to_all x1, blocking collectives, layer(): heads = lax.all_to_all(heads, 'tp', 0, 0, tiled=True)  9.64 us
    all_to_all x1, waiting for transfers between devices, layer(): lax.all_to_all(parts, 'kv', 0, 0, tiled=True, axis_index_groups=groups)  9.22 us
    all_to_all x1, waiting for transfers between devices, layer(): got = lax.all_to_all(sent, 'kv', 0, 0, tiled=True, axis_index_groups=groups)  8.82 us
    ppermute x3, waiting for transfers between devices, move(): return lax.ppermute(array, 'kv', [(i, target(i)) for i in range(kv_count)])  8.07 us
    pallas_call x1, Pallas kernels, attend(): pl.pallas_call(lambda *refs: attend_body(slots, *refs), out_shape=pltpu.H...  5.39 us
    all_to_all x1, starting transfers between devices, layer(): lax.all_to_all(parts, 'kv', 0, 0, tiled=True, axis_index_groups=groups)  3.55 us
    pallas_call x1, Pallas kernels, decode(): pl.pallas_call(decode_body, out_shape=pltpu.VMEM((1, 256), BF16), in_spec...  2.98 us
  transfers between devices with their start and end apart: 5, of which 3 were waited for; matrix products, arithmetic and copies ran while one was open for 0% of the time, Pallas kernels for 6%

profile of v7, /device:TPU:32, one launch (start us, length us, event | category | flops | bytes accessed | tf_op | source)
XLA Modules:
  0.0 68.0 jit_solution(14411609323345450263)
XLA Ops:
  0.6 0.0 copy-start
  0.6 0.0 copy-start.1
  0.7 2.6 %opening.1 = (bf16[4,576,128]{2,1,0:T(8,128)(2,1)S(1)}, bf16[16,16,256]{2,1,0:T(8,128)(2,1)}, bf16[1,256]{1,0:T(2,128)(2,1)}, bf16[1,2048]{1,0:T(2,128)(2,1)}) custom-call(bf16[1024,128]{1,0:T(8,128)(2,1)} %bitcast.13, bf16[1024,128]{1,0:T(8,128)(2,1)} %bitcast.14, bf16[16,2048]{1,0:T(8,128)(2,1)} %x.1, bf16[1,2048]{1,0:T(2,128)(2,1)} %x_dec.1, ...), custom_call_target="tpu_custom_call" | custom-call | flops 1000000000 | bytes 2097152 | tf_op jit(solution)/shard_map/opening/pallas_call | solution.py:94
  3.3 1.9 %collective-permute-start.1 = (bf16[4,576,128]{2,1,0:T(8,128)(2,1)S(1)}, bf16[4,576,128]{2,1,0:T(8,128)(2,1)S(1)}, u32[]{:S(2)}, u32[]{:S(2)}) collective-permute-start(bf16[4,576,128]{2,1,0:T(8,128)(2,1)S(1)} %get-tuple-element.11.refs_3_.refs_2_), channel_id=1, source_target_pairs={{0,32},{4,228},{8,40},{12,236},{16,48},{20,244},{24,56},{28,252},{... | collective-permute-start | bytes 1769480 | tf_op jit(solution)/shard_map/ppermute | solution.py:443
  5.2 0.0 collective-permute-start
  5.2 8.1 %collective-permute-done.1.refs_5_.refs_4_ = bf16[4,576,128]{2,1,0:T(8,128)(2,1)S(1)} collective-permute-done((bf16[4,576,128]{2,1,0:T(8,128)(2,1)S(1)}, bf16[4,576,128]{2,1,0:T(8,128)(2,1)S(1)}, u32[]{:S(2)}, u32[]{:S(2)}) %collective-permute-start.1) | collective-permute-done | bytes 589856 | tf_op jit(solution)/shard_map/ppermute | solution.py:443
  13.2 0.0 collective-permute-start.2
  13.2 10.3 %all-to-all-start = ((bf16[16,16,256]{2,1,0:T(8,128)(2,1)}), bf16[16,16,256]{2,1,0:T(8,128)(2,1)S(1)}, u32[]{:S(2)}, u32[]{:S(2)}) async-start(bf16[16,16,256]{2,1,0:T(8,128)(2,1)} %get-tuple-element.10), calls=%async_computation | async-start | bytes 262144 | tf_op jit(solution)/shard_map/all_to_all | solution.py:456
  23.5 0.0 copy-start.3
  23.6 0.0 collective-permute-done.refs_4_.refs_3_
  23.6 0.0 collective-permute-done.2.refs_6_.refs_5_
  23.6 0.0 copy-done
  23.6 0.0 copy-done.1
  23.6 0.6 copy-done.3
  24.2 1.4 %fresh.1 = (bf16[64,256]{1,0:T(8,128)(2,1)S(1)}, bf16[64,256]{1,0:T(8,128)(2,1)S(1)}, bf16[1,256]{1,0:T(2,128)(2,1)S(1)}, bf16[1,256]{1,0:T(2,128)(2,1)S(1)}) custom-call(bf16[1,2048]{1,0:T(2,128)(2,1)S(1)} %copy-done.3, bf16[2048,256]{1,0:T(8,128)(2,1)S(1)} %copy-done, bf16[2048,256]{1,0:T(8,128)(2,1)S(1)} %copy-done.1, ...), custom_call_target="tpu_custom_call" | custom-call | flops 1000000000 | bytes 2097152 | tf_op jit(solution)/shard_map/fresh/pallas_call | solution.py:204
  25.7 0.0 copy-start.4
  25.7 0.0 copy-start.5
  25.7 8.8 %all-to-all-done = bf16[16,16,256]{2,1,0:T(8,128)(2,1)S(1)} async-done(((bf16[16,16,256]{2,1,0:T(8,128)(2,1)}), bf16[16,16,256]{2,1,0:T(8,128)(2,1)S(1)}, u32[]{:S(2)}, u32[]{:S(2)}) %all-to-all-start) | async-done | bytes 131104 | tf_op jit(solution)/shard_map/all_to_all | solution.py:456
  34.5 0.0 copy-done.4
  34.5 0.0 copy-done.5
  34.5 5.4 %attend.1 = bf16[16,72,128]{2,1,0:T(8,128)(2,1)} custom-call(s32[1]{0:T(128)} %bitcast.refs_0_, bf16[256,256]{1,0:T(8,128)(2,1)S(1)} %bitcast.8, bf16[4,576,128]{2,1,0:T(8,128)(2,1)S(1)} %get-tuple-element.11.refs_3_.refs_2_, bf16[4,576,128]{2,1,0:T(8,128)(2,1)} %collective-permute-done.refs_4_.refs_3_, ...), custom_call_target="tpu_custom_call" | custom-call | flops 1107296256 | bytes 2097152 | tf_op jit(solution)/shard_map/attend/pallas_call | solution.py:316
  39.9 3.5 %all-to-all-start.1 = ((bf16[16,72,128]{2,1,0:T(8,128)(2,1)}), bf16[16,72,128]{2,1,0:T(8,128)(2,1)S(1)}, u32[]{:S(2)}, u32[]{:S(2)}) async-start(bf16[16,72,128]{2,1,0:T(8,128)(2,1)} %attend.1), calls=%async_computation.1 | async-start | bytes 589824 | tf_op jit(solution)/shard_map/all_to_all | solution.py:470
  44.1 0.0 copy-start.6
  44.1 0.0 copy-start.7
  44.1 0.0 copy-start.2
  44.2 3.0 %decode.1.dec_out = bf16[1,256]{1,0:T(2,128)(2,1)S(1)} custom-call(bf16[1,256]{1,0:T(2,128)(2,1)} %get-tuple-element.15.q_dec, bf16[1,256]{1,0:T(2,128)(2,1)} %copy-done.4, bf16[1,256]{1,0:T(2,128)(2,1)} %copy-done.5, bf16[4096,128]{1,0:T(8,128)(2,1)} %bitcast.11, bf16[4096,128]{1,0:T(8,128)(2,1)} %bitcast.12, s32[1]{0:T(128)S(6)} %copy.16.length, ...), custom_call_target="tpu_custom_call" | custom-call | flops 2000000000 | bytes 2097152 | tf_op jit(solution)/shard_map/decode/pallas_call | solution.py:164
  47.1 9.2 %all-to-all-done.1.parts = bf16[16,72,128]{2,1,0:T(8,128)(2,1)S(1)} async-done(((bf16[16,72,128]{2,1,0:T(8,128)(2,1)}), bf16[16,72,128]{2,1,0:T(8,128)(2,1)S(1)}, u32[]{:S(2)}, u32[]{:S(2)}) %all-to-all-start.1) | async-done | bytes 294944 | tf_op jit(solution)/shard_map/all_to_all | solution.py:470
  56.4 0.0 copy-done.6
  56.4 0.0 copy-done.7
  56.4 1.1 %combine.1 = bf16[4,24,256]{2,1,0:T(8,128)(2,1)S(1)} custom-call(bf16[16,72,128]{2,1,0:T(8,128)(2,1)S(1)} %all-to-all-done.1.parts, bf16[1,256]{1,0:T(2,128)(2,1)S(1)} %decode.1.dec_out, f32[2]{0:T(128)S(1)} %copy-done.6, f32[1,128]{1,0:T(1,128)S(1)} %bitcast.10), custom_call_target="tpu_custom_call" | custom-call | flops 100000000 | bytes 1048576 | tf_op jit(solution)/shard_map/combine/pallas_call | solution.py:371
  57.4 9.6 %all_to_all.15.heads = bf16[4,24,256]{2,1,0:T(8,128)(2,1)S(1)} all-to-all(bf16[4,24,256]{2,1,0:T(8,128)(2,1)S(1)} %combine.1), channel_id=1, replica_groups=mesh['kv'=64,'tp'=4] {'tp'}, dimensions={0} | all-to-all | bytes 98304 | tf_op jit(solution)/shard_map/all_to_all | solution.py:474
  67.1 0.0 copy-done.2
  67.1 0.9 %out_rows.1 = (bf16[16,512]{1,0:T(8,128)(2,1)}, bf16[1,512]{1,0:T(2,128)(2,1)}) custom-call(bf16[4,24,256]{2,1,0:T(8,128)(2,1)S(1)} %all_to_all.15.heads, bf16[1024,512]{1,0:T(8,128)(2,1)S(1)} %copy-done.2), custom_call_target="tpu_custom_call" | custom-call | flops 100000000 | bytes 1048576 | tf_op jit(solution)/shard_map/out_rows/pallas_call | solution.py:392
Async XLA Ops:
  0.6 23.0 %copy-start = (bf16[2048,256]{1,0:T(8,128)(2,1)S(1)}, bf16[2048,256]{1,0:T(8,128)(2,1)}, u32[]{:S(2)}) copy-start(bf16[2048,256]{1,0:T(8,128)(2,1)} %refs_1_.1) | copy-start | bytes 3145732
  0.6 23.0 %copy-start.1 = (bf16[2048,256]{1,0:T(8,128)(2,1)S(1)}, bf16[2048,256]{1,0:T(8,128)(2,1)}, u32[]{:S(2)}) copy-start(bf16[2048,256]{1,0:T(8,128)(2,1)} %refs_2_.1) | copy-start | bytes 3145732
  3.3 10.0 %collective-permute-start.1 = (bf16[4,576,128]{2,1,0:T(8,128)(2,1)S(1)}, bf16[4,576,128]{2,1,0:T(8,128)(2,1)S(1)}, u32[]{:S(2)}, u32[]{:S(2)}) collective-permute-start(bf16[4,576,128]{2,1,0:T(8,128)(2,1)S(1)} %get-tuple-element.11.refs_3_.refs_2_), channel_id=1, source_target_pairs={{0,32},{4,228},{8,40},{12,236},{16,48},{20,244},{24,56},{28,252},{... | collective-permute-start | bytes 1769480 | tf_op jit(solution)/shard_map/ppermute | solution.py:443
  5.2 18.4 %collective-permute-start = (bf16[4,576,128]{2,1,0:T(8,128)(2,1)S(1)}, bf16[4,576,128]{2,1,0:T(8,128)(2,1)}, u32[]{:S(2)}, u32[]{:S(2)}) collective-permute-start(bf16[4,576,128]{2,1,0:T(8,128)(2,1)S(1)} %get-tuple-element.11.refs_3_.refs_2_), channel_id=1, source_target_pairs={{0,4},{4,0},{8,12},{12,8},{16,20},{20,16},{24,28},{28,24},{32,36},... | collective-permute-start | bytes 1769480 | tf_op jit(solution)/shard_map/ppermute | solution.py:443
  13.2 10.3 %collective-permute-start.2 = (bf16[4,576,128]{2,1,0:T(8,128)(2,1)S(1)}, bf16[4,576,128]{2,1,0:T(8,128)(2,1)}, u32[]{:S(2)}, u32[]{:S(2)}) collective-permute-start(bf16[4,576,128]{2,1,0:T(8,128)(2,1)S(1)} %collective-permute-done.1.refs_5_.refs_4_), channel_id=1, source_target_pairs={{0,4},{4,0},{8,12},{12,8},{16,20},{20,16},{24,28},{28,24},{32,36},... | collective-permute-start | bytes 1769480 | tf_op jit(solution)/shard_map/ppermute | solution.py:443
  13.2 21.3 %all-to-all-start = ((bf16[16,16,256]{2,1,0:T(8,128)(2,1)}), bf16[16,16,256]{2,1,0:T(8,128)(2,1)S(1)}, u32[]{:S(2)}, u32[]{:S(2)}) async-start(bf16[16,16,256]{2,1,0:T(8,128)(2,1)} %get-tuple-element.10), calls=%async_computation | async-start | bytes 262144 | tf_op jit(solution)/shard_map/all_to_all | solution.py:456
  23.5 0.7 %copy-start.3 = (bf16[1,2048]{1,0:T(2,128)(2,1)S(1)}, bf16[1,2048]{1,0:T(2,128)(2,1)}, u32[]{:S(2)}) copy-start(bf16[1,2048]{1,0:T(2,128)(2,1)} %get-tuple-element.12.refs_0_) | copy-start | bytes 12292
  25.7 8.8 %copy-start.4 = (bf16[1,256]{1,0:T(2,128)(2,1)}, bf16[1,256]{1,0:T(2,128)(2,1)S(1)}, u32[]{:S(2)}) copy-start(bf16[1,256]{1,0:T(2,128)(2,1)S(1)} %get-tuple-element.16.k_dec) | copy-start | bytes 1540
  25.7 8.8 %copy-start.5 = (bf16[1,256]{1,0:T(2,128)(2,1)}, bf16[1,256]{1,0:T(2,128)(2,1)S(1)}, u32[]{:S(2)}) copy-start(bf16[1,256]{1,0:T(2,128)(2,1)S(1)} %get-tuple-element.17.v_dec) | copy-start | bytes 1540
  39.9 16.5 %all-to-all-start.1 = ((bf16[16,72,128]{2,1,0:T(8,128)(2,1)}), bf16[16,72,128]{2,1,0:T(8,128)(2,1)S(1)}, u32[]{:S(2)}, u32[]{:S(2)}) async-start(bf16[16,72,128]{2,1,0:T(8,128)(2,1)} %attend.1), calls=%async_computation.1 | async-start | bytes 589824 | tf_op jit(solution)/shard_map/all_to_all | solution.py:470
  44.1 12.2 %copy-start.6 = (f32[2]{0:T(128)S(1)}, f32[2]{0:T(128)}, u32[]{:S(2)}) copy-start(f32[2]{0:T(128)} %lambdas.3) | copy-start | bytes 28
  44.1 12.2 %copy-start.7 = (f32[128]{0:T(128)S(1)}, f32[128]{0:T(128)}, u32[]{:S(2)}) copy-start(f32[128]{0:T(128)} %param.21) | copy-start | bytes 1540
  44.1 22.9 %copy-start.2 = (bf16[1024,512]{1,0:T(8,128)(2,1)S(1)}, bf16[1024,512]{1,0:T(8,128)(2,1)}, u32[]{:S(2)}) copy-start(bf16[1024,512]{1,0:T(8,128)(2,1)} %w.3) | copy-start | bytes 3145732

commit v8 on v7

--- a/solution.py
+++ b/solution.py
@@ -13,7 +13,7 @@
 F32 = jnp.float32
 BF16 = jnp.bfloat16
 MIB = 1024 * 1024
-ATT, FRE, DEC, OPN = 20, 8, 60, 60
+ATT, FRE, DEC, OPN = 20, 8, 52, 60
 
 
 def nt_dot(a, b):
@@ -56,9 +56,9 @@
             (x, xs),
             (x_dec, xd),
             (gain, g),
+            (w, wq),
             (keys, kv.at[0]),
             (values, kv.at[1]),
-            (w, wq),
         ),
         sems,
     )
@@ -74,18 +74,18 @@
     for tile in range(x.shape[1] // 128):
         at = slots + rows * (tile // 4)
         pool[tile % 4, at : at + rows, :] = normed[:rows, tile * 128 : (tile + 1) * 128]
+    copies[3].wait()
+    result = nn_dot(normed[...], wq[...]).astype(BF16)
+    for member in range(out.shape[0]):
+        out[member] = result[:rows]
+    out_dec[...] = result[rows : rows + 1]
     for index in range(2):
-        copies[3 + index].wait()
+        copies[4 + index].wait()
         wide[index] = kv[index].astype(F32)
         for head in range(2):
             pool[2 * head + index, :slots] = wide[index, pl.ds(head, slots, stride=2), :].astype(
                 BF16
             )
-    copies[5].wait()
-    result = nn_dot(normed[...], wq[...]).astype(BF16)
-    for member in range(out.shape[0]):
-        out[member] = result[:rows]
-    out_dec[...] = result[rows : rows + 1]
 
 
 def opening(keys, values, x, x_dec, gain, w, members):

time: 68.4 us -> 68.4 us (level)
  local copies, waits for them, and re-layouts: 0.68 us -> 2.54 us
  waiting for transfers between devices: 26.1 us -> 25 us
  Pallas kernels: 14.3 us -> 13.5 us
    unnamed x16, local copies, waits for them, and re-layouts: 0.68 us -> 2.54 us
    all_to_all x1, waiting for transfers between devices: 9.22 us -> 8.13 us  [layer(): lax.all_to_all(parts, 'kv', 0, 0, tiled=True, axis_index_groups=groups)]
    pallas_call x1, Pallas kernels: 2.98 us -> 2.2 us  [decode(): pl.pallas_call(decode_body, out_shape=pltpu.VMEM((1, 256), BF16), in_spec...]
  transfers between devices with their start and end apart: 5 -> 5, of which waited for: 3 -> 3; matrix products, arithmetic and copies ran while one was open for 0% -> 0% of each run, Pallas kernels for 6% -> 5%
where the time goes in v8:
time: 68.4 us; the launch traced here: 67.9 us
  waiting for transfers between devices  25 us (37%)
  starting transfers between devices  15.8 us (23%)
  Pallas kernels  13.5 us (20%)
  blocking collectives  9.64 us (14%)
  local copies, waits for them, and re-layouts  2.54 us (4%)
  between operations  1.43 us (2%)
    all_to_all x1, starting transfers between devices, layer(): got = lax.all_to_all(sent, 'kv', 0, 0, tiled=True, axis_index_groups=groups)  10.3 us
    all_to_all x1, blocking collectives, layer(): heads = lax.all_to_all(heads, 'tp', 0, 0, tiled=True)  9.64 us
    all_to_all x1, waiting for transfers between devices, layer(): got = lax.all_to_all(sent, 'kv', 0, 0, tiled=True, axis_index_groups=groups)  8.84 us
    all_to_all x1, waiting for transfers between devices, layer(): lax.all_to_all(parts, 'kv', 0, 0, tiled=True, axis_index_groups=groups)  8.13 us
    ppermute x3, waiting for transfers between devices, move(): return lax.ppermute(array, 'kv', [(i, target(i)) for i in range(kv_count)])  8.07 us
    pallas_call x1, Pallas kernels, attend(): pl.pallas_call(lambda *refs: attend_body(slots, *refs), out_shape=pltpu.H...  5.41 us
    all_to_all x1, starting transfers between devices, layer(): lax.all_to_all(parts, 'kv', 0, 0, tiled=True, axis_index_groups=groups)  3.55 us
    unnamed x16, local copies, waits for them, and re-layouts  2.54 us
  transfers between devices with their start and end apart: 5, of which 3 were waited for; matrix products, arithmetic and copies ran while one was open for 0% of the time, Pallas kernels for 5%

profile of v8, /device:TPU:32, one launch (start us, length us, event | category | flops | bytes accessed | tf_op | source)
XLA Modules:
  0.0 67.9 jit_solution(7514899652341950843)
XLA Ops:
  0.6 0.0 copy-start
  0.6 0.0 copy-start.1
  0.7 2.5 %opening.1 = (bf16[4,576,128]{2,1,0:T(8,128)(2,1)S(1)}, bf16[16,16,256]{2,1,0:T(8,128)(2,1)}, bf16[1,256]{1,0:T(2,128)(2,1)}, bf16[1,2048]{1,0:T(2,128)(2,1)}) custom-call(bf16[1024,128]{1,0:T(8,128)(2,1)} %bitcast.13, bf16[1024,128]{1,0:T(8,128)(2,1)} %bitcast.14, bf16[16,2048]{1,0:T(8,128)(2,1)} %x.1, bf16[1,2048]{1,0:T(2,128)(2,1)} %x_dec.1, ...), custom_call_target="tpu_custom_call" | custom-call | flops 1000000000 | bytes 2097152 | tf_op jit(solution)/shard_map/opening/pallas_call | solution.py:94
  3.2 1.9 %collective-permute-start.1 = (bf16[4,576,128]{2,1,0:T(8,128)(2,1)S(1)}, bf16[4,576,128]{2,1,0:T(8,128)(2,1)S(1)}, u32[]{:S(2)}, u32[]{:S(2)}) collective-permute-start(bf16[4,576,128]{2,1,0:T(8,128)(2,1)S(1)} %get-tuple-element.11.refs_3_.refs_2_), channel_id=1, source_target_pairs={{0,32},{4,228},{8,40},{12,236},{16,48},{20,244},{24,56},{28,252},{... | collective-permute-start | bytes 1769480 | tf_op jit(solution)/shard_map/ppermute | solution.py:443
  5.1 0.0 collective-permute-start
  5.1 8.1 %collective-permute-done.1.refs_5_.refs_4_ = bf16[4,576,128]{2,1,0:T(8,128)(2,1)S(1)} collective-permute-done((bf16[4,576,128]{2,1,0:T(8,128)(2,1)S(1)}, bf16[4,576,128]{2,1,0:T(8,128)(2,1)S(1)}, u32[]{:S(2)}, u32[]{:S(2)}) %collective-permute-start.1) | collective-permute-done | bytes 589856 | tf_op jit(solution)/shard_map/ppermute | solution.py:443
  13.2 0.0 collective-permute-start.2
  13.2 10.3 %all-to-all-start = ((bf16[16,16,256]{2,1,0:T(8,128)(2,1)}), bf16[16,16,256]{2,1,0:T(8,128)(2,1)S(1)}, u32[]{:S(2)}, u32[]{:S(2)}) async-start(bf16[16,16,256]{2,1,0:T(8,128)(2,1)} %get-tuple-element.10), calls=%async_computation | async-start | bytes 262144 | tf_op jit(solution)/shard_map/all_to_all | solution.py:456
  23.5 0.0 copy-start.3
  23.5 0.0 collective-permute-done.refs_4_.refs_3_
  23.5 0.0 collective-permute-done.2.refs_6_.refs_5_
  23.5 0.0 copy-done
  23.5 0.0 copy-done.1
  23.5 0.6 copy-done.3
  24.2 1.4 %fresh.1 = (bf16[64,256]{1,0:T(8,128)(2,1)S(1)}, bf16[64,256]{1,0:T(8,128)(2,1)S(1)}, bf16[1,256]{1,0:T(2,128)(2,1)S(1)}, bf16[1,256]{1,0:T(2,128)(2,1)S(1)}) custom-call(bf16[1,2048]{1,0:T(2,128)(2,1)S(1)} %copy-done.3, bf16[2048,256]{1,0:T(8,128)(2,1)S(1)} %copy-done, bf16[2048,256]{1,0:T(8,128)(2,1)S(1)} %copy-done.1, ...), custom_call_target="tpu_custom_call" | custom-call | flops 1000000000 | bytes 2097152 | tf_op jit(solution)/shard_map/fresh/pallas_call | solution.py:204
  25.6 8.8 %all-to-all-done = bf16[16,16,256]{2,1,0:T(8,128)(2,1)S(1)} async-done(((bf16[16,16,256]{2,1,0:T(8,128)(2,1)}), bf16[16,16,256]{2,1,0:T(8,128)(2,1)S(1)}, u32[]{:S(2)}, u32[]{:S(2)}) %all-to-all-start) | async-done | bytes 131104 | tf_op jit(solution)/shard_map/all_to_all | solution.py:456
  34.4 5.4 %attend.1 = bf16[16,72,128]{2,1,0:T(8,128)(2,1)} custom-call(s32[1]{0:T(128)} %bitcast.refs_0_, bf16[256,256]{1,0:T(8,128)(2,1)S(1)} %bitcast.8, bf16[4,576,128]{2,1,0:T(8,128)(2,1)S(1)} %get-tuple-element.11.refs_3_.refs_2_, bf16[4,576,128]{2,1,0:T(8,128)(2,1)} %collective-permute-done.refs_4_.refs_3_, ...), custom_call_target="tpu_custom_call" | custom-call | flops 1107296256 | bytes 2097152 | tf_op jit(solution)/shard_map/attend/pallas_call | solution.py:316
  39.8 0.0 copy-start.7
  39.9 3.5 %all-to-all-start.1 = ((bf16[16,72,128]{2,1,0:T(8,128)(2,1)}), bf16[16,72,128]{2,1,0:T(8,128)(2,1)S(1)}, u32[]{:S(2)}, u32[]{:S(2)}) async-start(bf16[16,72,128]{2,1,0:T(8,128)(2,1)} %attend.1), calls=%async_computation.1 | async-start | bytes 589824 | tf_op jit(solution)/shard_map/all_to_all | solution.py:470
  44.1 0.0 copy-start.5
  44.1 0.0 copy-start.6
  44.1 0.0 copy-done.7
  44.1 0.6 copy-done.5
  44.7 0.0 copy-done.6
  44.7 0.0 copy-start.4
  44.7 1.2 %copy-done.4 = bf16[1,2048,2,128]{3,2,1,0:T(2,128)(2,1)S(1)} copy-done((bf16[1,2048,2,128]{3,2,1,0:T(2,128)(2,1)S(1)}, bf16[1,2048,2,128]{3,2,1,0:T(2,128)(2,1)}, u32[]{:S(2)}) %copy-start.4) | copy-done | bytes 1048600
  46.0 0.0 copy-start.2
  46.0 2.2 %decode.1.dec_out = bf16[1,256]{1,0:T(2,128)(2,1)S(1)} custom-call(bf16[1,256]{1,0:T(2,128)(2,1)S(1)} %copy-done.7, bf16[1,256]{1,0:T(2,128)(2,1)S(1)} %get-tuple-element.16.k_dec, bf16[1,256]{1,0:T(2,128)(2,1)S(1)} %get-tuple-element.17.v_dec, bf16[4096,128]{1,0:T(8,128)(2,1)S(1)} %bitcast.9, bf16[4096,128]{1,0:T(8,128)(2,1)} %bitcast.12, ...), custom_call_target="tpu_custom_call" | custom-call | flops 2000000000 | bytes 2097152 | tf_op jit(solution)/shard_map/decode/pallas_call | solution.py:164
  48.2 8.1 %all-to-all-done.1.parts = bf16[16,72,128]{2,1,0:T(8,128)(2,1)S(1)} async-done(((bf16[16,72,128]{2,1,0:T(8,128)(2,1)}), bf16[16,72,128]{2,1,0:T(8,128)(2,1)S(1)}, u32[]{:S(2)}, u32[]{:S(2)}) %all-to-all-start.1) | async-done | bytes 294944 | tf_op jit(solution)/shard_map/all_to_all | solution.py:470
  56.3 1.1 %combine.1 = bf16[4,24,256]{2,1,0:T(8,128)(2,1)S(1)} custom-call(bf16[16,72,128]{2,1,0:T(8,128)(2,1)S(1)} %all-to-all-done.1.parts, bf16[1,256]{1,0:T(2,128)(2,1)S(1)} %decode.1.dec_out, f32[2]{0:T(128)S(1)} %copy-done.5, f32[1,128]{1,0:T(1,128)S(1)} %bitcast.11), custom_call_target="tpu_custom_call" | custom-call | flops 100000000 | bytes 1048576 | tf_op jit(solution)/shard_map/combine/pallas_call | solution.py:371
  57.4 9.6 %all_to_all.15.heads = bf16[4,24,256]{2,1,0:T(8,128)(2,1)S(1)} all-to-all(bf16[4,24,256]{2,1,0:T(8,128)(2,1)S(1)} %combine.1), channel_id=1, replica_groups=mesh['kv'=64,'tp'=4] {'tp'}, dimensions={0} | all-to-all | bytes 98304 | tf_op jit(solution)/shard_map/all_to_all | solution.py:474
  67.0 0.0 copy-done.2
  67.0 0.9 %out_rows.1 = (bf16[16,512]{1,0:T(8,128)(2,1)}, bf16[1,512]{1,0:T(2,128)(2,1)}) custom-call(bf16[4,24,256]{2,1,0:T(8,128)(2,1)S(1)} %all_to_all.15.heads, bf16[1024,512]{1,0:T(8,128)(2,1)S(1)} %copy-done.2), custom_call_target="tpu_custom_call" | custom-call | flops 100000000 | bytes 1048576 | tf_op jit(solution)/shard_map/out_rows/pallas_call | solution.py:392
Async XLA Ops:
  0.6 22.9 %copy-start = (bf16[2048,256]{1,0:T(8,128)(2,1)S(1)}, bf16[2048,256]{1,0:T(8,128)(2,1)}, u32[]{:S(2)}) copy-start(bf16[2048,256]{1,0:T(8,128)(2,1)} %refs_1_.1) | copy-start | bytes 3145732
  0.6 22.9 %copy-start.1 = (bf16[2048,256]{1,0:T(8,128)(2,1)S(1)}, bf16[2048,256]{1,0:T(8,128)(2,1)}, u32[]{:S(2)}) copy-start(bf16[2048,256]{1,0:T(8,128)(2,1)} %refs_2_.1) | copy-start | bytes 3145732
  3.2 10.0 %collective-permute-start.1 = (bf16[4,576,128]{2,1,0:T(8,128)(2,1)S(1)}, bf16[4,576,128]{2,1,0:T(8,128)(2,1)S(1)}, u32[]{:S(2)}, u32[]{:S(2)}) collective-permute-start(bf16[4,576,128]{2,1,0:T(8,128)(2,1)S(1)} %get-tuple-element.11.refs_3_.refs_2_), channel_id=1, source_target_pairs={{0,32},{4,228},{8,40},{12,236},{16,48},{20,244},{24,56},{28,252},{... | collective-permute-start | bytes 1769480 | tf_op jit(solution)/shard_map/ppermute | solution.py:443
  5.1 18.4 %collective-permute-start = (bf16[4,576,128]{2,1,0:T(8,128)(2,1)S(1)}, bf16[4,576,128]{2,1,0:T(8,128)(2,1)}, u32[]{:S(2)}, u32[]{:S(2)}) collective-permute-start(bf16[4,576,128]{2,1,0:T(8,128)(2,1)S(1)} %get-tuple-element.11.refs_3_.refs_2_), channel_id=1, source_target_pairs={{0,4},{4,0},{8,12},{12,8},{16,20},{20,16},{24,28},{28,24},{32,36},... | collective-permute-start | bytes 1769480 | tf_op jit(solution)/shard_map/ppermute | solution.py:443
  13.2 10.3 %collective-permute-start.2 = (bf16[4,576,128]{2,1,0:T(8,128)(2,1)S(1)}, bf16[4,576,128]{2,1,0:T(8,128)(2,1)}, u32[]{:S(2)}, u32[]{:S(2)}) collective-permute-start(bf16[4,576,128]{2,1,0:T(8,128)(2,1)S(1)} %collective-permute-done.1.refs_5_.refs_4_), channel_id=1, source_target_pairs={{0,4},{4,0},{8,12},{12,8},{16,20},{20,16},{24,28},{28,24},{32,36},... | collective-permute-start | bytes 1769480 | tf_op jit(solution)/shard_map/ppermute | solution.py:443
  13.2 21.3 %all-to-all-start = ((bf16[16,16,256]{2,1,0:T(8,128)(2,1)}), bf16[16,16,256]{2,1,0:T(8,128)(2,1)S(1)}, u32[]{:S(2)}, u32[]{:S(2)}) async-start(bf16[16,16,256]{2,1,0:T(8,128)(2,1)} %get-tuple-element.10), calls=%async_computation | async-start | bytes 262144 | tf_op jit(solution)/shard_map/all_to_all | solution.py:456
  23.5 0.7 %copy-start.3 = (bf16[1,2048]{1,0:T(2,128)(2,1)S(1)}, bf16[1,2048]{1,0:T(2,128)(2,1)}, u32[]{:S(2)}) copy-start(bf16[1,2048]{1,0:T(2,128)(2,1)} %get-tuple-element.12.refs_0_) | copy-start | bytes 12292
  39.8 4.2 %copy-start.7 = (bf16[1,256]{1,0:T(2,128)(2,1)S(1)}, bf16[1,256]{1,0:T(2,128)(2,1)}, u32[]{:S(2)}) copy-start(bf16[1,256]{1,0:T(2,128)(2,1)} %get-tuple-element.15.q_dec) | copy-start | bytes 1540
  39.9 16.4 %all-to-all-start.1 = ((bf16[16,72,128]{2,1,0:T(8,128)(2,1)}), bf16[16,72,128]{2,1,0:T(8,128)(2,1)S(1)}, u32[]{:S(2)}, u32[]{:S(2)}) async-start(bf16[16,72,128]{2,1,0:T(8,128)(2,1)} %attend.1), calls=%async_computation.1 | async-start | bytes 589824 | tf_op jit(solution)/shard_map/all_to_all | solution.py:470
  44.1 0.7 copy-start.5
  44.1 0.7 copy-start.6
  44.7 1.2 %copy-start.4 = (bf16[1,2048,2,128]{3,2,1,0:T(2,128)(2,1)S(1)}, bf16[1,2048,2,128]{3,2,1,0:T(2,128)(2,1)}, u32[]{:S(2)}) copy-start(bf16[1,2048,2,128]{3,2,1,0:T(2,128)(2,1)} %param.25) | copy-start | bytes 3145732
  46.0 21.1 %copy-start.2 = (bf16[1024,512]{1,0:T(8,128)(2,1)S(1)}, bf16[1024,512]{1,0:T(8,128)(2,1)}, u32[]{:S(2)}) copy-start(bf16[1024,512]{1,0:T(8,128)(2,1)} %w.3) | copy-start | bytes 3145732

commit v9 on v8

--- a/solution.py
+++ b/solution.py
@@ -47,8 +47,8 @@
 
 
 def opening_body(
-    keys, values, x, x_dec, gain, w, pool, out, out_dec, row_dec, kv, xs, xd, g, wq, wide, normed,
-    sems
+    keys, values, x, x_dec, gain, w, pool, out_hbm, out_dec, row_dec, kv, xs, xd, g, wq, wide, normed,
+    out, sems
 ):
 
     copies = fetch(
@@ -79,6 +79,8 @@
     for member in range(out.shape[0]):
         out[member] = result[:rows]
     out_dec[...] = result[rows : rows + 1]
+    sent = pltpu.make_async_copy(out, out_hbm, sems.at[6])
+    sent.start()
     for index in range(2):
         copies[4 + index].wait()
         wide[index] = kv[index].astype(F32)
@@ -86,6 +88,7 @@
             pool[2 * head + index, :slots] = wide[index, pl.ds(head, slots, stride=2), :].astype(
                 BF16
             )
+    sent.wait()
 
 
 def opening(keys, values, x, x_dec, gain, w, members):
@@ -95,12 +98,12 @@
         opening_body,
         out_shape=(
             pltpu.VMEM((4, slots + rows * width // 512, 128), BF16),
-            pltpu.VMEM((members, rows, w.shape[1]), BF16),
+            pltpu.HBM((members, rows, w.shape[1]), BF16),
             jax.ShapeDtypeStruct((1, w.shape[1]), BF16),
             jax.ShapeDtypeStruct((1, width), BF16),
         ),
         in_specs=[HBM] * 6,
-        out_specs=tuple(vmem(4)),
+        out_specs=(vmem(1)[0], HBM, *vmem(2)),
         scratch_shapes=[
             pltpu.VMEM((2, 2 * slots, 128), BF16),
             pltpu.VMEM((rows, width), BF16),
@@ -109,7 +112,8 @@
             pltpu.VMEM(w.shape, BF16),
             pltpu.VMEM((2, 2 * slots, 128), F32),
             pltpu.VMEM((rows + 16, width), BF16),
-            pltpu.SemaphoreType.DMA((6,)),
+            pltpu.VMEM((members, rows, w.shape[1]), BF16),
+            pltpu.SemaphoreType.DMA((7,)),
         ],
         compiler_params=pltpu.CompilerParams(vmem_limit_bytes=OPN * MIB),
         cost_estimate=pl.CostEstimate(flops=10**9, bytes_accessed=2 * MIB, transcendentals=0),

time: 68.4 us -> 68.9 us (level)
  no operation moved by 1% of the time
where the time goes in v9:
time: 68.9 us; the launch traced here: 68.4 us
  waiting for transfers between devices  25 us (36%)
  starting transfers between devices  15.8 us (23%)
  Pallas kernels  14 us (20%)
  blocking collectives  9.63 us (14%)
  local copies, waits for them, and re-layouts  2.54 us (4%)
  between operations  1.43 us (2%)
    all_to_all x1, starting transfers between devices, layer(): got = lax.all_to_all(sent, 'kv', 0, 0, tiled=True, axis_index_groups=groups)  10.3 us
    all_to_all x1, blocking collectives, layer(): heads = lax.all_to_all(heads, 'tp', 0, 0, tiled=True)  9.63 us
    all_to_all x1, waiting for transfers between devices, layer(): got = lax.all_to_all(sent, 'kv', 0, 0, tiled=True, axis_index_groups=groups)  8.84 us
    all_to_all x1, waiting for transfers between devices, layer(): lax.all_to_all(parts, 'kv', 0, 0, tiled=True, axis_index_groups=groups)  8.14 us
    ppermute x3, waiting for transfers between devices, move(): return lax.ppermute(array, 'kv', [(i, target(i)) for i in range(kv_count)])  8.07 us
    pallas_call x1, Pallas kernels, attend(): pl.pallas_call(lambda *refs: attend_body(slots, *refs), out_shape=pltpu.H...  5.41 us
    all_to_all x1, starting transfers between devices, layer(): lax.all_to_all(parts, 'kv', 0, 0, tiled=True, axis_index_groups=groups)  3.55 us
    pallas_call x1, Pallas kernels, opening(): pl.pallas_call(opening_body, out_shape=(pltpu.VMEM((4, slots + rows * wid...  3.06 us
  transfers between devices with their start and end apart: 5, of which 3 were waited for; matrix products, arithmetic and copies ran while one was open for 0% of the time, Pallas kernels for 5%

profile of v9, /device:TPU:32, one launch (start us, length us, event | category | flops | bytes accessed | tf_op | source)
XLA Modules:
  0.0 68.4 jit_solution(8572555923454970736)
XLA Ops:
  0.6 0.0 copy-start
  0.6 0.0 copy-start.1
  0.7 3.1 %opening.1 = (bf16[4,576,128]{2,1,0:T(8,128)(2,1)S(1)}, bf16[16,16,256]{2,1,0:T(8,128)(2,1)}, bf16[1,256]{1,0:T(2,128)(2,1)}, bf16[1,2048]{1,0:T(2,128)(2,1)}) custom-call(bf16[1024,128]{1,0:T(8,128)(2,1)} %bitcast.13, bf16[1024,128]{1,0:T(8,128)(2,1)} %bitcast.14, bf16[16,2048]{1,0:T(8,128)(2,1)} %x.1, bf16[1,2048]{1,0:T(2,128)(2,1)} %x_dec.1, ...), custom_call_target="tpu_custom_call" | custom-call | flops 1000000000 | bytes 2097152 | tf_op jit(solution)/shard_map/opening/pallas_call | solution.py:97
  3.7 1.9 %collective-permute-start.1 = (bf16[4,576,128]{2,1,0:T(8,128)(2,1)S(1)}, bf16[4,576,128]{2,1,0:T(8,128)(2,1)S(1)}, u32[]{:S(2)}, u32[]{:S(2)}) collective-permute-start(bf16[4,576,128]{2,1,0:T(8,128)(2,1)S(1)} %get-tuple-element.11.refs_3_.refs_2_), channel_id=1, source_target_pairs={{0,32},{4,228},{8,40},{12,236},{16,48},{20,244},{24,56},{28,252},{... | collective-permute-start | bytes 1769480 | tf_op jit(solution)/shard_map/ppermute | solution.py:447
  5.6 0.0 collective-permute-start
  5.6 8.1 %collective-permute-done.1.refs_5_.refs_4_ = bf16[4,576,128]{2,1,0:T(8,128)(2,1)S(1)} collective-permute-done((bf16[4,576,128]{2,1,0:T(8,128)(2,1)S(1)}, bf16[4,576,128]{2,1,0:T(8,128)(2,1)S(1)}, u32[]{:S(2)}, u32[]{:S(2)}) %collective-permute-start.1) | collective-permute-done | bytes 589856 | tf_op jit(solution)/shard_map/ppermute | solution.py:447
  13.7 0.0 collective-permute-start.2
  13.7 10.3 %all-to-all-start = ((bf16[16,16,256]{2,1,0:T(8,128)(2,1)}), bf16[16,16,256]{2,1,0:T(8,128)(2,1)S(1)}, u32[]{:S(2)}, u32[]{:S(2)}) async-start(bf16[16,16,256]{2,1,0:T(8,128)(2,1)} %get-tuple-element.10), calls=%async_computation | async-start | bytes 262144 | tf_op jit(solution)/shard_map/all_to_all | solution.py:460
  24.0 0.0 copy-start.3
  24.0 0.0 collective-permute-done.refs_4_.refs_3_
  24.0 0.0 collective-permute-done.2.refs_6_.refs_5_
  24.0 0.0 copy-done
  24.0 0.0 copy-done.1
  24.1 0.6 copy-done.3
  24.7 1.4 %fresh.1 = (bf16[64,256]{1,0:T(8,128)(2,1)S(1)}, bf16[64,256]{1,0:T(8,128)(2,1)S(1)}, bf16[1,256]{1,0:T(2,128)(2,1)S(1)}, bf16[1,256]{1,0:T(2,128)(2,1)S(1)}) custom-call(bf16[1,2048]{1,0:T(2,128)(2,1)S(1)} %copy-done.3, bf16[2048,256]{1,0:T(8,128)(2,1)S(1)} %copy-done, bf16[2048,256]{1,0:T(8,128)(2,1)S(1)} %copy-done.1, ...), custom_call_target="tpu_custom_call" | custom-call | flops 1000000000 | bytes 2097152 | tf_op jit(solution)/shard_map/fresh/pallas_call | solution.py:208
  26.1 8.8 %all-to-all-done = bf16[16,16,256]{2,1,0:T(8,128)(2,1)S(1)} async-done(((bf16[16,16,256]{2,1,0:T(8,128)(2,1)}), bf16[16,16,256]{2,1,0:T(8,128)(2,1)S(1)}, u32[]{:S(2)}, u32[]{:S(2)}) %all-to-all-start) | async-done | bytes 131104 | tf_op jit(solution)/shard_map/all_to_all | solution.py:460
  35.0 5.4 %attend.1 = bf16[16,72,128]{2,1,0:T(8,128)(2,1)} custom-call(s32[1]{0:T(128)} %bitcast.refs_0_, bf16[256,256]{1,0:T(8,128)(2,1)S(1)} %bitcast.8, bf16[4,576,128]{2,1,0:T(8,128)(2,1)S(1)} %get-tuple-element.11.refs_3_.refs_2_, bf16[4,576,128]{2,1,0:T(8,128)(2,1)} %collective-permute-done.refs_4_.refs_3_, ...), custom_call_target="tpu_custom_call" | custom-call | flops 1107296256 | bytes 2097152 | tf_op jit(solution)/shard_map/attend/pallas_call | solution.py:320
  40.4 0.0 copy-start.7
  40.4 3.5 %all-to-all-start.1 = ((bf16[16,72,128]{2,1,0:T(8,128)(2,1)}), bf16[16,72,128]{2,1,0:T(8,128)(2,1)S(1)}, u32[]{:S(2)}, u32[]{:S(2)}) async-start(bf16[16,72,128]{2,1,0:T(8,128)(2,1)} %attend.1), calls=%async_computation.1 | async-start | bytes 589824 | tf_op jit(solution)/shard_map/all_to_all | solution.py:474
  44.6 0.0 copy-start.5
  44.6 0.0 copy-start.6
  44.6 0.0 copy-done.7
  44.6 0.6 copy-done.5
  45.3 0.0 copy-done.6
  45.3 0.0 copy-start.4
  45.3 1.2 %copy-done.4 = bf16[1,2048,2,128]{3,2,1,0:T(2,128)(2,1)S(1)} copy-done((bf16[1,2048,2,128]{3,2,1,0:T(2,128)(2,1)S(1)}, bf16[1,2048,2,128]{3,2,1,0:T(2,128)(2,1)}, u32[]{:S(2)}) %copy-start.4) | copy-done | bytes 1048600
  46.5 0.0 copy-start.2
  46.5 2.2 %decode.1.dec_out = bf16[1,256]{1,0:T(2,128)(2,1)S(1)} custom-call(bf16[1,256]{1,0:T(2,128)(2,1)S(1)} %copy-done.7, bf16[1,256]{1,0:T(2,128)(2,1)S(1)} %get-tuple-element.16.k_dec, bf16[1,256]{1,0:T(2,128)(2,1)S(1)} %get-tuple-element.17.v_dec, bf16[4096,128]{1,0:T(8,128)(2,1)S(1)} %bitcast.9, bf16[4096,128]{1,0:T(8,128)(2,1)} %bitcast.12, ...), custom_call_target="tpu_custom_call" | custom-call | flops 2000000000 | bytes 2097152 | tf_op jit(solution)/shard_map/decode/pallas_call | solution.py:168
  48.7 8.1 %all-to-all-done.1.parts = bf16[16,72,128]{2,1,0:T(8,128)(2,1)S(1)} async-done(((bf16[16,72,128]{2,1,0:T(8,128)(2,1)}), bf16[16,72,128]{2,1,0:T(8,128)(2,1)S(1)}, u32[]{:S(2)}, u32[]{:S(2)}) %all-to-all-start.1) | async-done | bytes 294944 | tf_op jit(solution)/shard_map/all_to_all | solution.py:474
  56.8 1.1 %combine.1 = bf16[4,24,256]{2,1,0:T(8,128)(2,1)S(1)} custom-call(bf16[16,72,128]{2,1,0:T(8,128)(2,1)S(1)} %all-to-all-done.1.parts, bf16[1,256]{1,0:T(2,128)(2,1)S(1)} %decode.1.dec_out, f32[2]{0:T(128)S(1)} %copy-done.5, f32[1,128]{1,0:T(1,128)S(1)} %bitcast.11), custom_call_target="tpu_custom_call" | custom-call | flops 100000000 | bytes 1048576 | tf_op jit(solution)/shard_map/combine/pallas_call | solution.py:375
  57.9 9.6 %all_to_all.15.heads = bf16[4,24,256]{2,1,0:T(8,128)(2,1)S(1)} all-to-all(bf16[4,24,256]{2,1,0:T(8,128)(2,1)S(1)} %combine.1), channel_id=1, replica_groups=mesh['kv'=64,'tp'=4] {'tp'}, dimensions={0} | all-to-all | bytes 98304 | tf_op jit(solution)/shard_map/all_to_all | solution.py:478
  67.5 0.0 copy-done.2
  67.5 0.9 %out_rows.1 = (bf16[16,512]{1,0:T(8,128)(2,1)}, bf16[1,512]{1,0:T(2,128)(2,1)}) custom-call(bf16[4,24,256]{2,1,0:T(8,128)(2,1)S(1)} %all_to_all.15.heads, bf16[1024,512]{1,0:T(8,128)(2,1)S(1)} %copy-done.2), custom_call_target="tpu_custom_call" | custom-call | flops 100000000 | bytes 1048576 | tf_op jit(solution)/shard_map/out_rows/pallas_call | solution.py:396
Async XLA Ops:
  0.6 23.4 %copy-start = (bf16[2048,256]{1,0:T(8,128)(2,1)S(1)}, bf16[2048,256]{1,0:T(8,128)(2,1)}, u32[]{:S(2)}) copy-start(bf16[2048,256]{1,0:T(8,128)(2,1)} %refs_1_.1) | copy-start | bytes 3145732
  0.6 23.4 %copy-start.1 = (bf16[2048,256]{1,0:T(8,128)(2,1)S(1)}, bf16[2048,256]{1,0:T(8,128)(2,1)}, u32[]{:S(2)}) copy-start(bf16[2048,256]{1,0:T(8,128)(2,1)} %refs_2_.1) | copy-start | bytes 3145732
  3.7 10.0 %collective-permute-start.1 = (bf16[4,576,128]{2,1,0:T(8,128)(2,1)S(1)}, bf16[4,576,128]{2,1,0:T(8,128)(2,1)S(1)}, u32[]{:S(2)}, u32[]{:S(2)}) collective-permute-start(bf16[4,576,128]{2,1,0:T(8,128)(2,1)S(1)} %get-tuple-element.11.refs_3_.refs_2_), channel_id=1, source_target_pairs={{0,32},{4,228},{8,40},{12,236},{16,48},{20,244},{24,56},{28,252},{... | collective-permute-start | bytes 1769480 | tf_op jit(solution)/shard_map/ppermute | solution.py:447
  5.6 18.4 %collective-permute-start = (bf16[4,576,128]{2,1,0:T(8,128)(2,1)S(1)}, bf16[4,576,128]{2,1,0:T(8,128)(2,1)}, u32[]{:S(2)}, u32[]{:S(2)}) collective-permute-start(bf16[4,576,128]{2,1,0:T(8,128)(2,1)S(1)} %get-tuple-element.11.refs_3_.refs_2_), channel_id=1, source_target_pairs={{0,4},{4,0},{8,12},{12,8},{16,20},{20,16},{24,28},{28,24},{32,36},... | collective-permute-start | bytes 1769480 | tf_op jit(solution)/shard_map/ppermute | solution.py:447
  13.7 10.3 %collective-permute-start.2 = (bf16[4,576,128]{2,1,0:T(8,128)(2,1)S(1)}, bf16[4,576,128]{2,1,0:T(8,128)(2,1)}, u32[]{:S(2)}, u32[]{:S(2)}) collective-permute-start(bf16[4,576,128]{2,1,0:T(8,128)(2,1)S(1)} %collective-permute-done.1.refs_5_.refs_4_), channel_id=1, source_target_pairs={{0,4},{4,0},{8,12},{12,8},{16,20},{20,16},{24,28},{28,24},{32,36},... | collective-permute-start | bytes 1769480 | tf_op jit(solution)/shard_map/ppermute | solution.py:447
  13.7 21.3 %all-to-all-start = ((bf16[16,16,256]{2,1,0:T(8,128)(2,1)}), bf16[16,16,256]{2,1,0:T(8,128)(2,1)S(1)}, u32[]{:S(2)}, u32[]{:S(2)}) async-start(bf16[16,16,256]{2,1,0:T(8,128)(2,1)} %get-tuple-element.10), calls=%async_computation | async-start | bytes 262144 | tf_op jit(solution)/shard_map/all_to_all | solution.py:460
  24.0 0.7 %copy-start.3 = (bf16[1,2048]{1,0:T(2,128)(2,1)S(1)}, bf16[1,2048]{1,0:T(2,128)(2,1)}, u32[]{:S(2)}) copy-start(bf16[1,2048]{1,0:T(2,128)(2,1)} %get-tuple-element.12.refs_0_) | copy-start | bytes 12292
  40.4 4.2 %copy-start.7 = (bf16[1,256]{1,0:T(2,128)(2,1)S(1)}, bf16[1,256]{1,0:T(2,128)(2,1)}, u32[]{:S(2)}) copy-start(bf16[1,256]{1,0:T(2,128)(2,1)} %get-tuple-element.15.q_dec) | copy-start | bytes 1540
  40.4 16.5 %all-to-all-start.1 = ((bf16[16,72,128]{2,1,0:T(8,128)(2,1)}), bf16[16,72,128]{2,1,0:T(8,128)(2,1)S(1)}, u32[]{:S(2)}, u32[]{:S(2)}) async-start(bf16[16,72,128]{2,1,0:T(8,128)(2,1)} %attend.1), calls=%async_computation.1 | async-start | bytes 589824 | tf_op jit(solution)/shard_map/all_to_all | solution.py:474
  44.6 0.7 copy-start.5
  44.6 0.7 copy-start.6
  45.3 1.2 %copy-start.4 = (bf16[1,2048,2,128]{3,2,1,0:T(2,128)(2,1)S(1)}, bf16[1,2048,2,128]{3,2,1,0:T(2,128)(2,1)}, u32[]{:S(2)}) copy-start(bf16[1,2048,2,128]{3,2,1,0:T(2,128)(2,1)} %param.25) | copy-start | bytes 3145732
  46.5 21.0 %copy-start.2 = (bf16[1024,512]{1,0:T(8,128)(2,1)S(1)}, bf16[1024,512]{1,0:T(8,128)(2,1)}, u32[]{:S(2)}) copy-start(bf16[1024,512]{1,0:T(8,128)(2,1)} %w.3) | copy-start | bytes 3145732
